TPU v7x, 512 devices: a whole 4x4x16 slice. The times are simulated.
512 devices in a mesh: sp: 16 (over z), dp: 32 (over y, x, core).
Axes of the slice: x: 4, y: 4, z: 16, core: 2. Of those that a mesh axis runs over, the one named last changes fastest.
Arguments:
- normed: bfloat16 [32, 1024, 2048], P('dp', None, 'sp'), may hold values from -6 to 6
- branch_in: bfloat16 [32, 1024, 2048], P('dp', 'sp'), may hold values from -12 to 12
- gate_pre: bfloat16 [32, 1024, 2048], P('dp', 'sp'), may hold values from -6 to 6
- cotangent: bfloat16 [32, 1024, 2048], P('dp', None, 'sp'), may hold values from -6 to 6
- decay_shift: float32 [32, 16, 2048], P('dp', 'sp'), may hold values from -1.2 to -9.765625e-05
- conv_weight: float32 [4, 1024], P(None, 'sp'), may hold values from -3 to 3
- recur_weight: float32 [16, 64, 64], P('sp'), may hold values from -0.75 to 0.75
- input_weight: float32 [16, 64, 64], P('sp'), may hold values from -0.75 to 0.75
- decay_param: float32 [1024], P('sp')
- branch_proj: bfloat16 [1024, 1024], P('dp'), may hold values from -0.1875 to 0.1875
Outputs:
- grad_normed: bfloat16 [32, 1024, 2048], P('dp', None, 'sp')
- grad_gate: bfloat16 [32, 1024, 2048], P('dp', 'sp')
- grad_proj: float32 [1024, 1024], P('dp', 'sp')
- grad_conv: float32 [4, 1024], P(None, 'sp')
- grad_recur: float32 [16, 64, 64], P('sp')
- grad_input: float32 [16, 64, 64], P('sp')
- grad_decay: float32 [1024], P('sp')
All inputs are finite; a program needn't handle non-finite values.
Results may differ from a plain program's by a relative error of at most 0.019.
Values may be sent and summed in bfloat16 or wider, within the bound.
No kernel may reach another device: no remote copies, remote signals or barrier semaphores. Data moves between devices by JAX's collectives and lax.ppermute only.
A program may use at most 64 MiB of HBM per device.

v0:
```python
import math

import jax
import jax.numpy as jnp
from jax import lax
from jax.sharding import PartitionSpec as P

BLOCK_W = 64
CONV = 4


gate_const = 8.0
far_below = -1e30


def from_everyone(array, axis):
    size = lax.axis_size(axis)
    return lax.all_to_all(
        jnp.broadcast_to(array[None], (size, *array.shape)), axis, 0, 0, tiled=True
    )


def taken_together(array, axis):
    return from_everyone(array, axis).astype(jnp.float32).sum(axis=0)


def in_blocks(array, dim, size):
    before, after = (array.shape[:dim], array.shape[dim + 1 :])
    return jnp.moveaxis(array.reshape(*before, size, -1, *after), dim, 0)


def summed_on_arrival(array, axis, dim):
    pieces = in_blocks(array, dim, lax.axis_size(axis))
    arrived = lax.all_to_all(pieces, axis, split_axis=0, concat_axis=0, tiled=True)
    return arrived.sum(axis=0)


def block_states(log_decay, pushed):
    channels, length = pushed.shape
    span_len = math.gcd(length, 128)
    count = length // span_len
    logs = log_decay.reshape(channels, count, span_len).transpose(1, 0, 2)
    inputs = pushed.reshape(channels, count, span_len).transpose(1, 0, 2)
    places = jnp.arange(span_len)
    lower = places[:, None] >= places[None, :]

    @jax.checkpoint
    def advance(carry, items):
        block_logs, block_inputs = items
        running = jnp.cumsum(block_logs, axis=1)
        spread = running[:, :, None] - running[:, None, :]
        weights = jnp.exp(jnp.where(lower[None], spread, far_below))
        inner = jnp.einsum("cts,cs->ct", weights, block_inputs)
        states = inner + jnp.exp(running) * carry[:, None]
        return (states[:, -1], states)

    start = jnp.zeros((channels,), jnp.float32)
    _, blocks = lax.scan(advance, start, (logs, inputs))
    return blocks.transpose(1, 0, 2).reshape(channels, length)


def mixer(branch, gate, shift, conv_weight, recur_weight, input_weight, decay_param):
    channels, length = branch.shape
    padded = jnp.pad(branch, ((0, 0), (CONV - 1, 0)))
    convolved = conv_weight[0][:, None] * padded[:, 0:length]
    for offset in range(1, CONV):
        convolved = convolved + conv_weight[offset][:, None] * padded[:, offset : offset + length]
    groups = channels // BLOCK_W
    grouped = convolved.reshape(groups, BLOCK_W, length)
    recur_gate = jax.nn.sigmoid(
        jnp.einsum("gil,gij->gjl", grouped, recur_weight).reshape(channels, length)
    )
    input_gate = jax.nn.sigmoid(
        jnp.einsum("gil,gij->gjl", grouped, input_weight).reshape(channels, length)
    )
    log_decay = -gate_const * recur_gate * jax.nn.softplus(-decay_param)[:, None] + jnp.repeat(
        shift, BLOCK_W, axis=0
    )
    pushed = jnp.sqrt(-jnp.expm1(2.0 * log_decay)) * input_gate * convolved
    states = block_states(log_decay, pushed)
    return states * jax.nn.gelu(gate)


def mixer_grads(
    branch, gate, shift, upstream, conv_weight, recur_weight, input_weight, decay_param
):

    def local(branch_f, gate_f, conv_f, recur_f, input_f, decay_f):
        return mixer(branch_f, gate_f, shift, conv_f, recur_f, input_f, decay_f)

    _, pullback = jax.vjp(
        local,
        branch.astype(jnp.float32),
        gate.astype(jnp.float32),
        conv_weight,
        recur_weight,
        input_weight,
        decay_param,
    )
    return pullback(upstream.astype(jnp.float32))


def body(
    normed,
    branch_in,
    gate_pre,
    cotangent,
    decay_shift,
    conv_weight,
    recur_weight,
    input_weight,
    decay_param,
    branch_proj,
):
    heads_cot = lax.all_to_all(cotangent, "sp", split_axis=1, concat_axis=2, tiled=True)
    grad_branch, grad_gate, grad_conv, grad_recur, grad_input, grad_decay = mixer_grads(
        branch_in[0],
        gate_pre[0],
        decay_shift[0],
        heads_cot[0],
        conv_weight,
        recur_weight,
        input_weight,
        decay_param,
    )
    small_sums = (
        taken_together(grad_conv.astype(jnp.bfloat16), "dp").astype(jnp.float32),
        taken_together(grad_recur.astype(jnp.bfloat16), "dp").astype(jnp.float32),
        taken_together(grad_input.astype(jnp.bfloat16), "dp").astype(jnp.float32),
        taken_together(grad_decay.astype(jnp.bfloat16), "dp").astype(jnp.float32),
    )
    branch_rounded = grad_branch.astype(jnp.bfloat16)[None]
    token_grad = lax.all_to_all(branch_rounded, "sp", split_axis=2, concat_axis=1, tiled=True)[0]
    grad_normed = jnp.dot(
        lax.all_gather(branch_proj, "dp", axis=0, tiled=True),
        token_grad,
        preferred_element_type=jnp.float32,
    ).astype(jnp.bfloat16)[None]
    partial_sum = lax.dot_general(
        normed[0], token_grad, (((1,), (1,)), ((), ())), preferred_element_type=jnp.float32
    )
    received = lax.all_to_all(
        partial_sum[None].astype(jnp.bfloat16), "dp", split_axis=1, concat_axis=0, tiled=True
    ).astype(jnp.float32)
    row_block = jnp.sum(received, axis=0)
    seq_count = lax.axis_size("sp")
    rows_here = row_block.shape[0]
    width_share = row_block.shape[1] // seq_count
    stacked = (
        row_block.reshape(rows_here, seq_count, width_share)
        .transpose(1, 0, 2)
        .reshape(seq_count * rows_here, width_share)
    )
    grad_proj = summed_on_arrival(stacked, "sp", 0)
    return (
        grad_normed,
        grad_gate.astype(jnp.bfloat16)[None],
        grad_proj,
        small_sums[0],
        small_sums[1],
        small_sums[2],
        small_sums[3],
    )


def solution(mesh):
    return jax.shard_map(
        body,
        mesh=mesh,
        in_specs=(
            P("dp", None, "sp"),
            P("dp", "sp", None),
            P("dp", "sp", None),
            P("dp", None, "sp"),
            P("dp", "sp", None),
            P(None, "sp"),
            P("sp", None, None),
            P("sp", None, None),
            P("sp"),
            P("dp", None),
        ),
        out_specs=(
            P("dp", None, "sp"),
            P("dp", "sp", None),
            P("dp", "sp"),
            P(None, "sp"),
            P("sp", None, None),
            P("sp", None, None),
            P("sp"),
        ),
        check_vma=False,
    )
```

profile of v0, /device:TPU:32, one launch (start us, length us, event | category | flops | bytes accessed | tf_op | source)
XLA Modules:
  0.0 544.2 jit_solution(5228442166205995358)
XLA Ops:
  12.1 15.3 %all-to-all-start = ((bf16[16,2,4096]{2,1,0:T(2,128)(2,1)}), bf16[16,2,4096]{2,1,0:T(2,128)(2,1)}, u32[]{:S(2)}, u32[]{:S(2)}) async-start(bf16[16,2,4096]{2,1,0:T(2,128)(2,1)} %reshape.247), calls=%async_computation | async-start | bytes 524288 | tf_op jit(solution)/shard_map/all_to_all | solution.py:115
  33.8 11.7 %all-to-all-done = bf16[16,2,4096]{2,1,0:T(2,128)(2,1)} async-done(((bf16[16,2,4096]{2,1,0:T(2,128)(2,1)}), bf16[16,2,4096]{2,1,0:T(2,128)(2,1)}, u32[]{:S(2)}, u32[]{:S(2)}) %all-to-all-start) | async-done | bytes 262176 | tf_op jit(solution)/shard_map/all_to_all | solution.py:115
  49.6 83.9 %while.35 = (s32[]{:T(128)}, f32[64]{0:T(128)S(1)}, f32[16,64,128]{2,1,0:T(8,128)S(1)}, f32[16,64]{1,0:T(8,128)}, f32[16,64,128]{2,1,0:T(8,128)}, /*index=5*/f32...) while((s32[]{:T(128)}, f32[64]{0:T(128)S(1)}, ...), condition=%wide.region_2.3_spmd.clone, body=%wide.region_0.2_spmd.clone.sunk | while | flops 5251074 | bytes 444033 | solution.py:58
  134.9 218.0 %while.36 = (s32[]{:T(128)}, f32[64]{0:T(128)}, f32[16,64,128]{2,1,0:T(8,128)S(1)}, f32[16,64,128]{2,1,0:T(8,128)S(1)}, f32[16,64]{1,0:T(8,128)}, /*index=5*/f32...) while((s32[]{:T(128)}, f32[64]{0:T(128)}, ...), condition=%wide.region_9.10_spmd.clone, body=%wide.region_3.9_spmd.clone.sunk | while | flops 13680579 | bytes 1035185 | solution.py:58
  142.8 3.7 fusion.121
  156.4 3.7 fusion.121
  170.0 3.7 fusion.121
  183.6 3.7 fusion.121
  197.3 3.7 fusion.121
  210.9 3.7 fusion.121
  224.5 3.7 fusion.121
  238.2 3.7 fusion.121
  251.8 3.7 fusion.121
  265.4 3.7 fusion.121
  279.0 3.7 fusion.121
  292.7 3.7 fusion.121
  306.3 3.7 fusion.121
  358.1 7.5 %all-to-all-start.7 = ((bf16[32,1,64]{2,1,0:T(2,128)(2,1)}), bf16[32,1,64]{2,1,0:T(2,128)(2,1)S(1)}, u32[]{:S(2)}, u32[]{:S(2)}) async-start(bf16[32,1,64]{2,1,0:T(2,128)(2,1)} %broadcast_in_dim.155), calls=%async_computation.7 | async-start | bytes 32768 | tf_op jit(solution)/shard_map/all_to_all | solution.py:18
  372.7 5.4 all-to-all-start.4
  383.0 12.3 %reduce.6 = bf16[2048,64]{1,0:T(8,128)(2,1)} reduce(bf16[2048,1,64]{2,1,0:T(2,128)(2,1)S(1)} %bitcast.290, bf16[]{:T(256)} %broadcast.168), dimensions={1}, to_apply=%bitcast.184.reduce_sub_computation | reduce | bytes 524290
  397.5 6.3 %all-to-all-start.1 = ((bf16[16,2,4096]{2,1,0:T(2,128)(2,1)}), bf16[16,2,4096]{2,1,0:T(2,128)(2,1)S(1)}, u32[]{:S(2)}, u32[]{:S(2)}) async-start(bf16[16,2,4096]{2,1,0:T(2,128)(2,1)} %reshape.249), calls=%async_computation.1 | async-start | bytes 524288 | tf_op jit(solution)/shard_map/all_to_all | solution.py:133
  407.0 15.2 %all-to-all-done.1 = bf16[16,2,4096]{2,1,0:T(2,128)(2,1)S(1)} async-done(((bf16[16,2,4096]{2,1,0:T(2,128)(2,1)}), bf16[16,2,4096]{2,1,0:T(2,128)(2,1)S(1)}, u32[]{:S(2)}, u32[]{:S(2)}) %all-to-all-start.1) | async-done | bytes 262176 | tf_op jit(solution)/shard_map/all_to_all | solution.py:133
  422.2 7.3 %all-to-all-start.6 = ((bf16[32,2,2048]{2,1,0:T(2,128)(2,1)}), bf16[32,2,2048]{2,1,0:T(2,128)(2,1)S(1)}, u32[]{:S(2)}, u32[]{:S(2)}) async-start(bf16[32,2,2048]{2,1,0:T(2,128)(2,1)} %reshape.259), calls=%async_computation.6 | async-start | bytes 524288 | tf_op jit(solution)/shard_map/all_to_all | solution.py:18
  432.4 6.3 %all-to-all-done.6 = bf16[32,2,2048]{2,1,0:T(2,128)(2,1)S(1)} async-done(((bf16[32,2,2048]{2,1,0:T(2,128)(2,1)}), bf16[32,2,2048]{2,1,0:T(2,128)(2,1)S(1)}, u32[]{:S(2)}, u32[]{:S(2)}) %all-to-all-start.6) | async-done | bytes 262176 | tf_op jit(solution)/shard_map/all_to_all | solution.py:18
  438.7 4.8 all-to-all-start.5
  444.4 7.7 %copy.152 = bf16[1,1024,1024]{2,0,1:T(2,128)(2,1)} copy(bf16[1,1024,1024]{1,2,0:T(8,128)(2,1)S(1)} %convert_bitcast_fusion) | data formatting | bytes 4194304 | tf_op jit(solution)/shard_map/convert_element_type | solution.py:143
  452.1 12.8 %reduce.7 = bf16[1024,1024]{1,0:T(8,128)(2,1)S(1)} reduce(bf16[1024,1,1024]{2,1,0:T(2,128)(2,1)} %bitcast.284, bf16[]{:T(256)} %broadcast.168), dimensions={1}, to_apply=%bitcast.186.reduce_sub_computation | reduce | bytes 4194306
  467.7 7.2 %all-to-all-start.2 = ((bf16[32,2,16384]{2,1,0:T(2,128)(2,1)}), bf16[32,2,16384]{2,1,0:T(2,128)(2,1)S(1)}, u32[]{:S(2)}, u32[]{:S(2)}) async-start(bf16[32,2,16384]{2,1,0:T(2,128)(2,1)} %reshape.251), calls=%async_computation.2 | async-start | bytes 4194304 | tf_op jit(solution)/shard_map/all_to_all | solution.py:142
  485.0 20.0 %all-to-all-done.2 = bf16[32,2,16384]{2,1,0:T(2,128)(2,1)S(1)} async-done(((bf16[32,2,16384]{2,1,0:T(2,128)(2,1)}), bf16[32,2,16384]{2,1,0:T(2,128)(2,1)S(1)}, u32[]{:S(2)}, u32[]{:S(2)}) %all-to-all-start.2) | async-done | bytes 2097184 | tf_op jit(solution)/shard_map/all_to_all | solution.py:142
  505.0 6.8 %reshape.252 = bf16[1024,1,1024]{2,1,0:T(2,128)(2,1)} reshape(bf16[32,2,16384]{2,1,0:T(2,128)(2,1)S(1)} %all-to-all-done.2) | data formatting | bytes 4194304
  516.2 6.1 %all-to-all-start.3 = ((f32[16,1,2048]{2,1,0:T(1,128)}), f32[16,1,2048]{2,1,0:T(1,128)S(1)}, u32[]{:S(2)}, u32[]{:S(2)}) async-start(f32[16,1,2048]{2,1,0:T(1,128)} %reshape.253), calls=%async_computation.3 | async-start | bytes 262144 | tf_op jit(solution)/shard_map/all_to_all | solution.py:34
  527.1 8.1 %all-to-all-done.3 = f32[16,1,2048]{2,1,0:T(1,128)S(1)} async-done(((f32[16,1,2048]{2,1,0:T(1,128)}), f32[16,1,2048]{2,1,0:T(1,128)S(1)}, u32[]{:S(2)}, u32[]{:S(2)}) %all-to-all-start.3) | async-done | bytes 131104 | tf_op jit(solution)/shard_map/all_to_all | solution.py:34
  (464 shorter events, 320.2 us)
Async XLA Ops:
  7.2 436.5 %copy-start = (bf16[1,1024,128]{2,1,0:T(8,128)(2,1)S(1)}, bf16[1,1024,128]{2,1,0:T(8,128)(2,1)}, u32[]{:S(2)}) copy-start(bf16[1,1024,128]{2,1,0:T(8,128)(2,1)} %param.14) | copy-start | bytes 786436
  7.2 23.8 %copy-start.23 = (f32[64]{0:T(128)S(1)}, f32[64]{0:T(128)}, u32[]{:S(2)}) copy-start(f32[64]{0:T(128)} %param.22) | copy-start | bytes 772
  7.2 24.5 %copy-start.10 = (f32[1,64,64]{2,1,0:T(8,128)S(1)}, f32[1,64,64]{2,1,0:T(8,128)}, u32[]{:S(2)}) copy-start(f32[1,64,64]{2,1,0:T(8,128)} %param.20) | copy-start | bytes 49156
  7.2 24.8 %copy-start.12 = (f32[1,64,64]{2,1,0:T(8,128)S(1)}, f32[1,64,64]{2,1,0:T(8,128)}, u32[]{:S(2)}) copy-start(f32[1,64,64]{2,1,0:T(8,128)} %param.21) | copy-start | bytes 49156
  12.1 20.3 %copy-start.8 = (f32[1,1,2048]{2,1,0:T(1,128)S(1)}, f32[1,1,2048]{2,1,0:T(1,128)}, u32[]{:S(2)}) copy-start(f32[1,1,2048]{2,1,0:T(1,128)} %param.18) | copy-start | bytes 24580
  12.1 33.4 %all-to-all-start = ((bf16[16,2,4096]{2,1,0:T(2,128)(2,1)}), bf16[16,2,4096]{2,1,0:T(2,128)(2,1)}, u32[]{:S(2)}, u32[]{:S(2)}) async-start(bf16[16,2,4096]{2,1,0:T(2,128)(2,1)} %reshape.247), calls=%async_computation | async-start | bytes 524288 | tf_op jit(solution)/shard_map/all_to_all | solution.py:115
  31.7 17.9 %copy-start.20 = (f32[64]{0:T(128)}, f32[64]{0:T(128)S(1)}, u32[]{:S(2)}) copy-start(f32[64]{0:T(128)S(1)} %get-tuple-element.393) | copy-start | bytes 772
  139.5 7.0 %copy-start.19 = (f32[64]{0:T(128)S(1)}, f32[64]{0:T(128)}, u32[]{:S(2)}) copy-start(f32[64]{0:T(128)} %fusion.120) | copy-start | bytes 772 | tf_op jit(solution)/shard_map/transpose(jvp())/while
  166.7 7.0 %copy-start.19 = (f32[64]{0:T(128)S(1)}, f32[64]{0:T(128)}, u32[]{:S(2)}) copy-start(f32[64]{0:T(128)} %fusion.120) | copy-start | bytes 772 | tf_op jit(solution)/shard_map/transpose(jvp())/while
  180.4 7.0 %copy-start.19 = (f32[64]{0:T(128)S(1)}, f32[64]{0:T(128)}, u32[]{:S(2)}) copy-start(f32[64]{0:T(128)} %fusion.120) | copy-start | bytes 772 | tf_op jit(solution)/shard_map/transpose(jvp())/while
  194.0 7.0 %copy-start.19 = (f32[64]{0:T(128)S(1)}, f32[64]{0:T(128)}, u32[]{:S(2)}) copy-start(f32[64]{0:T(128)} %fusion.120) | copy-start | bytes 772 | tf_op jit(solution)/shard_map/transpose(jvp())/while
  234.9 7.0 %copy-start.19 = (f32[64]{0:T(128)S(1)}, f32[64]{0:T(128)}, u32[]{:S(2)}) copy-start(f32[64]{0:T(128)} %fusion.120) | copy-start | bytes 772 | tf_op jit(solution)/shard_map/transpose(jvp())/while
  248.5 7.0 %copy-start.19 = (f32[64]{0:T(128)S(1)}, f32[64]{0:T(128)}, u32[]{:S(2)}) copy-start(f32[64]{0:T(128)} %fusion.120) | copy-start | bytes 772 | tf_op jit(solution)/shard_map/transpose(jvp())/while
  262.1 7.0 %copy-start.19 = (f32[64]{0:T(128)S(1)}, f32[64]{0:T(128)}, u32[]{:S(2)}) copy-start(f32[64]{0:T(128)} %fusion.120) | copy-start | bytes 772 | tf_op jit(solution)/shard_map/transpose(jvp())/while
  303.0 7.0 %copy-start.19 = (f32[64]{0:T(128)S(1)}, f32[64]{0:T(128)}, u32[]{:S(2)}) copy-start(f32[64]{0:T(128)} %fusion.120) | copy-start | bytes 772 | tf_op jit(solution)/shard_map/transpose(jvp())/while
  316.6 7.0 %copy-start.19 = (f32[64]{0:T(128)S(1)}, f32[64]{0:T(128)}, u32[]{:S(2)}) copy-start(f32[64]{0:T(128)} %fusion.120) | copy-start | bytes 772 | tf_op jit(solution)/shard_map/transpose(jvp())/while
  353.0 13.8 %copy-start.9 = (f32[1,1,2048]{2,1,0:T(1,128)S(1)}, f32[1,1,2048]{2,1,0:T(1,128)}, u32[]{:S(2)}) copy-start(f32[1,1,2048]{2,1,0:T(1,128)} %param.18) | copy-start | bytes 24580
  353.0 13.8 %copy-start.11 = (f32[1,64,64]{2,1,0:T(8,128)S(1)}, f32[1,64,64]{2,1,0:T(8,128)}, u32[]{:S(2)}) copy-start(f32[1,64,64]{2,1,0:T(8,128)} %param.20) | copy-start | bytes 49156
  353.0 13.8 %copy-start.14 = (f32[64]{0:T(128)S(1)}, f32[64]{0:T(128)}, u32[]{:S(2)}) copy-start(f32[64]{0:T(128)} %copy-done.13) | copy-start | bytes 772
  353.0 13.8 %copy-start.16 = (f32[64]{0:T(128)S(1)}, f32[64]{0:T(128)}, u32[]{:S(2)}) copy-start(f32[64]{0:T(128)} %copy-done.15) | copy-start | bytes 772
  358.1 14.6 %all-to-all-start.7 = ((bf16[32,1,64]{2,1,0:T(2,128)(2,1)}), bf16[32,1,64]{2,1,0:T(2,128)(2,1)S(1)}, u32[]{:S(2)}, u32[]{:S(2)}) async-start(bf16[32,1,64]{2,1,0:T(2,128)(2,1)} %broadcast_in_dim.155), calls=%async_computation.7 | async-start | bytes 32768 | tf_op jit(solution)/shard_map/all_to_all | solution.py:18
  370.1 34.4 %copy-start.2 = (f32[64,2048]{1,0:T(8,128)S(1)}, f32[64,2048]{1,0:T(8,128)}, u32[]{:S(2)}) copy-start(f32[64,2048]{1,0:T(8,128)} %copy-done.1) | copy-start | bytes 1572868
  372.7 24.8 %all-to-all-start.4 = ((bf16[32,2,128]{2,1,0:T(2,128)(2,1)}), bf16[32,2,128]{2,1,0:T(2,128)(2,1)S(1)}, u32[]{:S(2)}, u32[]{:S(2)}) async-start(bf16[32,2,128]{2,1,0:T(2,128)(2,1)} %reshape.255), calls=%async_computation.4 | async-start | bytes 32768 | tf_op jit(solution)/shard_map/all_to_all | solution.py:18
  378.1 51.4 %copy-start.22 = (f32[64]{0:T(128)S(1)}, f32[64]{0:T(128)}, u32[]{:S(2)}) copy-start(f32[64]{0:T(128)} %get-tuple-element.394) | copy-start | bytes 772
  397.5 24.7 %all-to-all-start.1 = ((bf16[16,2,4096]{2,1,0:T(2,128)(2,1)}), bf16[16,2,4096]{2,1,0:T(2,128)(2,1)S(1)}, u32[]{:S(2)}, u32[]{:S(2)}) async-start(bf16[16,2,4096]{2,1,0:T(2,128)(2,1)} %reshape.249), calls=%async_computation.1 | async-start | bytes 524288 | tf_op jit(solution)/shard_map/all_to_all | solution.py:133
  403.7 120.1 %all-gather.2.cloned.1.call-start = ((), (), s32[]{:S(2)}) async-start(), calls=%async_computation.8 | async-start | bytes 2162688 | tf_op jit(solution)/shard_map/all_gather | solution.py:135
  422.2 16.5 %all-to-all-start.6 = ((bf16[32,2,2048]{2,1,0:T(2,128)(2,1)}), bf16[32,2,2048]{2,1,0:T(2,128)(2,1)S(1)}, u32[]{:S(2)}, u32[]{:S(2)}) async-start(bf16[32,2,2048]{2,1,0:T(2,128)(2,1)} %reshape.259), calls=%async_computation.6 | async-start | bytes 524288 | tf_op jit(solution)/shard_map/all_to_all | solution.py:18
  438.7 29.0 %all-to-all-start.5 = ((bf16[32,2,2048]{2,1,0:T(2,128)(2,1)}), bf16[32,2,2048]{2,1,0:T(2,128)(2,1)}, u32[]{:S(2)}, u32[]{:S(2)}) async-start(bf16[32,2,2048]{2,1,0:T(2,128)(2,1)} %reshape.257), calls=%async_computation.5 | async-start | bytes 524288 | tf_op jit(solution)/shard_map/all_to_all | solution.py:18
  467.7 14.8 %copy-start.7 = (bf16[32,2,2048]{2,1,0:T(2,128)(2,1)S(1)}, bf16[32,2,2048]{2,1,0:T(2,128)(2,1)}, u32[]{:S(2)}) copy-start(bf16[32,2,2048]{2,1,0:T(2,128)(2,1)} %copy-done.6) | copy-start | bytes 786436
  467.7 37.3 %all-to-all-start.2 = ((bf16[32,2,16384]{2,1,0:T(2,128)(2,1)}), bf16[32,2,16384]{2,1,0:T(2,128)(2,1)S(1)}, u32[]{:S(2)}, u32[]{:S(2)}) async-start(bf16[32,2,16384]{2,1,0:T(2,128)(2,1)} %reshape.251), calls=%async_computation.2 | async-start | bytes 4194304 | tf_op jit(solution)/shard_map/all_to_all | solution.py:142
  511.8 11.3 %copy-start.4 = (bf16[32,1,64,64]{3,2,1,0:T(8,128)(2,1)S(1)}, bf16[32,1,64,64]{3,2,1,0:T(8,128)(2,1)}, u32[]{:S(2)}) copy-start(bf16[32,1,64,64]{3,2,1,0:T(8,128)(2,1)} %reshape.258) | copy-start | bytes 786436
  516.2 18.9 %all-to-all-start.3 = ((f32[16,1,2048]{2,1,0:T(1,128)}), f32[16,1,2048]{2,1,0:T(1,128)S(1)}, u32[]{:S(2)}, u32[]{:S(2)}) async-start(f32[16,1,2048]{2,1,0:T(1,128)} %reshape.253), calls=%async_computation.3 | async-start | bytes 262144 | tf_op jit(solution)/shard_map/all_to_all | solution.py:34
  (17 other events, 88.7 us)
Sparse Core Ops, SparseCore 0:
  407.7 59.8 all-gather.1
where the time goes:
time: 553 us; the launch traced here: 544 us
  local copies, waits for them, and re-layouts  175 us (32%)
  other arithmetic  149 us (27%)
  matrix products  80.8 us (15%)
  waiting for transfers between devices  63.8 us (12%)
  starting transfers between devices  60 us (11%)
  between operations  14.6 us (3%)
    dot_general x32, matrix products, advance(): inner = jnp.einsum('cts,cs->ct', weights, block_inputs)  71 us
    squeeze x80, local copies, waits for them, and re-layouts, block_states(): _, blocks = lax.scan(advance, start, (logs, inputs))  68.2 us
    reduce_sum x16, other arithmetic, advance(): spread = running[:, :, None] - running[:, None, :]  58.7 us
    dynamic_update_slice x32, local copies, waits for them, and re-layouts, block_states(): _, blocks = lax.scan(advance, start, (logs, inputs))  33.1 us
    another operation x64, other arithmetic, advance(): running = jnp.cumsum(block_logs, axis=1)  30.4 us
    unnamed x4, other arithmetic  28.3 us
    unnamed x67, local copies, waits for them, and re-layouts  25.5 us
    all_to_all x4, starting transfers between devices, from_everyone(): lax.all_to_all(jnp.broadcast_to(array[None], (size, *array.shape)), axis,...  25 us
  transfers between devices with their start and end apart: 9, of which 6 were waited for; matrix products, arithmetic and copies ran while one was open for 16% of the time, Pallas kernels for 0%

commit v1 on v0

v1 whole, which is shorter than its diff:
```python
import jax
import jax.numpy as jnp
from jax import lax
from jax.experimental import pallas as pl
from jax.experimental.pallas import tpu as pltpu
from jax.sharding import Mesh
from jax.sharding import PartitionSpec as P

SPAN = 128
GROUP = 64
CONV = 4
GATE = 8.0
f32 = jnp.float32
bf16 = jnp.bfloat16
DP = ("y", "x", "core")
NEAREST = (0, 1, 3, 2)


def lanes(shape):
    return lax.broadcasted_iota(jnp.int32, shape, 1)


def high_low(value):
    high = value.astype(bf16)
    return high, (value - high.astype(f32)).astype(bf16)


def strided(ref, n):
    return ref[pl.ds(n, SPAN, stride=8), :]


def before_of(block):
    row = lax.broadcasted_iota(jnp.int32, block.shape, 0)
    lane = lanes(block.shape)
    moved = pltpu.roll(block, 1, 0)
    across = jnp.where(lane >= GROUP, pltpu.roll(moved, GROUP, 1), 0.0)
    return jnp.where(row == 0, across, moved)


def after_of(block):
    row = lax.broadcasted_iota(jnp.int32, block.shape, 0)
    lane = lanes(block.shape)
    moved = pltpu.roll(block, 7, 0)
    across = jnp.where(lane < GROUP, pltpu.roll(moved, GROUP, 1), 0.0)
    return jnp.where(row == 7, across, moved)


def entering(factor, value, backward):
    row = lax.broadcasted_iota(jnp.int32, factor.shape, 0)
    lane = lanes(factor.shape)
    a, b = factor, value
    for step in (1, 2, 4):
        inside = row < 8 - step if backward else row >= step
        shift = 8 - step if backward else step
        b = b + a * jnp.where(inside, pltpu.roll(b, shift, 0), 0.0)
        a = a * jnp.where(inside, pltpu.roll(a, shift, 0), 1.0)
    edge = b[0:1] if backward else b[7:8]
    later = lane < GROUP if backward else lane >= GROUP
    base = jnp.where(later, jnp.broadcast_to(pltpu.roll(edge, GROUP, 1), factor.shape), 0.0)
    total = b + a * base
    return after_of(total) if backward else before_of(total)


def block_of(n):
    return pl.ds(pl.multiple_of(n * SPAN, SPAN), SPAN)


def moved_block(n, rows):
    return pl.ds(pl.multiple_of(n * SPAN + rows, 8), SPAN)


def tiled(row):
    return jnp.broadcast_to(row, (SPAN, SPAN))


def halves(top, low):
    return jnp.concatenate([top, low], axis=0)


def forward_kernel(
    branch, gate, shift, conv, decay_param, recur_map, input_map,
    next_o, c0_o, c1_o, c2_o, c3_o, branch_o, turned_o, g0_o, g1_o, back_o, rows,
    b_s, decay_s, fed_s, slope_s, rate_s, recur_s, local_s, power_s,
):
    lane = lanes((GROUP, SPAN))
    minus = -decay_param[...]
    softened = jnp.maximum(minus, 0.0) + jnp.log1p(jnp.exp(-jnp.abs(minus)))
    table = jnp.concatenate(
        [conv[...], -GATE * softened, GATE * (0.5 + 0.5 * jnp.tanh(0.5 * minus)), jnp.zeros((2, GROUP), f32)], axis=0
    )
    rows[...] = jnp.concatenate([table, table], axis=1)
    both = jnp.concatenate([recur_map[...], input_map[...]], axis=1)
    swapped = pltpu.roll(both, GROUP, 1)
    left = lane < GROUP
    first = halves(jnp.where(left, both, 0.0), jnp.where(left, 0.0, swapped))
    second = halves(jnp.where(left, swapped, 0.0), jnp.where(left, 0.0, both))
    w_high, w_low = high_low(jnp.concatenate([first, second], axis=1))
    back_high, back_low = high_low(halves(jnp.transpose(first), jnp.transpose(second)))
    back_o[0] = back_high
    back_o[1] = back_low
    for p in range(8):
        at = slice(p * SPAN, (p + 1) * SPAN)
        far = slice((8 + p) * SPAN, (9 + p) * SPAN)
        b_s[pl.ds(24 + p, SPAN, stride=8), :] = jnp.transpose(
            halves(branch[:, at].astype(f32), branch[:, far].astype(f32))
        )
        fed_s[pl.ds(p, SPAN, stride=8), :] = jnp.transpose(
            halves(
                jnp.broadcast_to(shift[:, at], (GROUP, SPAN)), jnp.broadcast_to(shift[:, far], (GROUP, SPAN))
            )
        )
    for m in range(3):
        b_s[8 * m : 8 * m + 8, :] = before_of(b_s[1024 + 8 * m : 1032 + 8 * m, :])

    def gates(n, _):
        here = block_of(n)
        x = tiled(rows[0:1, :]) * b_s[here, :]
        for k in (1, 2, 3):
            x = x + tiled(rows[k : k + 1, :]) * b_s[moved_block(n, 8 * k), :]
        branch_o[here, :] = b_s[moved_block(n, 24), :].astype(bf16)
        x_high, x_low = high_low(x)
        pre = (
            jnp.dot(x_high, w_high, preferred_element_type=f32)
            + jnp.dot(x_low, w_high, preferred_element_type=f32)
            + jnp.dot(x_high, w_low, preferred_element_type=f32)
        )
        tr = jnp.tanh(0.5 * pre[:, :SPAN])
        ti = jnp.tanh(0.5 * pre[:, SPAN:])
        recur = 0.5 + 0.5 * tr
        inp = 0.5 + 0.5 * ti
        rate = tiled(rows[4:5, :])
        log = rate * recur + fed_s[here, :]
        decay = jnp.exp(log)
        square = decay * decay
        u = 2.0 * log
        series = -u * (1 + u * (1 / 2) * (1 + u * (1 / 3) * (1 + u * (1 / 4) * (1 + u * (1 / 5) * (1 + u * (1 / 6))))))
        left_over = jnp.where(u > -0.25, series, 1.0 - square)
        inverse = lax.rsqrt(left_over)
        root = left_over * inverse
        fed = inp * x
        pushed = root * fed
        decay_s[here, :] = decay
        fed_s[here, :] = pushed
        slope_s[here, :] = square * inverse * fed
        rate_s[here, :] = rate * (0.25 - 0.25 * tr * tr)
        recur_s[here, :] = recur
        c0_o[here, :] = (root * inp).astype(bf16)
        c1_o[here, :] = (pushed * (0.5 - 0.5 * ti)).astype(bf16)
        turned_o[:, here] = jnp.transpose(x).astype(bf16)
        return 0

    lax.fori_loop(0, 8, gates, 0)

    local_s[0:8, :] = jnp.zeros((8, SPAN), f32)
    power_s[0:8, :] = jnp.ones((8, SPAN), f32)

    def scan(n, held):
        value, power = held
        for m in range(8):
            at = pl.ds(pl.multiple_of(n * 64 + 8 * m, 8), 8)
            a = decay_s[at, :]
            value = fed_s[at, :] + a * value
            power = a * power
            to = pl.ds(pl.multiple_of(n * 64 + 8 * m + 8, 8), 8)
            local_s[to, :] = value
            power_s[to, :] = power
        return value, power

    value, power = lax.fori_loop(0, 16, scan, (jnp.zeros((8, SPAN), f32), jnp.ones((8, SPAN), f32)))
    enters = jnp.broadcast_to(entering(power, value, False)[None], (16, 8, SPAN)).reshape(SPAN, SPAN)

    def slopes(n, _):
        here = block_of(n)
        previous = local_s[here, :] + power_s[here, :] * enters
        decay = decay_s[here, :]
        slope = previous * decay - slope_s[here, :]
        c2_o[here, :] = (slope * rate_s[here, :]).astype(bf16)
        c3_o[here, :] = (slope * recur_s[here, :]).astype(bf16)
        fed_s[here, :] = local_s[moved_block(n, 8), :] + power_s[moved_block(n, 8), :] * enters
        return 0

    lax.fori_loop(0, 8, slopes, 0)
    next_o[0:1016, :] = decay_s[8:1024, :]
    next_o[1016:1024, :] = after_of(decay_s[0:8, :])
    for p in range(8):
        state = jnp.transpose(strided(fed_s, p))
        for half, at in ((0, slice(p * SPAN, (p + 1) * SPAN)), (1, slice((8 + p) * SPAN, (9 + p) * SPAN))):
            g = gate[:, at].astype(f32)
            c = 0.7978845608028654
            inner = jnp.tanh(c * (g + 0.044715 * (g * g * g)))
            part = 0.5 + 0.5 * inner
            turn = part + 0.5 * g * (1.0 - inner * inner) * (c * (1.0 + 3 * 0.044715 * (g * g)))
            g0_o[:, at] = (g * part).astype(bf16)
            g1_o[:, at] = (state[GROUP * half : GROUP * half + GROUP] * turn).astype(bf16)


def backward_kernel(
    cot, next_r, c0_r, c1_r, c2_r, c3_r, branch_r, turned_r, g0_r, g1_r, back_r, rows,
    gb_o, gate_o, small_o, d_s, local_s, power_s, dx_s, pushed_s,
):
    for p in range(8):
        parts = []
        for j in (p, 8 + p):
            at = slice(j * SPAN, (j + 1) * SPAN)
            c = cot[j].astype(f32)
            gate_o[:, at] = (c * g1_r[:, at].astype(f32)).astype(bf16)
            parts.append(c * g0_r[:, at].astype(f32))
        d_s[pl.ds(p, SPAN, stride=8), :] = jnp.transpose(halves(*parts))

    def scan(n, held):
        value, power = held
        for m in range(8):
            at = pl.ds(pl.multiple_of(1016 - n * 64 - 8 * m, 8), 8)
            a = next_r[at, :]
            value = d_s[at, :] + a * value
            power = a * power
            local_s[at, :] = value
            power_s[at, :] = power
        return value, power

    value, power = lax.fori_loop(0, 16, scan, (jnp.zeros((8, SPAN), f32), jnp.ones((8, SPAN), f32)))
    enters = jnp.broadcast_to(entering(power, value, True)[None], (16, 8, SPAN)).reshape(SPAN, SPAN)

    def summed(block):
        return jnp.sum(block.reshape(16, 8, SPAN), axis=0)

    def spread(n, total):
        here = block_of(n)
        grad = local_s[here, :] + power_s[here, :] * enters
        high = jnp.concatenate(
            [(grad * c2_r[here, :].astype(f32)).astype(bf16), (grad * c1_r[here, :].astype(f32)).astype(bf16)], axis=1
        )
        pushed_s[here, :] = high
        back = jnp.dot(high, back_r[0], preferred_element_type=f32) + jnp.dot(
            high, back_r[1], preferred_element_type=f32
        )
        dx_s[here, :] = grad * c0_r[here, :].astype(f32) + back
        return total + summed(grad * c3_r[here, :].astype(f32))

    zero = jnp.zeros((8, SPAN), f32)
    decays = lax.fori_loop(0, 8, spread, zero)
    for m in range(3):
        dx_s[1024 + 8 * m : 1032 + 8 * m, :] = after_of(dx_s[8 * m : 8 * m + 8, :])

    def taps(n, totals):
        here = block_of(n)
        value = branch_r[here, :].astype(f32)
        gb, out = None, []
        for k in range(CONV):
            dx = dx_s[moved_block(n, 8 * (3 - k)), :]
            term = tiled(rows[k : k + 1, :]) * dx
            gb = term if gb is None else gb + term
            out.append(totals[k] + summed(value * dx))
        d_s[here, :] = gb
        return tuple(out)

    totals = lax.fori_loop(0, 8, taps, (zero,) * CONV)
    for p in range(8):
        gb = jnp.transpose(strided(d_s, p)).astype(bf16)
        gb_o[p] = gb[:GROUP]
        gb_o[8 + p] = gb[GROUP:]
    product = jnp.dot(turned_r[...], pushed_s[...], preferred_element_type=f32)
    low = lanes((GROUP, SPAN)) < GROUP
    r_part = product[:GROUP, :SPAN] + pltpu.roll(product[GROUP:, :SPAN], GROUP, 1)
    i_part = pltpu.roll(product[:GROUP, SPAN:], GROUP, 1) + product[GROUP:, SPAN:]
    small_o[0:GROUP, :] = jnp.where(low, r_part, i_part).astype(bf16)
    row = lax.broadcasted_iota(jnp.int32, (8, SPAN), 0)
    table = zero
    for k, total in enumerate((*totals, decays * jnp.broadcast_to(rows[5:6, :], (8, SPAN)))):
        flat = jnp.broadcast_to(jnp.sum(total, axis=0, keepdims=True), (8, SPAN))
        table = jnp.where(row == k, flat + pltpu.roll(flat, GROUP, 1), table)
    small_o[GROUP : GROUP + 8, :] = table.astype(bf16)


VMEM = pl.BlockSpec(memory_space=pltpu.VMEM)
FLAT = (1024, SPAN)


def forward_part(branch, gate, shift, conv, decay_param, recur_map, input_map):
    flat = jax.ShapeDtypeStruct(FLAT, bf16)
    plain = jax.ShapeDtypeStruct(branch.shape, bf16)
    return pl.pallas_call(
        forward_kernel,
        out_shape=[
            jax.ShapeDtypeStruct(FLAT, f32),
            *[flat] * 5,
            jax.ShapeDtypeStruct((SPAN, 1024), bf16),
            plain,
            plain,
            jax.ShapeDtypeStruct((2, 2 * SPAN, SPAN), bf16),
            jax.ShapeDtypeStruct((8, SPAN), f32),
        ],
        scratch_shapes=[pltpu.VMEM((1048, SPAN), f32)] + [pltpu.VMEM(FLAT, f32)] * 5 + [pltpu.VMEM((1032, SPAN), f32)] * 2,
        name="forward_part",
    )(branch, gate, shift, conv, decay_param, recur_map, input_map)


def backward_part(cot, saved):
    return pl.pallas_call(
        backward_kernel,
        out_shape=[
            jax.ShapeDtypeStruct((16, GROUP, SPAN), bf16),
            jax.ShapeDtypeStruct((GROUP, 2048), bf16),
            jax.ShapeDtypeStruct((GROUP + 8, 2 * GROUP), bf16),
        ],
        scratch_shapes=[pltpu.VMEM(FLAT, f32)] * 3 + [pltpu.VMEM((1048, SPAN), f32), pltpu.VMEM((1024, 2 * SPAN), bf16)],
        name="backward_part",
    )(cot, *saved)


def product_kernel(place, small, own, near, far, grads, out):
    total = None
    blocks = (own[...], near[...], far[0], far[1])
    for n, block in enumerate(blocks):
        theirs = grads[:, place[0] ^ NEAREST[n]].reshape(256, SPAN)
        term = lax.dot_general(block, theirs, (((1,), (1,)), ((), ())), preferred_element_type=f32)
        total = term if total is None else total + term
    pieces = out.shape[0]
    out[:, 0:32, :] = total.astype(bf16).reshape(pieces, 32, 256)
    top = jnp.concatenate([small[0:32, :], small[32:64, :]], axis=1)
    low = jnp.concatenate([small[64:72, :], jnp.zeros((8, SPAN), bf16)], axis=1)
    out[:, 32:72, :] = jnp.broadcast_to(jnp.concatenate([top, low], axis=0)[None], (pieces, 40, 256))


def gather_sum_kernel(arrived, packed_o, maps_o, rest_o):
    block = lax.broadcasted_iota(jnp.int32, (16, SPAN), 1) // 16
    totals, extra = [], None
    for n in range(4):
        total = arrived[8 * n, 0:32, :].astype(f32)
        for m in range(1, 8):
            total = total + arrived[8 * n + m, 0:32, :].astype(f32)
        totals.append(total)
    for n in range(32):
        term = arrived[n, 32:72, :].astype(f32)
        extra = term if extra is None else extra + term
    maps_o[0:32, :] = extra[0:32, 0:SPAN]
    maps_o[32:64, :] = extra[0:32, SPAN:]
    rest_o[...] = extra[32:40, 0:SPAN]
    for group in range(16):
        tile = slice((group // 8) * SPAN, (group // 8 + 1) * SPAN)
        piece = None
        for j in range(8):
            source = totals[j % 4][16 * (j // 4) : 16 * (j // 4) + 16, tile]
            shift = (16 * (j - group % 8)) % SPAN
            turned = pltpu.roll(source, shift, 1) if shift else source
            piece = turned if piece is None else jnp.where(block == j, turned, piece)
        packed_o[group] = piece.astype(bf16)


def last_sum_kernel(arrived, out):
    total = arrived[0].astype(f32)
    for n in range(1, arrived.shape[0]):
        total = total + arrived[n].astype(f32)
    out[0:16, :] = total[:, 0:GROUP]
    out[16:32, :] = pltpu.roll(total, GROUP, 1)[:, 0:GROUP]


def token_grad_kernel(place, proj, proj_other, own, one, two, three, out, tokens_s):
    for n, piece in enumerate((own, one, two, three)):
        tokens_s[:, (place[0] + 4 - n) % 4] = piece[...]
    tokens = tokens_s[...].reshape(1024, SPAN)
    for k, half in enumerate((proj, proj_other)):
        result = jnp.dot(half[...], tokens, preferred_element_type=f32).astype(bf16)
        for n in range(16):
            y, x = place[0] ^ NEAREST[n % 4], place[1] ^ NEAREST[n // 4]
            row = ((y * 4 + x) * 2 + (place[2] ^ k)) * 32
            out[pl.ds(pl.multiple_of(row, 32), 32), :] = result[32 * n : 32 * n + 32]


def exchanged(array, axis, bit):
    size = lax.axis_size(axis)
    return lax.ppermute(array, axis, [(n, n ^ bit) for n in range(size)])


def joined(array, axis, bits):
    return jnp.concatenate([array, exchanged(array, axis, bits)], axis=0)


def gathered_rows(rows):
    held = joined(joined(rows, "y", 1), "y", 3)
    held = joined(joined(held, "x", 1), "x", 3)
    return held, exchanged(held, "core", 1)


def steps(
    normed, branch_in, gate_pre, cotangent, decay_shift,
    conv_weight, recur_weight, input_weight, decay_param, branch_proj,
):
    spans = lax.axis_size("sp")
    cot = lax.all_to_all(cotangent[0].reshape(spans, GROUP, SPAN), "sp", 0, 0, tiled=True)
    saved = forward_part(
        branch_in[0], gate_pre[0], decay_shift[0], conv_weight, decay_param[None], recur_weight[0], input_weight[0]
    )
    own = normed[0]
    near = exchanged(own, "y", 1)
    far = exchanged(jnp.stack([own, near]), "y", 3)
    gb, grad_gate, small = backward_part(cot, saved)
    grads = lax.all_to_all(gb.reshape(64, 16, SPAN), ("sp", "y"), 0, 0, tiled=True)
    grads = grads.reshape(16, 4, 16, SPAN)
    here = lax.axis_index("y")
    place = jnp.stack([lax.axis_index(axis) for axis in DP]).astype(jnp.int32)
    smem = pl.BlockSpec(memory_space=pltpu.SMEM)
    pieces = pl.pallas_call(
        product_kernel,
        in_specs=[smem] + [VMEM] * 5,
        out_specs=VMEM,
        out_shape=jax.ShapeDtypeStruct((32, 72, 256), bf16),
        name="product",
    )(place, small, own, near, far, grads)
    arrived = lax.all_to_all(pieces, DP, 0, 0, tiled=True)
    own_part = [lax.dynamic_index_in_dim(grads, (here + step) % 4, 1, keepdims=False) for step in range(4)]
    for step in (1, 2, 3):
        own_part[step] = lax.ppermute(own_part[step], "y", [(n, (n + step) % 4) for n in range(4)])
    packed, map_sums, rest = pl.pallas_call(
        gather_sum_kernel,
        out_shape=[
            jax.ShapeDtypeStruct((16, 16, SPAN), bf16),
            jax.ShapeDtypeStruct((GROUP, SPAN), f32),
            jax.ShapeDtypeStruct((8, SPAN), f32),
        ],
        name="gather_sum",
    )(arrived)
    last = lax.all_to_all(packed, "sp", 0, 0, tiled=True)
    grad_proj = pl.pallas_call(
        last_sum_kernel, out_shape=jax.ShapeDtypeStruct((32, GROUP), f32), name="last_sum"
    )(last)
    proj, proj_other = gathered_rows(branch_proj)
    grad_normed = pl.pallas_call(
        token_grad_kernel,
        in_specs=[smem] + [VMEM] * 6,
        out_specs=VMEM,
        out_shape=jax.ShapeDtypeStruct((1024, SPAN), bf16),
        scratch_shapes=[pltpu.VMEM((16, 4, 16, SPAN), bf16)],
        name="token_grad",
    )(place, proj, proj_other, *own_part)
    return (
        grad_normed[None],
        grad_gate[None],
        grad_proj,
        rest[0:CONV, 0:GROUP],
        map_sums[None, :, 0:GROUP],
        map_sums[None, :, GROUP:],
        rest[CONV, 0:GROUP],
    )


def solution(mesh):
    split = Mesh(mesh.devices.reshape(16, 4, 4, 2), ("sp", *DP))
    return jax.shard_map(
        steps,
        mesh=split,
        in_specs=(
            P(DP, None, "sp"),
            P(DP, "sp", None),
            P(DP, "sp", None),
            P(DP, None, "sp"),
            P(DP, "sp", None),
            P(None, "sp"),
            P("sp", None, None),
            P("sp", None, None),
            P("sp"),
            P(DP, None),
        ),
        out_specs=(
            P(DP, None, "sp"),
            P(DP, "sp", None),
            P(DP, "sp"),
            P(None, "sp"),
            P("sp", None, None),
            P("sp", None, None),
            P("sp"),
        ),
        check_vma=False,
    )
```

time: 553 us -> 140 us (0.25)
  the two profiles are of different devices: /device:TPU:32 before, /device:TPU:4 now
where the time goes in v1:
time: 140 us; the launch traced here: 139 us
  starting transfers between devices  80 us (57%)
  waiting for transfers between devices  27.1 us (19%)
  Pallas kernels  21.2 us (15%)
  local copies, waits for them, and re-layouts  8.43 us (6%)
  other arithmetic  1.55 us (1%)
    ppermute x7, starting transfers between devices, exchanged(): return lax.ppermute(array, axis, [(n, n ^ bit) for n in range(size)])  22.7 us
    all_to_all x1, starting transfers between devices, steps(): lax.all_to_all(cotangent[0].reshape(spans, GROUP, SPAN), 'sp', 0, 0, tile...  15.2 us
    all_to_all x1, starting transfers between devices, steps(): lax.all_to_all(gb.reshape(64, 16, SPAN), ('sp', 'y'), 0, 0, tiled=True)  14.4 us
    ppermute x7, waiting for transfers between devices, exchanged(): return lax.ppermute(array, axis, [(n, n ^ bit) for n in range(size)])  11.3 us
    ppermute x3, starting transfers between devices, steps(): lax.ppermute(own_part[step], 'y', [(n, (n + step) % 4) for n in range(4)])  11.3 us
    all_to_all x1, starting transfers between devices, steps(): last = lax.all_to_all(packed, 'sp', 0, 0, tiled=True)  10.1 us
    all_to_all x1, waiting for transfers between devices, steps(): last = lax.all_to_all(packed, 'sp', 0, 0, tiled=True)  9.1 us
    all_to_all x1, starting transfers between devices, steps(): arrived = lax.all_to_all(pieces, DP, 0, 0, tiled=True)  6.28 us
  transfers between devices with their start and end apart: 14, of which 7 were waited for; matrix products, arithmetic and copies ran while one was open for 5% of the time, Pallas kernels for 13%

profile of v1, /device:TPU:4, one launch (start us, length us, event | category | flops | bytes accessed | tf_op | source)
XLA Modules:
  0.0 139.2 jit_solution(4342846333245365731)
XLA Ops:
  0.6 15.2 %all-to-all-start = ((bf16[16,64,128]{2,1,0:T(8,128)(2,1)}), bf16[16,64,128]{2,1,0:T(8,128)(2,1)S(1)}, u32[]{:S(2)}, u32[]{:S(2)}) async-start(bf16[16,64,128]{2,1,0:T(8,128)(2,1)} %bitcast.37), calls=%async_computation | async-start | bytes 524288 | tf_op jit(solution)/shard_map/all_to_all | solution.py:390
  15.8 3.5 %collective-permute-start = (bf16[32,1024]{1,0:T(8,128)(2,1)}, bf16[32,1024]{1,0:T(8,128)(2,1)S(1)}, u32[]{:S(2)}, u32[]{:S(2)}) collective-permute-start(bf16[32,1024]{1,0:T(8,128)(2,1)} %param.19), channel_id=1, source_target_pairs={{0,8},{8,0},{16,24},{24,16},{1,9},{9,1},{17,25},{25,17},{2,10},{10... | collective-permute-start | bytes 196616 | tf_op jit(solution)/shard_map/ppermute | solution.py:372
  19.3 2.9 %collective-permute-done = bf16[32,1024]{1,0:T(8,128)(2,1)S(1)} collective-permute-done((bf16[32,1024]{1,0:T(8,128)(2,1)}, bf16[32,1024]{1,0:T(8,128)(2,1)S(1)}, u32[]{:S(2)}, u32[]{:S(2)}) %collective-permute-start) | collective-permute-done | bytes 65568 | tf_op jit(solution)/shard_map/ppermute | solution.py:372
  22.2 0.8 pad_maximum_fusion.3
  23.1 4.9 %collective-permute-start.1 = (bf16[64,1024]{1,0:T(8,128)(2,1)S(1)}, bf16[64,1024]{1,0:T(8,128)(2,1)S(1)}, u32[]{:S(2)}, u32[]{:S(2)}) collective-permute-start(bf16[64,1024]{1,0:T(8,128)(2,1)S(1)} %pad_maximum_fusion.3), channel_id=1, source_target_pairs={{0,24},{8,16},{16,8},{24,0},{1,25},{9,17},{17,9},{25,1},{2,26},{10... | collective-permute-start | bytes 393224 | tf_op jit(solution)/shard_map/ppermute | solution.py:372
  28.0 2.0 %collective-permute-start.8 = (bf16[1024,128]{1,0:T(8,128)(2,1)}, bf16[1024,128]{1,0:T(8,128)(2,1)S(1)}, u32[]{:S(2)}, u32[]{:S(2)}) collective-permute-start(bf16[1024,128]{1,0:T(8,128)(2,1)} %bitcast.32), channel_id=1, source_target_pairs={{0,8},{8,0},{16,24},{24,16},{1,9},{9,1},{17,25},{25,17},{2,10},{10... | collective-permute-start | bytes 786440 | tf_op jit(solution)/shard_map/ppermute | solution.py:372
  30.1 6.2 %forward_part.1 = (f32[1024,128]{1,0:T(8,128)}, bf16[1024,128]{1,0:T(8,128)(2,1)}, bf16[1024,128]{1,0:T(8,128)(2,1)}, bf16[1024,128]{1,0:T(8,128)(2,1)}, bf16[10...) custom-call(bf16[64,2048]{1,0:T(8,128)(2,1)} %bitcast.35, ...), custom_call_target="tpu_custom_call" | custom-call | tf_op jit(solution)/shard_map/forward_part/pallas_call | solution.py:282
  36.9 5.3 %backward_part.1 = (bf16[16,64,128]{2,1,0:T(8,128)(2,1)}, bf16[64,2048]{1,0:T(8,128)(2,1)}, bf16[72,128]{1,0:T(8,128)(2,1)}) custom-call(bf16[16,64,128]{2,1,0:T(8,128)(2,1)} %copy-done.4, f32[1024,128]{1,0:T(8,128)} %get-tuple-element.24.next_r, bf16[1024,128]{1,0:T(8,128)(2,1)} %get-tuple-element.25.c0_r, bf16[1024,128]{1,0:T(8,128)(2,1)} %get-tuple-element.26.c1_r, ...), custom_call_target="tpu_custom_call" | custom-call | tf_op jit(solution)/shard_map/backward_part/pallas_call | solution.py:299
  42.2 14.4 %all-to-all-start.1 = ((bf16[64,16,128]{2,1,0:T(8,128)(2,1)}), bf16[64,16,128]{2,1,0:T(8,128)(2,1)S(1)}, u32[]{:S(2)}, u32[]{:S(2)}) async-start(bf16[64,16,128]{2,1,0:T(8,128)(2,1)} %bitcast.38), calls=%async_computation.1 | async-start | bytes 524288 | tf_op jit(solution)/shard_map/all_to_all | solution.py:398
  56.6 3.1 %collective-permute-start.2 = (bf16[128,1024]{1,0:T(8,128)(2,1)S(1)}, bf16[128,1024]{1,0:T(8,128)(2,1)S(1)}, u32[]{:S(2)}, u32[]{:S(2)}) collective-permute-start(bf16[128,1024]{1,0:T(8,128)(2,1)S(1)} %pad_maximum_fusion.2), channel_id=1, source_target_pairs={{0,2},{2,0},{4,6},{6,4},{1,3},{3,1},{5,7},{7,5},{8,10},{10,8},{12,... | collective-permute-start | bytes 786440 | tf_op jit(solution)/shard_map/ppermute | solution.py:372
  59.8 4.7 %collective-permute-start.9 = (bf16[2,1024,128]{2,1,0:T(8,128)(2,1)S(1)}, bf16[2,1024,128]{2,1,0:T(8,128)(2,1)}, u32[]{:S(2)}, u32[]{:S(2)}) collective-permute-start(bf16[2,1024,128]{2,1,0:T(8,128)(2,1)S(1)} %pad_maximum_fusion.1), channel_id=1, source_target_pairs={{0,24},{8,16},{16,8},{24,0},{1,25},{9,17},{17,9},{25,1},{2,26},{10... | collective-permute-start | bytes 1572872 | tf_op jit(solution)/shard_map/ppermute | solution.py:372
  64.9 2.4 %collective-permute-start.3 = (bf16[256,1024]{1,0:T(8,128)(2,1)S(1)}, bf16[256,1024]{1,0:T(8,128)(2,1)S(1)}, u32[]{:S(2)}, u32[]{:S(2)}) collective-permute-start(bf16[256,1024]{1,0:T(8,128)(2,1)S(1)} %pad_maximum_fusion), channel_id=1, source_target_pairs={{0,6},{2,4},{4,2},{6,0},{1,7},{3,5},{5,3},{7,1},{8,14},{10,12},{12... | collective-permute-start | bytes 1572872 | tf_op jit(solution)/shard_map/ppermute | solution.py:372
  68.1 8.1 %collective-permute-done.9.far = bf16[2,1024,128]{2,1,0:T(8,128)(2,1)} collective-permute-done((bf16[2,1024,128]{2,1,0:T(8,128)(2,1)S(1)}, bf16[2,1024,128]{2,1,0:T(8,128)(2,1)}, u32[]{:S(2)}, u32[]{:S(2)}) %collective-permute-start.9) | collective-permute-done | bytes 524320 | tf_op jit(solution)/shard_map/ppermute | solution.py:372
  76.2 1.3 all-to-all-done.1
  77.5 0.7 copy-done.1
  78.2 3.0 %product.1 = bf16[32,72,256]{2,1,0:T(8,128)(2,1)} custom-call(s32[3]{0:T(128)} %pad_add_fusion.place, bf16[72,128]{1,0:T(8,128)(2,1)} %get-tuple-element.37.small, bf16[1024,128]{1,0:T(8,128)(2,1)} %bitcast.33, bf16[1024,128]{1,0:T(8,128)(2,1)} %copy-done.7, bf16[2,1024,128]{2,1,0:T(8,128)(2,1)} %collective-permute-done.9.far, bf16[16,4,16,128]{3,2,1,0:T(8,128)(2,1)} %bitcast.30), custom_call_target="tpu_custom_call" | custom-call | tf_op jit(solution)/shard_map/product/pallas_call | solution.py:403
  81.2 6.3 %all-to-all-start.2 = ((bf16[32,72,256]{2,1,0:T(8,128)(2,1)}), bf16[32,72,256]{2,1,0:T(8,128)(2,1)S(1)}, u32[]{:S(2)}, u32[]{:S(2)}) async-start(bf16[32,72,256]{2,1,0:T(8,128)(2,1)} %product.1), calls=%async_computation.2 | async-start | bytes 2359296 | tf_op jit(solution)/shard_map/all_to_all | solution.py:410
  87.6 2.0 %collective-permute-start.4 = (bf16[512,1024]{1,0:T(8,128)(2,1)S(1)}, bf16[512,1024]{1,0:T(8,128)(2,1)S(1)}, u32[]{:S(2)}, u32[]{:S(2)}) collective-permute-start(bf16[512,1024]{1,0:T(8,128)(2,1)S(1)} %constant_dynamic-update-slice_fusion.proj), channel_id=1, source_target_pairs={{0,1},{1,0},{2,3},{3,2},{4,5},{5,4},{6,7},{7,6},{8,9},{9,8},{10,11... | collective-permute-start | bytes 3145736 | tf_op jit(solution)/shard_map/ppermute | solution.py:372
  90.3 3.4 %collective-permute-start.5 = (bf16[16,16,128]{2,1,0:T(8,128)(2,1)S(1)}, bf16[16,16,128]{2,1,0:T(8,128)(2,1)S(1)}, u32[]{:S(2)}, u32[]{:S(2)}) collective-permute-start(bf16[16,16,128]{2,1,0:T(8,128)(2,1)S(1)} %get-tuple-element.43), channel_id=1, source_target_pairs={{0,8},{8,16},{16,24},{24,0},{1,9},{9,17},{17,25},{25,1},{2,10},{10... | collective-permute-start | bytes 196616 | tf_op jit(solution)/shard_map/ppermute | solution.py:413
  93.7 4.7 %collective-permute-start.6 = (bf16[16,16,128]{2,1,0:T(8,128)(2,1)S(1)}, bf16[16,16,128]{2,1,0:T(8,128)(2,1)S(1)}, u32[]{:S(2)}, u32[]{:S(2)}) collective-permute-start(bf16[16,16,128]{2,1,0:T(8,128)(2,1)S(1)} %get-tuple-element.42), channel_id=1, source_target_pairs={{0,16},{8,24},{16,0},{24,8},{1,17},{9,25},{17,1},{25,9},{2,18},{10... | collective-permute-start | bytes 196616 | tf_op jit(solution)/shard_map/ppermute | solution.py:413
  98.4 3.3 %collective-permute-start.7 = (bf16[16,16,128]{2,1,0:T(8,128)(2,1)S(1)}, bf16[16,16,128]{2,1,0:T(8,128)(2,1)S(1)}, u32[]{:S(2)}, u32[]{:S(2)}) collective-permute-start(bf16[16,16,128]{2,1,0:T(8,128)(2,1)S(1)} %get-tuple-element.41), channel_id=1, source_target_pairs={{0,24},{8,0},{16,8},{24,16},{1,25},{9,1},{17,9},{25,17},{2,26},{10... | collective-permute-start | bytes 196616 | tf_op jit(solution)/shard_map/ppermute | solution.py:413
  101.7 3.6 %collective-permute-done.5.one = bf16[16,16,128]{2,1,0:T(8,128)(2,1)S(1)} collective-permute-done((bf16[16,16,128]{2,1,0:T(8,128)(2,1)S(1)}, bf16[16,16,128]{2,1,0:T(8,128)(2,1)S(1)}, u32[]{:S(2)}, u32[]{:S(2)}) %collective-permute-start.5) | collective-permute-done | bytes 65568 | tf_op jit(solution)/shard_map/ppermute | solution.py:413
  105.3 1.7 %collective-permute-done.6.two = bf16[16,16,128]{2,1,0:T(8,128)(2,1)S(1)} collective-permute-done((bf16[16,16,128]{2,1,0:T(8,128)(2,1)S(1)}, bf16[16,16,128]{2,1,0:T(8,128)(2,1)S(1)}, u32[]{:S(2)}, u32[]{:S(2)}) %collective-permute-start.6) | collective-permute-done | bytes 65568 | tf_op jit(solution)/shard_map/ppermute | solution.py:413
  107.6 3.0 %token_grad.1 = bf16[1024,128]{1,0:T(8,128)(2,1)} custom-call(s32[3]{0:T(128)} %pad_add_fusion.place, bf16[512,1024]{1,0:T(8,128)(2,1)} %copy-done.3, bf16[512,1024]{1,0:T(8,128)(2,1)} %copy-done.5, bf16[16,16,128]{2,1,0:T(8,128)(2,1)} %get-tuple-element.44.own, bf16[16,16,128]{2,1,0:T(8,128)(2,1)} %copy-done.10, bf16[16,16,128]{2,1,0:T(8,128)(2,1)} %copy-done.11, ...), custom_call_target="tpu_custom_call" | custom-call | tf_op jit(solution)/shard_map/token_grad/pallas_call | solution.py:428
  110.7 1.0 copy-done
  111.7 2.1 %gather_sum.1 = (bf16[16,16,128]{2,1,0:T(8,128)(2,1)}, f32[64,128]{1,0:T(8,128)}, f32[8,128]{1,0:T(8,128)}) custom-call(bf16[32,72,256]{2,1,0:T(8,128)(2,1)} %copy-done), custom_call_target="tpu_custom_call" | custom-call | tf_op jit(solution)/shard_map/gather_sum/pallas_call | solution.py:414
  113.8 10.1 %all-to-all-start.3 = ((bf16[16,16,128]{2,1,0:T(8,128)(2,1)}), bf16[16,16,128]{2,1,0:T(8,128)(2,1)S(1)}, u32[]{:S(2)}, u32[]{:S(2)}) async-start(bf16[16,16,128]{2,1,0:T(8,128)(2,1)} %get-tuple-element.38), calls=%async_computation.3 | async-start | bytes 131072 | tf_op jit(solution)/shard_map/all_to_all | solution.py:423
  123.9 1.2 slice_bitcast_fusion.2
  125.2 1.3 slice.12
  126.4 1.5 %slice_bitcast_fusion = (f32[1,64,64]{2,1,0:T(8,128)}, f32[1,64,64]{2,1,0:T(8,128)}) fusion(f32[64,128]{1,0:T(8,128)} %get-tuple-element.40), kind=kLoop, calls=%fused_computation.8 | loop fusion | bytes 65536 | tf_op jit(solution)/shard_map/broadcast_in_dim | solution.py:442
  127.9 9.1 %all-to-all-done.3.arrived = bf16[16,16,128]{2,1,0:T(8,128)(2,1)S(1)} async-done(((bf16[16,16,128]{2,1,0:T(8,128)(2,1)}), bf16[16,16,128]{2,1,0:T(8,128)(2,1)S(1)}, u32[]{:S(2)}, u32[]{:S(2)}) %all-to-all-start.3) | async-done | bytes 65568 | tf_op jit(solution)/shard_map/all_to_all | solution.py:423
  137.7 1.5 %last_sum.1 = f32[32,64]{1,0:T(8,128)} custom-call(bf16[16,16,128]{2,1,0:T(8,128)(2,1)} %copy-done.9), custom_call_target="tpu_custom_call" | custom-call | tf_op jit(solution)/shard_map/last_sum/pallas_call | solution.py:424
  (42 shorter events, 3.8 us)
Async XLA Ops:
  0.6 35.6 %all-to-all-start = ((bf16[16,64,128]{2,1,0:T(8,128)(2,1)}), bf16[16,64,128]{2,1,0:T(8,128)(2,1)S(1)}, u32[]{:S(2)}, u32[]{:S(2)}) async-start(bf16[16,64,128]{2,1,0:T(8,128)(2,1)} %bitcast.37), calls=%async_computation | async-start | bytes 524288 | tf_op jit(solution)/shard_map/all_to_all | solution.py:390
  15.8 6.4 %collective-permute-start = (bf16[32,1024]{1,0:T(8,128)(2,1)}, bf16[32,1024]{1,0:T(8,128)(2,1)S(1)}, u32[]{:S(2)}, u32[]{:S(2)}) collective-permute-start(bf16[32,1024]{1,0:T(8,128)(2,1)} %param.19), channel_id=1, source_target_pairs={{0,8},{8,0},{16,24},{24,16},{1,9},{9,1},{17,25},{25,17},{2,10},{10... | collective-permute-start | bytes 196616 | tf_op jit(solution)/shard_map/ppermute | solution.py:372
  23.1 33.5 %collective-permute-start.1 = (bf16[64,1024]{1,0:T(8,128)(2,1)S(1)}, bf16[64,1024]{1,0:T(8,128)(2,1)S(1)}, u32[]{:S(2)}, u32[]{:S(2)}) collective-permute-start(bf16[64,1024]{1,0:T(8,128)(2,1)S(1)} %pad_maximum_fusion.3), channel_id=1, source_target_pairs={{0,24},{8,16},{16,8},{24,0},{1,25},{9,17},{17,9},{25,1},{2,26},{10... | collective-permute-start | bytes 393224 | tf_op jit(solution)/shard_map/ppermute | solution.py:372
  28.0 31.8 %collective-permute-start.8 = (bf16[1024,128]{1,0:T(8,128)(2,1)}, bf16[1024,128]{1,0:T(8,128)(2,1)S(1)}, u32[]{:S(2)}, u32[]{:S(2)}) collective-permute-start(bf16[1024,128]{1,0:T(8,128)(2,1)} %bitcast.32), channel_id=1, source_target_pairs={{0,8},{8,0},{16,24},{24,16},{1,9},{9,1},{17,25},{25,17},{2,10},{10... | collective-permute-start | bytes 786440 | tf_op jit(solution)/shard_map/ppermute | solution.py:372
  36.2 0.7 copy-start.4
  36.9 19.7 %copy-start.8 = (bf16[32,1024]{1,0:T(8,128)(2,1)S(1)}, bf16[32,1024]{1,0:T(8,128)(2,1)}, u32[]{:S(2)}) copy-start(bf16[32,1024]{1,0:T(8,128)(2,1)} %param.19) | copy-start | bytes 196612
  42.2 17.6 %copy-start.6 = (bf16[1,1024,128]{2,1,0:T(8,128)(2,1)S(1)}, bf16[1,1024,128]{2,1,0:T(8,128)(2,1)}, u32[]{:S(2)}) copy-start(bf16[1,1024,128]{2,1,0:T(8,128)(2,1)} %param.10) | copy-start | bytes 786436
  42.2 35.3 %all-to-all-start.1 = ((bf16[64,16,128]{2,1,0:T(8,128)(2,1)}), bf16[64,16,128]{2,1,0:T(8,128)(2,1)S(1)}, u32[]{:S(2)}, u32[]{:S(2)}) async-start(bf16[64,16,128]{2,1,0:T(8,128)(2,1)} %bitcast.38), calls=%async_computation.1 | async-start | bytes 524288 | tf_op jit(solution)/shard_map/all_to_all | solution.py:398
  56.6 8.3 %collective-permute-start.2 = (bf16[128,1024]{1,0:T(8,128)(2,1)S(1)}, bf16[128,1024]{1,0:T(8,128)(2,1)S(1)}, u32[]{:S(2)}, u32[]{:S(2)}) collective-permute-start(bf16[128,1024]{1,0:T(8,128)(2,1)S(1)} %pad_maximum_fusion.2), channel_id=1, source_target_pairs={{0,2},{2,0},{4,6},{6,4},{1,3},{3,1},{5,7},{7,5},{8,10},{10,8},{12,... | collective-permute-start | bytes 786440 | tf_op jit(solution)/shard_map/ppermute | solution.py:372
  59.8 8.2 %copy-start.7 = (bf16[1024,128]{1,0:T(8,128)(2,1)}, bf16[1024,128]{1,0:T(8,128)(2,1)S(1)}, u32[]{:S(2)}) copy-start(bf16[1024,128]{1,0:T(8,128)(2,1)S(1)} %collective-permute-done.8.near) | copy-start | bytes 786436
  59.8 16.3 %collective-permute-start.9 = (bf16[2,1024,128]{2,1,0:T(8,128)(2,1)S(1)}, bf16[2,1024,128]{2,1,0:T(8,128)(2,1)}, u32[]{:S(2)}, u32[]{:S(2)}) collective-permute-start(bf16[2,1024,128]{2,1,0:T(8,128)(2,1)S(1)} %pad_maximum_fusion.1), channel_id=1, source_target_pairs={{0,24},{8,16},{16,8},{24,0},{1,25},{9,17},{17,9},{25,1},{2,26},{10... | collective-permute-start | bytes 1572872 | tf_op jit(solution)/shard_map/ppermute | solution.py:372
  64.9 22.6 %collective-permute-start.3 = (bf16[256,1024]{1,0:T(8,128)(2,1)S(1)}, bf16[256,1024]{1,0:T(8,128)(2,1)S(1)}, u32[]{:S(2)}, u32[]{:S(2)}) collective-permute-start(bf16[256,1024]{1,0:T(8,128)(2,1)S(1)} %pad_maximum_fusion), channel_id=1, source_target_pairs={{0,6},{2,4},{4,2},{6,0},{1,7},{3,5},{5,3},{7,1},{8,14},{10,12},{12... | collective-permute-start | bytes 1572872 | tf_op jit(solution)/shard_map/ppermute | solution.py:372
  77.5 0.7 copy-start.1
  81.2 8.4 %copy-start.2 = (bf16[64,16,128]{2,1,0:T(8,128)(2,1)S(1)}, bf16[64,16,128]{2,1,0:T(8,128)(2,1)}, u32[]{:S(2)}) copy-start(bf16[64,16,128]{2,1,0:T(8,128)(2,1)} %copy-done.1) | copy-start | bytes 786436
  81.2 29.5 %all-to-all-start.2 = ((bf16[32,72,256]{2,1,0:T(8,128)(2,1)}), bf16[32,72,256]{2,1,0:T(8,128)(2,1)S(1)}, u32[]{:S(2)}, u32[]{:S(2)}) async-start(bf16[32,72,256]{2,1,0:T(8,128)(2,1)} %product.1), calls=%async_computation.2 | async-start | bytes 2359296 | tf_op jit(solution)/shard_map/all_to_all | solution.py:410
  87.6 19.4 %copy-start.3 = (bf16[512,1024]{1,0:T(8,128)(2,1)}, bf16[512,1024]{1,0:T(8,128)(2,1)S(1)}, u32[]{:S(2)}) copy-start(bf16[512,1024]{1,0:T(8,128)(2,1)S(1)} %constant_dynamic-update-slice_fusion.proj) | copy-start | bytes 3145732
  87.6 14.1 %collective-permute-start.4 = (bf16[512,1024]{1,0:T(8,128)(2,1)S(1)}, bf16[512,1024]{1,0:T(8,128)(2,1)S(1)}, u32[]{:S(2)}, u32[]{:S(2)}) collective-permute-start(bf16[512,1024]{1,0:T(8,128)(2,1)S(1)} %constant_dynamic-update-slice_fusion.proj), channel_id=1, source_target_pairs={{0,1},{1,0},{2,3},{3,2},{4,5},{5,4},{6,7},{7,6},{8,9},{9,8},{10,11... | collective-permute-start | bytes 3145736 | tf_op jit(solution)/shard_map/ppermute | solution.py:372
  90.3 15.0 %collective-permute-start.5 = (bf16[16,16,128]{2,1,0:T(8,128)(2,1)S(1)}, bf16[16,16,128]{2,1,0:T(8,128)(2,1)S(1)}, u32[]{:S(2)}, u32[]{:S(2)}) collective-permute-start(bf16[16,16,128]{2,1,0:T(8,128)(2,1)S(1)} %get-tuple-element.43), channel_id=1, source_target_pairs={{0,8},{8,16},{16,24},{24,0},{1,9},{9,17},{17,25},{25,1},{2,10},{10... | collective-permute-start | bytes 196616 | tf_op jit(solution)/shard_map/ppermute | solution.py:413
  93.7 13.3 %collective-permute-start.6 = (bf16[16,16,128]{2,1,0:T(8,128)(2,1)S(1)}, bf16[16,16,128]{2,1,0:T(8,128)(2,1)S(1)}, u32[]{:S(2)}, u32[]{:S(2)}) collective-permute-start(bf16[16,16,128]{2,1,0:T(8,128)(2,1)S(1)} %get-tuple-element.42), channel_id=1, source_target_pairs={{0,16},{8,24},{16,0},{24,8},{1,17},{9,25},{17,1},{25,9},{2,18},{10... | collective-permute-start | bytes 196616 | tf_op jit(solution)/shard_map/ppermute | solution.py:413
  98.4 8.6 %collective-permute-start.7 = (bf16[16,16,128]{2,1,0:T(8,128)(2,1)S(1)}, bf16[16,16,128]{2,1,0:T(8,128)(2,1)S(1)}, u32[]{:S(2)}, u32[]{:S(2)}) collective-permute-start(bf16[16,16,128]{2,1,0:T(8,128)(2,1)S(1)} %get-tuple-element.41), channel_id=1, source_target_pairs={{0,24},{8,0},{16,8},{24,16},{1,25},{9,1},{17,9},{25,17},{2,26},{10... | collective-permute-start | bytes 196616 | tf_op jit(solution)/shard_map/ppermute | solution.py:413
  101.7 5.3 %copy-start.5 = (bf16[512,1024]{1,0:T(8,128)(2,1)}, bf16[512,1024]{1,0:T(8,128)(2,1)S(1)}, u32[]{:S(2)}) copy-start(bf16[512,1024]{1,0:T(8,128)(2,1)S(1)} %collective-permute-done.4.proj_other) | copy-start | bytes 3145732
  105.3 1.7 %copy-start.10 = (bf16[16,16,128]{2,1,0:T(8,128)(2,1)}, bf16[16,16,128]{2,1,0:T(8,128)(2,1)S(1)}, u32[]{:S(2)}) copy-start(bf16[16,16,128]{2,1,0:T(8,128)(2,1)S(1)} %collective-permute-done.5.one) | copy-start | bytes 196612
  107.0 0.6 copy-start.11
  107.0 0.6 copy-start.12
  110.7 1.0 copy-start
  113.8 23.2 %all-to-all-start.3 = ((bf16[16,16,128]{2,1,0:T(8,128)(2,1)}), bf16[16,16,128]{2,1,0:T(8,128)(2,1)S(1)}, u32[]{:S(2)}, u32[]{:S(2)}) async-start(bf16[16,16,128]{2,1,0:T(8,128)(2,1)} %get-tuple-element.38), calls=%async_computation.3 | async-start | bytes 131072 | tf_op jit(solution)/shard_map/all_to_all | solution.py:423
  137.0 0.6 copy-start.9

commit v2 on v1

--- a/solution.py
+++ b/solution.py
@@ -276,6 +276,10 @@
 FLAT = (1024, SPAN)
 
 
+def here_in_vmem(array):
+    return pltpu.with_memory_space_constraint(array, pltpu.VMEM)
+
+
 def forward_part(branch, gate, shift, conv, decay_param, recur_map, input_map):
     flat = jax.ShapeDtypeStruct(FLAT, bf16)
     plain = jax.ShapeDtypeStruct(branch.shape, bf16)
@@ -308,34 +312,43 @@
     )(cot, *saved)
 
 
-def product_kernel(place, small, own, near, far, grads, out):
+def product_kernel(place, small, partner, own, near, far, grads, out):
     total = None
-    blocks = (own[...], near[...], far[0], far[1])
+    blocks = (own[...], near[0:1024, :], far[0, 0:1024, :], far[1, 0:1024, :])
     for n, block in enumerate(blocks):
         theirs = grads[:, place[0] ^ NEAREST[n]].reshape(256, SPAN)
         term = lax.dot_general(block, theirs, (((1,), (1,)), ((), ())), preferred_element_type=f32)
         total = term if total is None else total + term
     pieces = out.shape[0]
     out[:, 0:32, :] = total.astype(bf16).reshape(pieces, 32, 256)
-    top = jnp.concatenate([small[0:32, :], small[32:64, :]], axis=1)
-    low = jnp.concatenate([small[64:72, :], jnp.zeros((8, SPAN), bf16)], axis=1)
-    out[:, 32:72, :] = jnp.broadcast_to(jnp.concatenate([top, low], axis=0)[None], (pieces, 40, 256))
-
-
-def gather_sum_kernel(arrived, packed_o, maps_o, rest_o):
+    mine = pl.ds(pl.multiple_of(place[2] * 32, 32), 32)
+    maps = (small[mine, :].astype(f32) + partner[mine, :].astype(f32)).astype(bf16)
+    rest = (small[64:72, :].astype(f32) + partner[64:72, :].astype(f32)).astype(bf16)
+    top = jnp.concatenate([maps[0:16], maps[16:32]], axis=1)
+    low = jnp.concatenate([rest, jnp.zeros((8, SPAN), bf16)], axis=1)
+    out[:, 32:56, :] = jnp.broadcast_to(jnp.concatenate([top, low], axis=0)[None], (pieces, 24, 256))
+
+
+def gather_sum_kernel(arrived, packed_o, conv_o, recur_o, input_o, decay_o):
     block = lax.broadcasted_iota(jnp.int32, (16, SPAN), 1) // 16
-    totals, extra = [], None
+    totals = []
     for n in range(4):
         total = arrived[8 * n, 0:32, :].astype(f32)
         for m in range(1, 8):
             total = total + arrived[8 * n + m, 0:32, :].astype(f32)
         totals.append(total)
-    for n in range(32):
-        term = arrived[n, 32:72, :].astype(f32)
-        extra = term if extra is None else extra + term
-    maps_o[0:32, :] = extra[0:32, 0:SPAN]
-    maps_o[32:64, :] = extra[0:32, SPAN:]
-    rest_o[...] = extra[32:40, 0:SPAN]
+    for core in range(2):
+        extra = arrived[core, 32:56, :].astype(f32)
+        for n in range(core + 2, 32, 2):
+            extra = extra + arrived[n, 32:56, :].astype(f32)
+        for n in range(2):
+            at = slice(32 * core + 16 * n, 32 * core + 16 * n + 16)
+            half = extra[0:16, n * SPAN : (n + 1) * SPAN]
+            recur_o[at, :] = half[:, 0:GROUP]
+            input_o[at, :] = pltpu.roll(half, GROUP, 1)[:, 0:GROUP]
+        if core == 0:
+            conv_o[...] = extra[16:20, 0:GROUP]
+            decay_o[...] = extra[20:21, 0:GROUP]
     for group in range(16):
         tile = slice((group // 8) * SPAN, (group // 8 + 1) * SPAN)
         piece = None
@@ -357,10 +370,17 @@
 
 def token_grad_kernel(place, proj, proj_other, own, one, two, three, out, tokens_s):
     for n, piece in enumerate((own, one, two, three)):
-        tokens_s[:, (place[0] + 4 - n) % 4] = piece[...]
+        tokens_s[:, place[0] ^ n] = piece[...]
     tokens = tokens_s[...].reshape(1024, SPAN)
     for k, half in enumerate((proj, proj_other)):
-        result = jnp.dot(half[...], tokens, preferred_element_type=f32).astype(bf16)
+        tiles = half[...].reshape(16, 4, 8, 8, SPAN)
+        result = None
+        for n in range(8):
+            term = jnp.dot(
+                tiles[:, :, n].reshape(512, SPAN), tokens[n * SPAN : (n + 1) * SPAN], preferred_element_type=f32
+            )
+            result = term if result is None else result + term
+        result = result.astype(bf16)
         for n in range(16):
             y, x = place[0] ^ NEAREST[n % 4], place[1] ^ NEAREST[n // 4]
             row = ((y * 4 + x) * 2 + (place[2] ^ k)) * 32
@@ -374,12 +394,6 @@
 
 def joined(array, axis, bits):
     return jnp.concatenate([array, exchanged(array, axis, bits)], axis=0)
-
-
-def gathered_rows(rows):
-    held = joined(joined(rows, "y", 1), "y", 3)
-    held = joined(joined(held, "x", 1), "x", 3)
-    return held, exchanged(held, "core", 1)
 
 
 def steps(
@@ -392,9 +406,16 @@
         branch_in[0], gate_pre[0], decay_shift[0], conv_weight, decay_param[None], recur_weight[0], input_weight[0]
     )
     own = normed[0]
-    near = exchanged(own, "y", 1)
-    far = exchanged(jnp.stack([own, near]), "y", 3)
-    gb, grad_gate, small = backward_part(cot, saved)
+    width = branch_proj.shape[1] // SPAN
+    rows = branch_proj.reshape(4, 8, width, SPAN).transpose(0, 2, 1, 3).reshape(-1, SPAN)
+    packed = jnp.concatenate([own, rows], axis=0)
+    near = exchanged(packed, "y", 1)
+    far = exchanged(jnp.stack([packed, near]), "y", 3)
+    held = jnp.stack([rows, near[1024:], far[0, 1024:], far[1, 1024:]])
+    proj = joined(joined(held, "x", 1), "x", 3)
+    proj_other = exchanged(proj, "core", 1)
+    gb, grad_gate, small = backward_part(here_in_vmem(cot), [*map(here_in_vmem, saved[:5]), *saved[5:]])
+    partner = exchanged(small, "core", 1)
     grads = lax.all_to_all(gb.reshape(64, 16, SPAN), ("sp", "y"), 0, 0, tiled=True)
     grads = grads.reshape(16, 4, 16, SPAN)
     here = lax.axis_index("y")
@@ -402,29 +423,33 @@
     smem = pl.BlockSpec(memory_space=pltpu.SMEM)
     pieces = pl.pallas_call(
         product_kernel,
-        in_specs=[smem] + [VMEM] * 5,
+        in_specs=[smem] + [VMEM] * 6,
         out_specs=VMEM,
-        out_shape=jax.ShapeDtypeStruct((32, 72, 256), bf16),
+        out_shape=jax.ShapeDtypeStruct((32, 56, 256), bf16),
         name="product",
-    )(place, small, own, near, far, grads)
+    )(place, small, here_in_vmem(partner), own, near, here_in_vmem(far), here_in_vmem(grads))
     arrived = lax.all_to_all(pieces, DP, 0, 0, tiled=True)
-    own_part = [lax.dynamic_index_in_dim(grads, (here + step) % 4, 1, keepdims=False) for step in range(4)]
-    for step in (1, 2, 3):
-        own_part[step] = lax.ppermute(own_part[step], "y", [(n, (n + step) % 4) for n in range(4)])
-    packed, map_sums, rest = pl.pallas_call(
+
+    def part_for(n):
+        return lax.dynamic_index_in_dim(grads, here ^ n, 1, keepdims=False)
+
+    own_part = part_for(0)
+    others = [exchanged(part_for(n), "y", n) for n in (1, 2, 3)]
+    sums, grad_conv, grad_recur, grad_input, grad_decay = pl.pallas_call(
         gather_sum_kernel,
         out_shape=[
             jax.ShapeDtypeStruct((16, 16, SPAN), bf16),
-            jax.ShapeDtypeStruct((GROUP, SPAN), f32),
-            jax.ShapeDtypeStruct((8, SPAN), f32),
+            jax.ShapeDtypeStruct((CONV, GROUP), f32),
+            jax.ShapeDtypeStruct((GROUP, GROUP), f32),
+            jax.ShapeDtypeStruct((GROUP, GROUP), f32),
+            jax.ShapeDtypeStruct((1, GROUP), f32),
         ],
         name="gather_sum",
-    )(arrived)
-    last = lax.all_to_all(packed, "sp", 0, 0, tiled=True)
+    )(here_in_vmem(arrived))
+    last = lax.all_to_all(sums, "sp", 0, 0, tiled=True)
     grad_proj = pl.pallas_call(
         last_sum_kernel, out_shape=jax.ShapeDtypeStruct((32, GROUP), f32), name="last_sum"
-    )(last)
-    proj, proj_other = gathered_rows(branch_proj)
+    )(here_in_vmem(last))
     grad_normed = pl.pallas_call(
         token_grad_kernel,
         in_specs=[smem] + [VMEM] * 6,
@@ -432,15 +457,15 @@
         out_shape=jax.ShapeDtypeStruct((1024, SPAN), bf16),
         scratch_shapes=[pltpu.VMEM((16, 4, 16, SPAN), bf16)],
         name="token_grad",
-    )(place, proj, proj_other, *own_part)
+    )(place, proj, here_in_vmem(proj_other), *map(here_in_vmem, (own_part, *others)))
     return (
         grad_normed[None],
         grad_gate[None],
         grad_proj,
-        rest[0:CONV, 0:GROUP],
-        map_sums[None, :, 0:GROUP],
-        map_sums[None, :, GROUP:],
-        rest[CONV, 0:GROUP],
+        grad_conv,
+        grad_recur[None],
+        grad_input[None],
+        grad_decay[0],
     )
 
 

time: 140 us -> 128 us (0.914)
  the two profiles are of different devices: /device:TPU:4 before, /device:TPU:32 now
where the time goes in v2:
time: 128 us; the launch traced here: 127 us
  starting transfers between devices  67.9 us (53%)
  waiting for transfers between devices  31.6 us (25%)
  Pallas kernels  17.8 us (14%)
  local copies, waits for them, and re-layouts  7.47 us (6%)
  other arithmetic  1.82 us (1%)
    ppermute x9, starting transfers between devices, exchanged(): return lax.ppermute(array, axis, [(n, n ^ bit) for n in range(size)])  30.1 us
    all_to_all x1, starting transfers between devices, steps(): lax.all_to_all(cotangent[0].reshape(spans, GROUP, SPAN), 'sp', 0, 0, tile...  15.2 us
    all_to_all x1, waiting for transfers between devices, steps(): arrived = lax.all_to_all(pieces, DP, 0, 0, tiled=True)  12.8 us
    ppermute x9, waiting for transfers between devices, exchanged(): return lax.ppermute(array, axis, [(n, n ^ bit) for n in range(size)])  9.3 us
    all_to_all x1, starting transfers between devices, steps(): lax.all_to_all(gb.reshape(64, 16, SPAN), ('sp', 'y'), 0, 0, tiled=True)  8.91 us
    all_to_all x1, starting transfers between devices, steps(): last = lax.all_to_all(sums, 'sp', 0, 0, tiled=True)  7.65 us
    pallas_call x1, Pallas kernels, forward_part(): pl.pallas_call(forward_kernel, out_shape=[jax.ShapeDtypeStruct(FLAT, f32)...  6.23 us
    all_to_all x1, waiting for transfers between devices, steps(): lax.all_to_all(cotangent[0].reshape(spans, GROUP, SPAN), 'sp', 0, 0, tile...  6.14 us
  transfers between devices with their start and end apart: 13, of which 6 were waited for; matrix products, arithmetic and copies ran while one was open for 3% of the time, Pallas kernels for 13%

profile of v2, /device:TPU:32, one launch (start us, length us, event | category | flops | bytes accessed | tf_op | source)
XLA Modules:
  0.0 127.5 jit_solution(14427448022397115315)
XLA Ops:
  0.6 1.1 fusion
  1.7 3.5 %collective-permute-start = (bf16[1280,128]{1,0:T(8,128)(2,1)S(1)}, bf16[1280,128]{1,0:T(8,128)(2,1)S(1)}, u32[]{:S(2)}, u32[]{:S(2)}) collective-permute-start(bf16[1280,128]{1,0:T(8,128)(2,1)S(1)} %get-tuple-element.48), channel_id=1, source_target_pairs={{0,8},{8,0},{16,24},{24,16},{1,9},{9,1},{17,25},{25,17},{2,10},{10... | collective-permute-start | bytes 983048 | tf_op jit(solution)/shard_map/ppermute | solution.py:392
  5.2 15.2 %all-to-all-start = ((bf16[16,64,128]{2,1,0:T(8,128)(2,1)}), bf16[16,64,128]{2,1,0:T(8,128)(2,1)S(1)}, u32[]{:S(2)}, u32[]{:S(2)}) async-start(bf16[16,64,128]{2,1,0:T(8,128)(2,1)} %bitcast.13), calls=%async_computation | async-start | bytes 524288 | tf_op jit(solution)/shard_map/all_to_all | solution.py:404
  20.5 4.1 %collective-permute-start.1 = (bf16[2,1280,128]{2,1,0:T(8,128)(2,1)S(1)}, bf16[2,1280,128]{2,1,0:T(8,128)(2,1)S(1)}, u32[]{:S(2)}, u32[]{:S(2)}) collective-permute-start(bf16[2,1280,128]{2,1,0:T(8,128)(2,1)S(1)} %pad_maximum_fusion), channel_id=1, source_target_pairs={{0,24},{8,16},{16,8},{24,0},{1,25},{9,17},{17,9},{25,1},{2,26},{10... | collective-permute-start | bytes 1966088 | tf_op jit(solution)/shard_map/ppermute | solution.py:392
  24.6 6.2 %forward_part.1 = (f32[1024,128]{1,0:T(8,128)}, bf16[1024,128]{1,0:T(8,128)(2,1)}, bf16[1024,128]{1,0:T(8,128)(2,1)}, bf16[1024,128]{1,0:T(8,128)(2,1)}, bf16[10...) custom-call(bf16[64,2048]{1,0:T(8,128)(2,1)} %bitcast.49, ...), custom_call_target="tpu_custom_call" | custom-call | tf_op jit(solution)/shard_map/forward_part/pallas_call | solution.py:286
  32.1 6.1 %all-to-all-done.cot = bf16[16,64,128]{2,1,0:T(8,128)(2,1)S(1)} async-done(((bf16[16,64,128]{2,1,0:T(8,128)(2,1)}), bf16[16,64,128]{2,1,0:T(8,128)(2,1)S(1)}, u32[]{:S(2)}, u32[]{:S(2)}) %all-to-all-start) | async-done | bytes 262176 | tf_op jit(solution)/shard_map/all_to_all | solution.py:404
  38.3 1.0 copy-done
  39.3 0.9 copy-done.2
  40.3 0.9 copy-done.3
  41.2 0.9 copy-done.4
  42.2 4.6 %backward_part.1 = (bf16[16,64,128]{2,1,0:T(8,128)(2,1)}, bf16[64,2048]{1,0:T(8,128)(2,1)}, bf16[72,128]{1,0:T(8,128)(2,1)}) custom-call(bf16[16,64,128]{2,1,0:T(8,128)(2,1)S(1)} %all-to-all-done.cot, f32[1024,128]{1,0:T(8,128)S(1)} %copy-done, bf16[1024,128]{1,0:T(8,128)(2,1)S(1)} %copy-done.1, bf16[1024,128]{1,0:T(8,128)(2,1)S(1)} %copy-done.2, ...), custom_call_target="tpu_custom_call" | custom-call | tf_op jit(solution)/shard_map/backward_part/pallas_call | solution.py:303
  46.8 8.9 %all-to-all-start.1 = ((bf16[64,16,128]{2,1,0:T(8,128)(2,1)}), bf16[64,16,128]{2,1,0:T(8,128)(2,1)S(1)}, u32[]{:S(2)}, u32[]{:S(2)}) async-start(bf16[64,16,128]{2,1,0:T(8,128)(2,1)} %bitcast.51), calls=%async_computation.1 | async-start | bytes 524288 | tf_op jit(solution)/shard_map/all_to_all | solution.py:419
  55.7 0.7 fusion.1
  56.5 3.4 %collective-permute-start.2 = (bf16[4,256,128]{2,1,0:T(8,128)(2,1)S(1)}, bf16[4,256,128]{2,1,0:T(8,128)(2,1)S(1)}, u32[]{:S(2)}, u32[]{:S(2)}) collective-permute-start(bf16[4,256,128]{2,1,0:T(8,128)(2,1)S(1)} %pad_maximum_fusion.3), channel_id=1, source_target_pairs={{0,2},{2,0},{4,6},{6,4},{1,3},{3,1},{5,7},{7,5},{8,10},{10,8},{12,... | collective-permute-start | bytes 786440 | tf_op jit(solution)/shard_map/ppermute | solution.py:392
  59.9 5.9 %collective-permute-done.2 = bf16[4,256,128]{2,1,0:T(8,128)(2,1)S(1)} collective-permute-done((bf16[4,256,128]{2,1,0:T(8,128)(2,1)S(1)}, bf16[4,256,128]{2,1,0:T(8,128)(2,1)S(1)}, u32[]{:S(2)}, u32[]{:S(2)}) %collective-permute-start.2) | collective-permute-done | bytes 262176 | tf_op jit(solution)/shard_map/ppermute | solution.py:392
  65.8 4.7 %collective-permute-start.3 = (bf16[8,256,128]{2,1,0:T(8,128)(2,1)S(1)}, bf16[8,256,128]{2,1,0:T(8,128)(2,1)S(1)}, u32[]{:S(2)}, u32[]{:S(2)}) collective-permute-start(bf16[8,256,128]{2,1,0:T(8,128)(2,1)S(1)} %pad_maximum_fusion.1), channel_id=1, source_target_pairs={{0,6},{2,4},{4,2},{6,0},{1,7},{3,5},{5,3},{7,1},{8,14},{10,12},{12... | collective-permute-start | bytes 1572872 | tf_op jit(solution)/shard_map/ppermute | solution.py:392
  71.1 1.9 %collective-permute-start.8 = (bf16[72,128]{1,0:T(8,128)(2,1)S(1)}, bf16[72,128]{1,0:T(8,128)(2,1)S(1)}, u32[]{:S(2)}, u32[]{:S(2)}) collective-permute-start(bf16[72,128]{1,0:T(8,128)(2,1)S(1)} %copy-done.7), channel_id=1, source_target_pairs={{0,1},{1,0},{2,3},{3,2},{4,5},{5,4},{6,7},{7,6},{8,9},{9,8},{10,11... | collective-permute-start | bytes 55304 | tf_op jit(solution)/shard_map/ppermute | solution.py:392
  73.0 0.7 constant_dynamic-update-slice_fusion.1
  74.2 3.3 %all-to-all-done.1 = bf16[64,16,128]{2,1,0:T(8,128)(2,1)S(1)} async-done(((bf16[64,16,128]{2,1,0:T(8,128)(2,1)}), bf16[64,16,128]{2,1,0:T(8,128)(2,1)S(1)}, u32[]{:S(2)}, u32[]{:S(2)}) %all-to-all-start.1) | async-done | bytes 262176 | tf_op jit(solution)/shard_map/all_to_all | solution.py:419
  77.5 2.7 %product.1 = bf16[32,56,256]{2,1,0:T(8,128)(2,1)} custom-call(s32[3]{0:T(128)} %pad_add_fusion.place, bf16[72,128]{1,0:T(8,128)(2,1)} %get-tuple-element.39.small, bf16[72,128]{1,0:T(8,128)(2,1)S(1)} %collective-permute-done.8.partner, bf16[1024,128]{1,0:T(8,128)(2,1)} %bitcast.44, bf16[1280,128]{1,0:T(8,128)(2,1)} %copy-done.5, ...), custom_call_target="tpu_custom_call" | custom-call | tf_op jit(solution)/shard_map/product/pallas_call | solution.py:424
  80.2 6.0 %all-to-all-start.2 = ((bf16[32,56,256]{2,1,0:T(8,128)(2,1)}), bf16[32,56,256]{2,1,0:T(8,128)(2,1)S(1)}, u32[]{:S(2)}, u32[]{:S(2)}) async-start(bf16[32,56,256]{2,1,0:T(8,128)(2,1)} %product.1), calls=%async_computation.2 | async-start | bytes 1835008 | tf_op jit(solution)/shard_map/all_to_all | solution.py:431
  86.3 0.8 constant_dynamic-update-slice_fusion.proj
  87.1 2.2 %collective-permute-start.4 = (bf16[16,256,128]{2,1,0:T(8,128)(2,1)}, bf16[16,256,128]{2,1,0:T(8,128)(2,1)S(1)}, u32[]{:S(2)}, u32[]{:S(2)}) collective-permute-start(bf16[16,256,128]{2,1,0:T(8,128)(2,1)} %constant_dynamic-update-slice_fusion.proj), channel_id=1, source_target_pairs={{0,1},{1,0},{2,3},{3,2},{4,5},{5,4},{6,7},{7,6},{8,9},{9,8},{10,11... | collective-permute-start | bytes 3145736 | tf_op jit(solution)/shard_map/ppermute | solution.py:392
  89.3 12.8 %all-to-all-done.2.arrived = bf16[32,56,256]{2,1,0:T(8,128)(2,1)S(1)} async-done(((bf16[32,56,256]{2,1,0:T(8,128)(2,1)}), bf16[32,56,256]{2,1,0:T(8,128)(2,1)S(1)}, u32[]{:S(2)}, u32[]{:S(2)}) %all-to-all-start.2) | async-done | bytes 917536 | tf_op jit(solution)/shard_map/all_to_all | solution.py:431
  102.1 0.9 gather_sum.1
  103.0 7.6 %all-to-all-start.3 = ((bf16[16,16,128]{2,1,0:T(8,128)(2,1)}), bf16[16,16,128]{2,1,0:T(8,128)(2,1)S(1)}, u32[]{:S(2)}, u32[]{:S(2)}) async-start(bf16[16,16,128]{2,1,0:T(8,128)(2,1)} %get-tuple-element.40), calls=%async_computation.3 | async-start | bytes 131072 | tf_op jit(solution)/shard_map/all_to_all | solution.py:449
  110.7 1.9 %collective-permute-start.5 = (bf16[16,16,128]{2,1,0:T(8,128)(2,1)S(1)}, bf16[16,16,128]{2,1,0:T(8,128)(2,1)S(1)}, u32[]{:S(2)}, u32[]{:S(2)}) collective-permute-start(bf16[16,16,128]{2,1,0:T(8,128)(2,1)S(1)} %get-tuple-element.51), channel_id=1, source_target_pairs={{0,8},{8,0},{16,24},{24,16},{1,9},{9,1},{17,25},{25,17},{2,10},{10... | collective-permute-start | bytes 196616 | tf_op jit(solution)/shard_map/ppermute | solution.py:392
  112.6 4.1 %collective-permute-start.6 = (bf16[16,16,128]{2,1,0:T(8,128)(2,1)S(1)}, bf16[16,16,128]{2,1,0:T(8,128)(2,1)S(1)}, u32[]{:S(2)}, u32[]{:S(2)}) collective-permute-start(bf16[16,16,128]{2,1,0:T(8,128)(2,1)S(1)} %get-tuple-element.50), channel_id=1, source_target_pairs={{0,16},{8,24},{16,0},{24,8},{1,17},{9,25},{17,1},{25,9},{2,18},{10... | collective-permute-start | bytes 196616 | tf_op jit(solution)/shard_map/ppermute | solution.py:392
  116.7 4.4 %collective-permute-start.7 = (bf16[16,16,128]{2,1,0:T(8,128)(2,1)S(1)}, bf16[16,16,128]{2,1,0:T(8,128)(2,1)S(1)}, u32[]{:S(2)}, u32[]{:S(2)}) collective-permute-start(bf16[16,16,128]{2,1,0:T(8,128)(2,1)S(1)} %get-tuple-element.49), channel_id=1, source_target_pairs={{0,24},{8,16},{16,8},{24,0},{1,25},{9,17},{17,9},{25,1},{2,26},{10... | collective-permute-start | bytes 196616 | tf_op jit(solution)/shard_map/ppermute | solution.py:392
  121.2 3.0 %collective-permute-done.7.three = bf16[16,16,128]{2,1,0:T(8,128)(2,1)S(1)} collective-permute-done((bf16[16,16,128]{2,1,0:T(8,128)(2,1)S(1)}, bf16[16,16,128]{2,1,0:T(8,128)(2,1)S(1)}, u32[]{:S(2)}, u32[]{:S(2)}) %collective-permute-start.7) | collective-permute-done | bytes 65568 | tf_op jit(solution)/shard_map/ppermute | solution.py:392
  124.1 2.7 %token_grad.1 = bf16[1024,128]{1,0:T(8,128)(2,1)} custom-call(s32[3]{0:T(128)} %pad_add_fusion.place, bf16[16,256,128]{2,1,0:T(8,128)(2,1)} %constant_dynamic-update-slice_fusion.proj, bf16[16,256,128]{2,1,0:T(8,128)(2,1)S(1)} %collective-permute-done.4.proj_other, bf16[16,16,128]{2,1,0:T(8,128)(2,1)S(1)} %get-tuple-element.52.own, ...), custom_call_target="tpu_custom_call" | custom-call | tf_op jit(solution)/shard_map/token_grad/pallas_call | solution.py:453
  126.8 0.7 last_sum.1
  (28 shorter events, 2.5 us)
Async XLA Ops:
  1.7 18.7 %collective-permute-start = (bf16[1280,128]{1,0:T(8,128)(2,1)S(1)}, bf16[1280,128]{1,0:T(8,128)(2,1)S(1)}, u32[]{:S(2)}, u32[]{:S(2)}) collective-permute-start(bf16[1280,128]{1,0:T(8,128)(2,1)S(1)} %get-tuple-element.48), channel_id=1, source_target_pairs={{0,8},{8,0},{16,24},{24,16},{1,9},{9,1},{17,25},{25,17},{2,10},{10... | collective-permute-start | bytes 983048 | tf_op jit(solution)/shard_map/ppermute | solution.py:392
  5.2 33.1 %all-to-all-start = ((bf16[16,64,128]{2,1,0:T(8,128)(2,1)}), bf16[16,64,128]{2,1,0:T(8,128)(2,1)S(1)}, u32[]{:S(2)}, u32[]{:S(2)}) async-start(bf16[16,64,128]{2,1,0:T(8,128)(2,1)} %bitcast.13), calls=%async_computation | async-start | bytes 524288 | tf_op jit(solution)/shard_map/all_to_all | solution.py:404
  20.4 11.1 %copy-start.5 = (bf16[1280,128]{1,0:T(8,128)(2,1)}, bf16[1280,128]{1,0:T(8,128)(2,1)S(1)}, u32[]{:S(2)}) copy-start(bf16[1280,128]{1,0:T(8,128)(2,1)S(1)} %collective-permute-done.near) | copy-start | bytes 983044
  20.5 35.2 %collective-permute-start.1 = (bf16[2,1280,128]{2,1,0:T(8,128)(2,1)S(1)}, bf16[2,1280,128]{2,1,0:T(8,128)(2,1)S(1)}, u32[]{:S(2)}, u32[]{:S(2)}) collective-permute-start(bf16[2,1280,128]{2,1,0:T(8,128)(2,1)S(1)} %pad_maximum_fusion), channel_id=1, source_target_pairs={{0,24},{8,16},{16,8},{24,0},{1,25},{9,17},{17,9},{25,1},{2,26},{10... | collective-permute-start | bytes 1966088 | tf_op jit(solution)/shard_map/ppermute | solution.py:392
  24.6 6.2 %copy-start.6 = (bf16[32,1024]{1,0:T(8,128)(2,1)S(1)}, bf16[32,1024]{1,0:T(8,128)(2,1)}, u32[]{:S(2)}) copy-start(bf16[32,1024]{1,0:T(8,128)(2,1)} %param.19) | copy-start | bytes 196612
  30.9 7.4 %copy-start.1 = (bf16[1024,128]{1,0:T(8,128)(2,1)S(1)}, bf16[1024,128]{1,0:T(8,128)(2,1)}, u32[]{:S(2)}) copy-start(bf16[1024,128]{1,0:T(8,128)(2,1)} %get-tuple-element.27.c0_r) | copy-start | bytes 786436
  38.3 1.0 copy-start
  39.3 0.9 copy-start.2
  40.3 0.9 copy-start.3
  41.2 0.9 copy-start.4
  46.8 30.7 %all-to-all-start.1 = ((bf16[64,16,128]{2,1,0:T(8,128)(2,1)}), bf16[64,16,128]{2,1,0:T(8,128)(2,1)S(1)}, u32[]{:S(2)}, u32[]{:S(2)}) async-start(bf16[64,16,128]{2,1,0:T(8,128)(2,1)} %bitcast.51), calls=%async_computation.1 | async-start | bytes 524288 | tf_op jit(solution)/shard_map/all_to_all | solution.py:419
  56.5 9.3 %collective-permute-start.2 = (bf16[4,256,128]{2,1,0:T(8,128)(2,1)S(1)}, bf16[4,256,128]{2,1,0:T(8,128)(2,1)S(1)}, u32[]{:S(2)}, u32[]{:S(2)}) collective-permute-start(bf16[4,256,128]{2,1,0:T(8,128)(2,1)S(1)} %pad_maximum_fusion.3), channel_id=1, source_target_pairs={{0,2},{2,0},{4,6},{6,4},{1,3},{3,1},{5,7},{7,5},{8,10},{10,8},{12,... | collective-permute-start | bytes 786440 | tf_op jit(solution)/shard_map/ppermute | solution.py:392
  65.8 5.3 %copy-start.7 = (bf16[72,128]{1,0:T(8,128)(2,1)S(1)}, bf16[72,128]{1,0:T(8,128)(2,1)}, u32[]{:S(2)}) copy-start(bf16[72,128]{1,0:T(8,128)(2,1)} %get-tuple-element.39.small) | copy-start | bytes 55300
  65.8 20.4 %collective-permute-start.3 = (bf16[8,256,128]{2,1,0:T(8,128)(2,1)S(1)}, bf16[8,256,128]{2,1,0:T(8,128)(2,1)S(1)}, u32[]{:S(2)}, u32[]{:S(2)}) collective-permute-start(bf16[8,256,128]{2,1,0:T(8,128)(2,1)S(1)} %pad_maximum_fusion.1), channel_id=1, source_target_pairs={{0,6},{2,4},{4,2},{6,0},{1,7},{3,5},{5,3},{7,1},{8,14},{10,12},{12... | collective-permute-start | bytes 1572872 | tf_op jit(solution)/shard_map/ppermute | solution.py:392
  71.1 3.1 %collective-permute-start.8 = (bf16[72,128]{1,0:T(8,128)(2,1)S(1)}, bf16[72,128]{1,0:T(8,128)(2,1)S(1)}, u32[]{:S(2)}, u32[]{:S(2)}) collective-permute-start(bf16[72,128]{1,0:T(8,128)(2,1)S(1)} %copy-done.7), channel_id=1, source_target_pairs={{0,1},{1,0},{2,3},{3,2},{4,5},{5,4},{6,7},{7,6},{8,9},{9,8},{10,11... | collective-permute-start | bytes 55304 | tf_op jit(solution)/shard_map/ppermute | solution.py:392
  80.2 21.9 %all-to-all-start.2 = ((bf16[32,56,256]{2,1,0:T(8,128)(2,1)}), bf16[32,56,256]{2,1,0:T(8,128)(2,1)S(1)}, u32[]{:S(2)}, u32[]{:S(2)}) async-start(bf16[32,56,256]{2,1,0:T(8,128)(2,1)} %product.1), calls=%async_computation.2 | async-start | bytes 1835008 | tf_op jit(solution)/shard_map/all_to_all | solution.py:431
  87.1 37.0 %collective-permute-start.4 = (bf16[16,256,128]{2,1,0:T(8,128)(2,1)}, bf16[16,256,128]{2,1,0:T(8,128)(2,1)S(1)}, u32[]{:S(2)}, u32[]{:S(2)}) collective-permute-start(bf16[16,256,128]{2,1,0:T(8,128)(2,1)} %constant_dynamic-update-slice_fusion.proj), channel_id=1, source_target_pairs={{0,1},{1,0},{2,3},{3,2},{4,5},{5,4},{6,7},{7,6},{8,9},{9,8},{10,11... | collective-permute-start | bytes 3145736 | tf_op jit(solution)/shard_map/ppermute | solution.py:392
  103.0 23.8 %all-to-all-start.3 = ((bf16[16,16,128]{2,1,0:T(8,128)(2,1)}), bf16[16,16,128]{2,1,0:T(8,128)(2,1)S(1)}, u32[]{:S(2)}, u32[]{:S(2)}) async-start(bf16[16,16,128]{2,1,0:T(8,128)(2,1)} %get-tuple-element.40), calls=%async_computation.3 | async-start | bytes 131072 | tf_op jit(solution)/shard_map/all_to_all | solution.py:449
  110.7 10.4 %collective-permute-start.5 = (bf16[16,16,128]{2,1,0:T(8,128)(2,1)S(1)}, bf16[16,16,128]{2,1,0:T(8,128)(2,1)S(1)}, u32[]{:S(2)}, u32[]{:S(2)}) collective-permute-start(bf16[16,16,128]{2,1,0:T(8,128)(2,1)S(1)} %get-tuple-element.51), channel_id=1, source_target_pairs={{0,8},{8,0},{16,24},{24,16},{1,9},{9,1},{17,25},{25,17},{2,10},{10... | collective-permute-start | bytes 196616 | tf_op jit(solution)/shard_map/ppermute | solution.py:392
  112.6 8.5 %collective-permute-start.6 = (bf16[16,16,128]{2,1,0:T(8,128)(2,1)S(1)}, bf16[16,16,128]{2,1,0:T(8,128)(2,1)S(1)}, u32[]{:S(2)}, u32[]{:S(2)}) collective-permute-start(bf16[16,16,128]{2,1,0:T(8,128)(2,1)S(1)} %get-tuple-element.50), channel_id=1, source_target_pairs={{0,16},{8,24},{16,0},{24,8},{1,17},{9,25},{17,1},{25,9},{2,18},{10... | collective-permute-start | bytes 196616 | tf_op jit(solution)/shard_map/ppermute | solution.py:392
  116.7 7.4 %collective-permute-start.7 = (bf16[16,16,128]{2,1,0:T(8,128)(2,1)S(1)}, bf16[16,16,128]{2,1,0:T(8,128)(2,1)S(1)}, u32[]{:S(2)}, u32[]{:S(2)}) collective-permute-start(bf16[16,16,128]{2,1,0:T(8,128)(2,1)S(1)} %get-tuple-element.49), channel_id=1, source_target_pairs={{0,24},{8,16},{16,8},{24,0},{1,25},{9,17},{17,9},{25,1},{2,26},{10... | collective-permute-start | bytes 196616 | tf_op jit(solution)/shard_map/ppermute | solution.py:392

commit v3 on v2

--- a/solution.py
+++ b/solution.py
@@ -77,12 +77,31 @@
     return jnp.concatenate([top, low], axis=0)
 
 
+def gelu_parts(g):
+    c = 0.7978845608028654
+    inner = jnp.tanh(c * (g + 0.044715 * (g * g * g)))
+    part = 0.5 + 0.5 * inner
+    return g * part, part + 0.5 * g * (1.0 - inner * inner) * (c * (1.0 + 3 * 0.044715 * (g * g)))
+
+
 def forward_kernel(
     branch, gate, shift, conv, decay_param, recur_map, input_map,
-    next_o, c0_o, c1_o, c2_o, c3_o, branch_o, turned_o, g0_o, g1_o, back_o, rows,
-    b_s, decay_s, fed_s, slope_s, rate_s, recur_s, local_s, power_s,
+    next_h, c0_h, c1_h, c2_h, c3_h, branch_h, turned_h, g0_h, state_h, back_o, rows,
+    next_o, c0_o, c1_o, c2_o, c3_o, branch_o, turned_o, g0_o,
+    b_s, decay_s, fed_s, slope_s, rate_s, recur_s, local_s, power_s, state_s, sems,
 ):
+    copies = [
+        pltpu.make_async_copy(source, target, sems.at[n])
+        for n, (source, target) in enumerate(
+            (
+                (g0_o, g0_h), (next_o, next_h), (c0_o, c0_h), (c1_o, c1_h), (branch_o, branch_h),
+                (turned_o, turned_h), (c2_o, c2_h), (c3_o, c3_h), (state_s, state_h),
+            )
+        )
+    ]
     lane = lanes((GROUP, SPAN))
+    g0_o[...] = gelu_parts(gate[...].astype(f32))[0].astype(bf16)
+    copies[0].start()
     minus = -decay_param[...]
     softened = jnp.maximum(minus, 0.0) + jnp.log1p(jnp.exp(-jnp.abs(minus)))
     table = jnp.concatenate(
@@ -98,16 +117,14 @@
     back_high, back_low = high_low(halves(jnp.transpose(first), jnp.transpose(second)))
     back_o[0] = back_high
     back_o[1] = back_low
+    wide = lanes((SPAN, SPAN)) < GROUP
+    turned_shift = jnp.transpose(shift[...])
     for p in range(8):
         at = slice(p * SPAN, (p + 1) * SPAN)
         far = slice((8 + p) * SPAN, (9 + p) * SPAN)
-        b_s[pl.ds(24 + p, SPAN, stride=8), :] = jnp.transpose(
-            halves(branch[:, at].astype(f32), branch[:, far].astype(f32))
-        )
-        fed_s[pl.ds(p, SPAN, stride=8), :] = jnp.transpose(
-            halves(
-                jnp.broadcast_to(shift[:, at], (GROUP, SPAN)), jnp.broadcast_to(shift[:, far], (GROUP, SPAN))
-            )
+        b_s[pl.ds(24 + p, SPAN, stride=8), :] = jnp.transpose(halves(branch[:, at], branch[:, far])).astype(f32)
+        fed_s[pl.ds(p, SPAN, stride=8), :] = jnp.where(
+            wide, tiled(turned_shift[:, p : p + 1]), tiled(turned_shift[:, 8 + p : 9 + p])
         )
     for m in range(3):
         b_s[8 * m : 8 * m + 8, :] = before_of(b_s[1024 + 8 * m : 1032 + 8 * m, :])
@@ -146,11 +163,14 @@
         recur_s[here, :] = recur
         c0_o[here, :] = (root * inp).astype(bf16)
         c1_o[here, :] = (pushed * (0.5 - 0.5 * ti)).astype(bf16)
-        turned_o[:, here] = jnp.transpose(x).astype(bf16)
+        turned_o[:, here] = jnp.transpose(x_high)
         return 0
 
-    lax.fori_loop(0, 8, gates, 0)
-
+    lax.fori_loop(0, 8, gates, 0, unroll=8)
+    next_o[0:1016, :] = decay_s[8:1024, :]
+    next_o[1016:1024, :] = after_of(decay_s[0:8, :])
+    for copy in copies[1:6]:
+        copy.start()
     local_s[0:8, :] = jnp.zeros((8, SPAN), f32)
     power_s[0:8, :] = jnp.ones((8, SPAN), f32)
 
@@ -176,34 +196,36 @@
         slope = previous * decay - slope_s[here, :]
         c2_o[here, :] = (slope * rate_s[here, :]).astype(bf16)
         c3_o[here, :] = (slope * recur_s[here, :]).astype(bf16)
-        fed_s[here, :] = local_s[moved_block(n, 8), :] + power_s[moved_block(n, 8), :] * enters
+        state_s[here, :] = local_s[moved_block(n, 8), :] + power_s[moved_block(n, 8), :] * enters
         return 0
 
     lax.fori_loop(0, 8, slopes, 0)
-    next_o[0:1016, :] = decay_s[8:1024, :]
-    next_o[1016:1024, :] = after_of(decay_s[0:8, :])
+    for copy in copies[6:]:
+        copy.start()
+    for copy in copies:
+        copy.wait()
+
+
+def gate_kernel(cot, gate, state_r, gate_o):
     for p in range(8):
-        state = jnp.transpose(strided(fed_s, p))
-        for half, at in ((0, slice(p * SPAN, (p + 1) * SPAN)), (1, slice((8 + p) * SPAN, (9 + p) * SPAN))):
-            g = gate[:, at].astype(f32)
-            c = 0.7978845608028654
-            inner = jnp.tanh(c * (g + 0.044715 * (g * g * g)))
-            part = 0.5 + 0.5 * inner
-            turn = part + 0.5 * g * (1.0 - inner * inner) * (c * (1.0 + 3 * 0.044715 * (g * g)))
-            g0_o[:, at] = (g * part).astype(bf16)
-            g1_o[:, at] = (state[GROUP * half : GROUP * half + GROUP] * turn).astype(bf16)
+        state = jnp.transpose(strided(state_r, p))
+        for half in range(2):
+            j = 8 * half + p
+            at = slice(j * SPAN, (j + 1) * SPAN)
+            turn = gelu_parts(gate[:, at].astype(f32))[1]
+            here = state[GROUP * half : GROUP * half + GROUP]
+            gate_o[:, at] = (cot[j].astype(f32) * here * turn).astype(bf16)
 
 
 def backward_kernel(
-    cot, next_r, c0_r, c1_r, c2_r, c3_r, branch_r, turned_r, g0_r, g1_r, back_r, rows,
-    gb_o, gate_o, small_o, d_s, local_s, power_s, dx_s, pushed_s,
+    cot, next_r, c0_r, c1_r, c2_r, c3_r, branch_r, turned_r, g0_r, back_r, rows,
+    gb_o, small_o, d_s, local_s, power_s, dx_s, pushed_s,
 ):
     for p in range(8):
         parts = []
         for j in (p, 8 + p):
             at = slice(j * SPAN, (j + 1) * SPAN)
             c = cot[j].astype(f32)
-            gate_o[:, at] = (c * g1_r[:, at].astype(f32)).astype(bf16)
             parts.append(c * g0_r[:, at].astype(f32))
         d_s[pl.ds(p, SPAN, stride=8), :] = jnp.transpose(halves(*parts))
 
@@ -238,7 +260,7 @@
         return total + summed(grad * c3_r[here, :].astype(f32))
 
     zero = jnp.zeros((8, SPAN), f32)
-    decays = lax.fori_loop(0, 8, spread, zero)
+    decays = lax.fori_loop(0, 8, spread, zero, unroll=8)
     for m in range(3):
         dx_s[1024 + 8 * m : 1032 + 8 * m, :] = after_of(dx_s[8 * m : 8 * m + 8, :])
 
@@ -254,7 +276,7 @@
         d_s[here, :] = gb
         return tuple(out)
 
-    totals = lax.fori_loop(0, 8, taps, (zero,) * CONV)
+    totals = lax.fori_loop(0, 8, taps, (zero,) * CONV, unroll=8)
     for p in range(8):
         gb = jnp.transpose(strided(d_s, p)).astype(bf16)
         gb_o[p] = gb[:GROUP]
@@ -273,6 +295,7 @@
 
 
 VMEM = pl.BlockSpec(memory_space=pltpu.VMEM)
+ANY = pl.BlockSpec(memory_space=pl.ANY)
 FLAT = (1024, SPAN)
 
 
@@ -281,20 +304,18 @@
 
 
 def forward_part(branch, gate, shift, conv, decay_param, recur_map, input_map):
-    flat = jax.ShapeDtypeStruct(FLAT, bf16)
-    plain = jax.ShapeDtypeStruct(branch.shape, bf16)
+    flat = [(FLAT, f32)] + [(FLAT, bf16)] * 5 + [((SPAN, 1024), bf16), (branch.shape, bf16)]
+    ends = [((2, 2 * SPAN, SPAN), bf16), ((8, SPAN), f32)]
     return pl.pallas_call(
         forward_kernel,
-        out_shape=[
-            jax.ShapeDtypeStruct(FLAT, f32),
-            *[flat] * 5,
-            jax.ShapeDtypeStruct((SPAN, 1024), bf16),
-            plain,
-            plain,
-            jax.ShapeDtypeStruct((2, 2 * SPAN, SPAN), bf16),
-            jax.ShapeDtypeStruct((8, SPAN), f32),
-        ],
-        scratch_shapes=[pltpu.VMEM((1048, SPAN), f32)] + [pltpu.VMEM(FLAT, f32)] * 5 + [pltpu.VMEM((1032, SPAN), f32)] * 2,
+        in_specs=[VMEM] * 7,
+        out_specs=[ANY] * 9 + [VMEM] * 2,
+        out_shape=[jax.ShapeDtypeStruct(*each) for each in (*flat, (FLAT, f32), *ends)],
+        scratch_shapes=[pltpu.VMEM(*each) for each in flat]
+        + [pltpu.VMEM((1048, SPAN), f32)]
+        + [pltpu.VMEM(FLAT, f32)] * 5
+        + [pltpu.VMEM((1032, SPAN), f32)] * 2
+        + [pltpu.VMEM(FLAT, f32), pltpu.SemaphoreType.DMA((9,))],
         name="forward_part",
     )(branch, gate, shift, conv, decay_param, recur_map, input_map)
 
@@ -304,12 +325,17 @@
         backward_kernel,
         out_shape=[
             jax.ShapeDtypeStruct((16, GROUP, SPAN), bf16),
-            jax.ShapeDtypeStruct((GROUP, 2048), bf16),
             jax.ShapeDtypeStruct((GROUP + 8, 2 * GROUP), bf16),
         ],
         scratch_shapes=[pltpu.VMEM(FLAT, f32)] * 3 + [pltpu.VMEM((1048, SPAN), f32), pltpu.VMEM((1024, 2 * SPAN), bf16)],
         name="backward_part",
     )(cot, *saved)
+
+
+def gate_part(cot, gate, state):
+    return pl.pallas_call(gate_kernel, out_shape=jax.ShapeDtypeStruct(gate.shape, bf16), name="gate_part")(
+        cot, gate, state
+    )
 
 
 def product_kernel(place, small, partner, own, near, far, grads, out):
@@ -393,7 +419,8 @@
 
 
 def joined(array, axis, bits):
-    return jnp.concatenate([array, exchanged(array, axis, bits)], axis=0)
+    both = lax.optimization_barrier((array, exchanged(array, axis, bits)))
+    return jnp.concatenate(both, axis=0)
 
 
 def steps(
@@ -402,9 +429,11 @@
 ):
     spans = lax.axis_size("sp")
     cot = lax.all_to_all(cotangent[0].reshape(spans, GROUP, SPAN), "sp", 0, 0, tiled=True)
-    saved = forward_part(
-        branch_in[0], gate_pre[0], decay_shift[0], conv_weight, decay_param[None], recur_weight[0], input_weight[0]
+    *saved, state, back_maps, taps = forward_part(
+        here_in_vmem(branch_in[0]), here_in_vmem(gate_pre[0]), decay_shift.reshape(spans, SPAN),
+        conv_weight, decay_param[None], recur_weight[0], input_weight[0],
     )
+    saved = [*map(here_in_vmem, saved[:4]), *saved[4:], back_maps, taps]
     own = normed[0]
     width = branch_proj.shape[1] // SPAN
     rows = branch_proj.reshape(4, 8, width, SPAN).transpose(0, 2, 1, 3).reshape(-1, SPAN)
@@ -414,7 +443,7 @@
     held = jnp.stack([rows, near[1024:], far[0, 1024:], far[1, 1024:]])
     proj = joined(joined(held, "x", 1), "x", 3)
     proj_other = exchanged(proj, "core", 1)
-    gb, grad_gate, small = backward_part(here_in_vmem(cot), [*map(here_in_vmem, saved[:5]), *saved[5:]])
+    gb, small = backward_part(here_in_vmem(cot), saved)
     partner = exchanged(small, "core", 1)
     grads = lax.all_to_all(gb.reshape(64, 16, SPAN), ("sp", "y"), 0, 0, tiled=True)
     grads = grads.reshape(16, 4, 16, SPAN)
@@ -427,7 +456,7 @@
         out_specs=VMEM,
         out_shape=jax.ShapeDtypeStruct((32, 56, 256), bf16),
         name="product",
-    )(place, small, here_in_vmem(partner), own, near, here_in_vmem(far), here_in_vmem(grads))
+    )(place, small, here_in_vmem(partner), own, near, far, here_in_vmem(grads))
     arrived = lax.all_to_all(pieces, DP, 0, 0, tiled=True)
 
     def part_for(n):
@@ -458,6 +487,7 @@
         scratch_shapes=[pltpu.VMEM((16, 4, 16, SPAN), bf16)],
         name="token_grad",
     )(place, proj, here_in_vmem(proj_other), *map(here_in_vmem, (own_part, *others)))
+    grad_gate = gate_part(cot, gate_pre[0], state)
     return (
         grad_normed[None],
         grad_gate[None],

time: 128 us -> 141 us (1.10)
  waiting for transfers between devices: 31.6 us -> 41 us
  starting transfers between devices: 67.9 us -> 72.9 us
  local copies, waits for them, and re-layouts: 7.47 us -> 5.8 us
    ppermute x9, waiting for transfers between devices: 9.3 us -> 22.9 us  [exchanged(): return lax.ppermute(array, axis, [(n, n ^ bit) for n in range(size)])]
    all_to_all x1, waiting for transfers between devices: 6.14 us -> 0.01 us  [steps(): lax.all_to_all(cotangent[0].reshape(spans, GROUP, SPAN), 'sp', 0, 0, tile...]
    all_to_all x1, starting transfers between devices: 8.91 us -> 14.2 us  [steps(): lax.all_to_all(gb.reshape(64, 16, SPAN), ('sp', 'y'), 0, 0, tiled=True)]
    pallas_call x1 -> x2, Pallas kernels: 6.23 us -> 7.36 us  [the longest x1 5.02 us: forward_part(): pl.pallas_call(forward_kernel, in_specs=[VMEM] * 7, out_specs=[ANY] * 9 +...]
    unnamed x19 -> x30, local copies, waits for them, and re-layouts: 5.9 us -> 5.65 us
  transfers between devices with their start and end apart: 13 -> 13, of which waited for: 6 -> 5; matrix products, arithmetic and copies ran while one was open for 3% -> 1% of each run, Pallas kernels for 13% -> 10%
where the time goes in v3:
time: 141 us; the launch traced here: 140 us
  starting transfers between devices  72.9 us (52%)
  waiting for transfers between devices  41 us (29%)
  Pallas kernels  18 us (13%)
  local copies, waits for them, and re-layouts  5.8 us (4%)
  other arithmetic  1.76 us (1%)
    ppermute x9, starting transfers between devices, exchanged(): return lax.ppermute(array, axis, [(n, n ^ bit) for n in range(size)])  29.6 us
    ppermute x9, waiting for transfers between devices, exchanged(): return lax.ppermute(array, axis, [(n, n ^ bit) for n in range(size)])  22.9 us
    all_to_all x1, starting transfers between devices, steps(): lax.all_to_all(cotangent[0].reshape(spans, GROUP, SPAN), 'sp', 0, 0, tile...  15.2 us
    all_to_all x1, starting transfers between devices, steps(): lax.all_to_all(gb.reshape(64, 16, SPAN), ('sp', 'y'), 0, 0, tiled=True)  14.2 us
    all_to_all x1, waiting for transfers between devices, steps(): arrived = lax.all_to_all(pieces, DP, 0, 0, tiled=True)  13.6 us
    all_to_all x1, starting transfers between devices, steps(): last = lax.all_to_all(sums, 'sp', 0, 0, tiled=True)  7.87 us
    all_to_all x1, starting transfers between devices, steps(): arrived = lax.all_to_all(pieces, DP, 0, 0, tiled=True)  6.03 us
    unnamed x30, local copies, waits for them, and re-layouts  5.65 us
  transfers between devices with their start and end apart: 13, of which 5 were waited for; matrix products, arithmetic and copies ran while one was open for 1% of the time, Pallas kernels for 10%

profile of v3, /device:TPU:32, one launch (start us, length us, event | category | flops | bytes accessed | tf_op | source)
XLA Modules:
  0.0 140.4 jit_solution(6417465967232621362)
XLA Ops:
  0.6 1.1 fusion
  1.7 3.5 %collective-permute-start = (bf16[1280,128]{1,0:T(8,128)(2,1)S(1)}, bf16[1280,128]{1,0:T(8,128)(2,1)S(1)}, u32[]{:S(2)}, u32[]{:S(2)}) collective-permute-start(bf16[1280,128]{1,0:T(8,128)(2,1)S(1)} %get-tuple-element.52), channel_id=1, source_target_pairs={{0,8},{8,0},{16,24},{24,16},{1,9},{9,1},{17,25},{25,17},{2,10},{10... | collective-permute-start | bytes 983048 | tf_op jit(solution)/shard_map/ppermute | solution.py:418
  5.2 15.2 %all-to-all-start = ((bf16[16,64,128]{2,1,0:T(8,128)(2,1)}), bf16[16,64,128]{2,1,0:T(8,128)(2,1)S(1)}, u32[]{:S(2)}, u32[]{:S(2)}) async-start(bf16[16,64,128]{2,1,0:T(8,128)(2,1)} %bitcast.12), calls=%async_computation | async-start | bytes 524288 | tf_op jit(solution)/shard_map/all_to_all | solution.py:431
  20.5 4.1 %collective-permute-start.1 = (bf16[2,1280,128]{2,1,0:T(8,128)(2,1)S(1)}, bf16[2,1280,128]{2,1,0:T(8,128)(2,1)S(1)}, u32[]{:S(2)}, u32[]{:S(2)}) collective-permute-start(bf16[2,1280,128]{2,1,0:T(8,128)(2,1)S(1)} %pad_maximum_fusion), channel_id=1, source_target_pairs={{0,24},{8,16},{16,8},{24,0},{1,25},{9,17},{17,9},{25,1},{2,26},{10... | collective-permute-start | bytes 1966088 | tf_op jit(solution)/shard_map/ppermute | solution.py:418
  24.6 14.6 %collective-permute-done.1.far = bf16[2,1280,128]{2,1,0:T(8,128)(2,1)S(1)} collective-permute-done((bf16[2,1280,128]{2,1,0:T(8,128)(2,1)S(1)}, bf16[2,1280,128]{2,1,0:T(8,128)(2,1)S(1)}, u32[]{:S(2)}, u32[]{:S(2)}) %collective-permute-start.1) | collective-permute-done | bytes 655392 | tf_op jit(solution)/shard_map/ppermute | solution.py:418
  39.3 0.8 copy-done.9
  40.1 3.5 %collective-permute-start.2 = (bf16[4,256,128]{2,1,0:T(8,128)(2,1)S(1)}, bf16[4,256,128]{2,1,0:T(8,128)(2,1)S(1)}, u32[]{:S(2)}, u32[]{:S(2)}) collective-permute-start(bf16[4,256,128]{2,1,0:T(8,128)(2,1)S(1)} %pad_maximum_fusion.2), channel_id=1, source_target_pairs={{0,2},{2,0},{4,6},{6,4},{1,3},{3,1},{5,7},{7,5},{8,10},{10,8},{12,... | collective-permute-start | bytes 786440 | tf_op jit(solution)/shard_map/ppermute | solution.py:418
  43.7 5.0 %forward_part.1 = (f32[1024,128]{1,0:T(8,128)}, bf16[1024,128]{1,0:T(8,128)(2,1)}, bf16[1024,128]{1,0:T(8,128)(2,1)}, bf16[1024,128]{1,0:T(8,128)(2,1)}, bf16[10...) custom-call(bf16[64,2048]{1,0:T(8,128)(2,1)S(1)} %bitcast.42, ...), custom_call_target="tpu_custom_call" | custom-call | tf_op jit(solution)/shard_map/forward_part/pallas_call | solution.py:309
  48.8 1.1 copy-done.2
  49.9 0.9 copy-done.4
  50.8 0.9 copy-done.5
  51.8 0.9 copy-done.6
  52.7 3.4 %backward_part.1 = (bf16[16,64,128]{2,1,0:T(8,128)(2,1)}, bf16[72,128]{1,0:T(8,128)(2,1)}) custom-call(bf16[16,64,128]{2,1,0:T(8,128)(2,1)S(1)} %all-to-all-done.cot, f32[1024,128]{1,0:T(8,128)S(1)} %copy-done.2, bf16[1024,128]{1,0:T(8,128)(2,1)S(1)} %copy-done.4, bf16[1024,128]{1,0:T(8,128)(2,1)S(1)} %copy-done.5, bf16[1024,128]{1,0:T(8,128)(2,1)S(1)} %copy-done.6, ...), custom_call_target="tpu_custom_call" | custom-call | tf_op jit(solution)/shard_map/backward_part/pallas_call | solution.py:324
  56.2 14.2 %all-to-all-start.1 = ((bf16[64,16,128]{2,1,0:T(8,128)(2,1)}), bf16[64,16,128]{2,1,0:T(8,128)(2,1)S(1)}, u32[]{:S(2)}, u32[]{:S(2)}) async-start(bf16[64,16,128]{2,1,0:T(8,128)(2,1)} %bitcast.47), calls=%async_computation.1 | async-start | bytes 524288 | tf_op jit(solution)/shard_map/all_to_all | solution.py:448
  70.5 4.0 %collective-permute-start.3 = (bf16[8,256,128]{2,1,0:T(8,128)(2,1)S(1)}, bf16[8,256,128]{2,1,0:T(8,128)(2,1)S(1)}, u32[]{:S(2)}, u32[]{:S(2)}) collective-permute-start(bf16[8,256,128]{2,1,0:T(8,128)(2,1)S(1)} %constant_dynamic-update-slice_fusion), channel_id=1, source_target_pairs={{0,6},{2,4},{4,2},{6,0},{1,7},{3,5},{5,3},{7,1},{8,14},{10,12},{12... | collective-permute-start | bytes 1572872 | tf_op jit(solution)/shard_map/ppermute | solution.py:418
  75.1 1.9 %collective-permute-start.8 = (bf16[72,128]{1,0:T(8,128)(2,1)S(1)}, bf16[72,128]{1,0:T(8,128)(2,1)S(1)}, u32[]{:S(2)}, u32[]{:S(2)}) collective-permute-start(bf16[72,128]{1,0:T(8,128)(2,1)S(1)} %copy-done.13), channel_id=1, source_target_pairs={{0,1},{1,0},{2,3},{3,2},{4,5},{5,4},{6,7},{7,6},{8,9},{9,8},{10,11... | collective-permute-start | bytes 55304 | tf_op jit(solution)/shard_map/ppermute | solution.py:418
  77.0 7.7 %collective-permute-done.3 = bf16[8,256,128]{2,1,0:T(8,128)(2,1)S(1)} collective-permute-done((bf16[8,256,128]{2,1,0:T(8,128)(2,1)S(1)}, bf16[8,256,128]{2,1,0:T(8,128)(2,1)S(1)}, u32[]{:S(2)}, u32[]{:S(2)}) %collective-permute-start.3) | collective-permute-done | bytes 524320 | tf_op jit(solution)/shard_map/ppermute | solution.py:418
  84.7 0.8 copy-done.10
  85.5 4.5 %all-to-all-done.1 = bf16[64,16,128]{2,1,0:T(8,128)(2,1)S(1)} async-done(((bf16[64,16,128]{2,1,0:T(8,128)(2,1)}), bf16[64,16,128]{2,1,0:T(8,128)(2,1)S(1)}, u32[]{:S(2)}, u32[]{:S(2)}) %all-to-all-start.1) | async-done | bytes 262176 | tf_op jit(solution)/shard_map/all_to_all | solution.py:448
  90.0 2.9 %product.1 = bf16[32,56,256]{2,1,0:T(8,128)(2,1)} custom-call(s32[3]{0:T(128)} %pad_add_fusion.place, bf16[72,128]{1,0:T(8,128)(2,1)} %get-tuple-element.45.small, bf16[72,128]{1,0:T(8,128)(2,1)S(1)} %collective-permute-done.8.partner, bf16[1024,128]{1,0:T(8,128)(2,1)} %bitcast.45, bf16[1280,128]{1,0:T(8,128)(2,1)} %copy-done.8, ...), custom_call_target="tpu_custom_call" | custom-call | tf_op jit(solution)/shard_map/product/pallas_call | solution.py:453
  92.9 6.0 %all-to-all-start.2 = ((bf16[32,56,256]{2,1,0:T(8,128)(2,1)}), bf16[32,56,256]{2,1,0:T(8,128)(2,1)S(1)}, u32[]{:S(2)}, u32[]{:S(2)}) async-start(bf16[32,56,256]{2,1,0:T(8,128)(2,1)} %product.1), calls=%async_computation.2 | async-start | bytes 1835008 | tf_op jit(solution)/shard_map/all_to_all | solution.py:460
  99.1 2.2 %collective-permute-start.4 = (bf16[16,256,128]{2,1,0:T(8,128)(2,1)S(1)}, bf16[16,256,128]{2,1,0:T(8,128)(2,1)S(1)}, u32[]{:S(2)}, u32[]{:S(2)}) collective-permute-start(bf16[16,256,128]{2,1,0:T(8,128)(2,1)S(1)} %constant_dynamic-update-slice_fusion.2.proj), channel_id=1, source_target_pairs={{0,1},{1,0},{2,3},{3,2},{4,5},{5,4},{6,7},{7,6},{8,9},{9,8},{10,11... | collective-permute-start | bytes 3145736 | tf_op jit(solution)/shard_map/ppermute | solution.py:418
  101.3 13.6 %all-to-all-done.2.arrived = bf16[32,56,256]{2,1,0:T(8,128)(2,1)S(1)} async-done(((bf16[32,56,256]{2,1,0:T(8,128)(2,1)}), bf16[32,56,256]{2,1,0:T(8,128)(2,1)S(1)}, u32[]{:S(2)}, u32[]{:S(2)}) %all-to-all-start.2) | async-done | bytes 917536 | tf_op jit(solution)/shard_map/all_to_all | solution.py:460
  114.8 0.9 gather_sum.1
  115.7 7.9 %all-to-all-start.3 = ((bf16[16,16,128]{2,1,0:T(8,128)(2,1)}), bf16[16,16,128]{2,1,0:T(8,128)(2,1)S(1)}, u32[]{:S(2)}, u32[]{:S(2)}) async-start(bf16[16,16,128]{2,1,0:T(8,128)(2,1)} %get-tuple-element.46), calls=%async_computation.3 | async-start | bytes 131072 | tf_op jit(solution)/shard_map/all_to_all | solution.py:478
  123.6 1.9 %collective-permute-start.5 = (bf16[16,16,128]{2,1,0:T(8,128)(2,1)S(1)}, bf16[16,16,128]{2,1,0:T(8,128)(2,1)S(1)}, u32[]{:S(2)}, u32[]{:S(2)}) collective-permute-start(bf16[16,16,128]{2,1,0:T(8,128)(2,1)S(1)} %get-tuple-element.55), channel_id=1, source_target_pairs={{0,8},{8,0},{16,24},{24,16},{1,9},{9,1},{17,25},{25,17},{2,10},{10... | collective-permute-start | bytes 196616 | tf_op jit(solution)/shard_map/ppermute | solution.py:418
  125.5 4.1 %collective-permute-start.6 = (bf16[16,16,128]{2,1,0:T(8,128)(2,1)S(1)}, bf16[16,16,128]{2,1,0:T(8,128)(2,1)S(1)}, u32[]{:S(2)}, u32[]{:S(2)}) collective-permute-start(bf16[16,16,128]{2,1,0:T(8,128)(2,1)S(1)} %get-tuple-element.54), channel_id=1, source_target_pairs={{0,16},{8,24},{16,0},{24,8},{1,17},{9,25},{17,1},{25,9},{2,18},{10... | collective-permute-start | bytes 196616 | tf_op jit(solution)/shard_map/ppermute | solution.py:418
  129.7 4.4 %collective-permute-start.7 = (bf16[16,16,128]{2,1,0:T(8,128)(2,1)S(1)}, bf16[16,16,128]{2,1,0:T(8,128)(2,1)S(1)}, u32[]{:S(2)}, u32[]{:S(2)}) collective-permute-start(bf16[16,16,128]{2,1,0:T(8,128)(2,1)S(1)} %get-tuple-element.53), channel_id=1, source_target_pairs={{0,24},{8,16},{16,8},{24,0},{1,25},{9,17},{17,9},{25,1},{2,26},{10... | collective-permute-start | bytes 196616 | tf_op jit(solution)/shard_map/ppermute | solution.py:418
  134.1 2.3 %gate_part.1 = bf16[64,2048]{1,0:T(8,128)(2,1)} custom-call(bf16[16,64,128]{2,1,0:T(8,128)(2,1)} %copy-done, bf16[64,2048]{1,0:T(8,128)(2,1)} %bitcast.40, f32[1024,128]{1,0:T(8,128)} %get-tuple-element.44.state_r), custom_call_target="tpu_custom_call" | custom-call | tf_op jit(solution)/shard_map/gate_part/pallas_call | solution.py:336
  136.4 0.6 collective-permute-done.7.three
  137.0 2.7 %token_grad.1 = bf16[1024,128]{1,0:T(8,128)(2,1)} custom-call(s32[3]{0:T(128)} %pad_add_fusion.place, bf16[16,256,128]{2,1,0:T(8,128)(2,1)} %copy-done.7, bf16[16,256,128]{2,1,0:T(8,128)(2,1)S(1)} %collective-permute-done.4.proj_other, bf16[16,16,128]{2,1,0:T(8,128)(2,1)S(1)} %get-tuple-element.56.own, bf16[16,16,128]{2,1,0:T(8,128)(2,1)S(1)} %collective-permute-done.5.one, ...), custom_call_target="tpu_custom_call" | custom-call | tf_op jit(solution)/shard_map/token_grad/pallas_call | solution.py:482
  139.7 0.7 last_sum.1
  (40 shorter events, 1.0 us)
Async XLA Ops:
  1.7 18.7 %collective-permute-start = (bf16[1280,128]{1,0:T(8,128)(2,1)S(1)}, bf16[1280,128]{1,0:T(8,128)(2,1)S(1)}, u32[]{:S(2)}, u32[]{:S(2)}) collective-permute-start(bf16[1280,128]{1,0:T(8,128)(2,1)S(1)} %get-tuple-element.52), channel_id=1, source_target_pairs={{0,8},{8,0},{16,24},{24,16},{1,9},{9,1},{17,25},{25,17},{2,10},{10... | collective-permute-start | bytes 983048 | tf_op jit(solution)/shard_map/ppermute | solution.py:418
  5.2 43.5 %all-to-all-start = ((bf16[16,64,128]{2,1,0:T(8,128)(2,1)}), bf16[16,64,128]{2,1,0:T(8,128)(2,1)S(1)}, u32[]{:S(2)}, u32[]{:S(2)}) async-start(bf16[16,64,128]{2,1,0:T(8,128)(2,1)} %bitcast.12), calls=%async_computation | async-start | bytes 524288 | tf_op jit(solution)/shard_map/all_to_all | solution.py:431
  20.4 4.2 %copy-start.8 = (bf16[1280,128]{1,0:T(8,128)(2,1)}, bf16[1280,128]{1,0:T(8,128)(2,1)S(1)}, u32[]{:S(2)}) copy-start(bf16[1280,128]{1,0:T(8,128)(2,1)S(1)} %collective-permute-done.near) | copy-start | bytes 983044
  20.5 18.7 %collective-permute-start.1 = (bf16[2,1280,128]{2,1,0:T(8,128)(2,1)S(1)}, bf16[2,1280,128]{2,1,0:T(8,128)(2,1)S(1)}, u32[]{:S(2)}, u32[]{:S(2)}) collective-permute-start(bf16[2,1280,128]{2,1,0:T(8,128)(2,1)S(1)} %pad_maximum_fusion), channel_id=1, source_target_pairs={{0,24},{8,16},{16,8},{24,0},{1,25},{9,17},{17,9},{25,1},{2,26},{10... | collective-permute-start | bytes 1966088 | tf_op jit(solution)/shard_map/ppermute | solution.py:418
  24.6 15.5 %copy-start.12 = (bf16[32,1024]{1,0:T(8,128)(2,1)S(1)}, bf16[32,1024]{1,0:T(8,128)(2,1)}, u32[]{:S(2)}) copy-start(bf16[32,1024]{1,0:T(8,128)(2,1)} %param.19) | copy-start | bytes 196612
  39.3 0.8 copy-start.9
  40.1 3.6 %copy-start.1 = (bf16[1,64,2048]{2,1,0:T(8,128)(2,1)S(1)}, bf16[1,64,2048]{2,1,0:T(8,128)(2,1)}, u32[]{:S(2)}) copy-start(bf16[1,64,2048]{2,1,0:T(8,128)(2,1)} %param.12) | copy-start | bytes 786436
  40.1 3.6 %copy-start.3 = (bf16[1,64,2048]{2,1,0:T(8,128)(2,1)S(1)}, bf16[1,64,2048]{2,1,0:T(8,128)(2,1)}, u32[]{:S(2)}) copy-start(bf16[1,64,2048]{2,1,0:T(8,128)(2,1)} %param.11) | copy-start | bytes 786436
  40.1 30.2 %collective-permute-start.2 = (bf16[4,256,128]{2,1,0:T(8,128)(2,1)S(1)}, bf16[4,256,128]{2,1,0:T(8,128)(2,1)S(1)}, u32[]{:S(2)}, u32[]{:S(2)}) collective-permute-start(bf16[4,256,128]{2,1,0:T(8,128)(2,1)S(1)} %pad_maximum_fusion.2), channel_id=1, source_target_pairs={{0,2},{2,0},{4,6},{6,4},{1,3},{3,1},{5,7},{7,5},{8,10},{10,8},{12,... | collective-permute-start | bytes 786440 | tf_op jit(solution)/shard_map/ppermute | solution.py:418
  48.7 7.4 %copy-start = (bf16[16,64,128]{2,1,0:T(8,128)(2,1)}, bf16[16,64,128]{2,1,0:T(8,128)(2,1)S(1)}, u32[]{:S(2)}) copy-start(bf16[16,64,128]{2,1,0:T(8,128)(2,1)S(1)} %all-to-all-done.cot) | copy-start | bytes 786436
  48.7 1.1 copy-start.2
  49.9 0.9 copy-start.4
  50.8 0.9 copy-start.5
  51.8 0.9 copy-start.6
  56.2 33.9 %all-to-all-start.1 = ((bf16[64,16,128]{2,1,0:T(8,128)(2,1)}), bf16[64,16,128]{2,1,0:T(8,128)(2,1)S(1)}, u32[]{:S(2)}, u32[]{:S(2)}) async-start(bf16[64,16,128]{2,1,0:T(8,128)(2,1)} %bitcast.47), calls=%async_computation.1 | async-start | bytes 524288 | tf_op jit(solution)/shard_map/all_to_all | solution.py:448
  70.4 4.6 %copy-start.13 = (bf16[72,128]{1,0:T(8,128)(2,1)S(1)}, bf16[72,128]{1,0:T(8,128)(2,1)}, u32[]{:S(2)}) copy-start(bf16[72,128]{1,0:T(8,128)(2,1)} %get-tuple-element.45.small) | copy-start | bytes 55300
  70.5 14.2 %collective-permute-start.3 = (bf16[8,256,128]{2,1,0:T(8,128)(2,1)S(1)}, bf16[8,256,128]{2,1,0:T(8,128)(2,1)S(1)}, u32[]{:S(2)}, u32[]{:S(2)}) collective-permute-start(bf16[8,256,128]{2,1,0:T(8,128)(2,1)S(1)} %constant_dynamic-update-slice_fusion), channel_id=1, source_target_pairs={{0,6},{2,4},{4,2},{6,0},{1,7},{3,5},{5,3},{7,1},{8,14},{10,12},{12... | collective-permute-start | bytes 1572872 | tf_op jit(solution)/shard_map/ppermute | solution.py:418
  75.1 10.4 %collective-permute-start.8 = (bf16[72,128]{1,0:T(8,128)(2,1)S(1)}, bf16[72,128]{1,0:T(8,128)(2,1)S(1)}, u32[]{:S(2)}, u32[]{:S(2)}) collective-permute-start(bf16[72,128]{1,0:T(8,128)(2,1)S(1)} %copy-done.13), channel_id=1, source_target_pairs={{0,1},{1,0},{2,3},{3,2},{4,5},{5,4},{6,7},{7,6},{8,9},{9,8},{10,11... | collective-permute-start | bytes 55304 | tf_op jit(solution)/shard_map/ppermute | solution.py:418
  84.7 0.8 copy-start.10
  92.9 6.0 %copy-start.11 = (bf16[8,256,128]{2,1,0:T(8,128)(2,1)S(1)}, bf16[8,256,128]{2,1,0:T(8,128)(2,1)}, u32[]{:S(2)}) copy-start(bf16[8,256,128]{2,1,0:T(8,128)(2,1)} %copy-done.10) | copy-start | bytes 1572868
  92.9 21.9 %all-to-all-start.2 = ((bf16[32,56,256]{2,1,0:T(8,128)(2,1)}), bf16[32,56,256]{2,1,0:T(8,128)(2,1)S(1)}, u32[]{:S(2)}, u32[]{:S(2)}) async-start(bf16[32,56,256]{2,1,0:T(8,128)(2,1)} %product.1), calls=%async_computation.2 | async-start | bytes 1835008 | tf_op jit(solution)/shard_map/all_to_all | solution.py:460
  99.1 37.3 %copy-start.7 = (bf16[16,256,128]{2,1,0:T(8,128)(2,1)}, bf16[16,256,128]{2,1,0:T(8,128)(2,1)S(1)}, u32[]{:S(2)}) copy-start(bf16[16,256,128]{2,1,0:T(8,128)(2,1)S(1)} %constant_dynamic-update-slice_fusion.2.proj) | copy-start | bytes 3145732
  99.1 38.0 %collective-permute-start.4 = (bf16[16,256,128]{2,1,0:T(8,128)(2,1)S(1)}, bf16[16,256,128]{2,1,0:T(8,128)(2,1)S(1)}, u32[]{:S(2)}, u32[]{:S(2)}) collective-permute-start(bf16[16,256,128]{2,1,0:T(8,128)(2,1)S(1)} %constant_dynamic-update-slice_fusion.2.proj), channel_id=1, source_target_pairs={{0,1},{1,0},{2,3},{3,2},{4,5},{5,4},{6,7},{7,6},{8,9},{9,8},{10,11... | collective-permute-start | bytes 3145736 | tf_op jit(solution)/shard_map/ppermute | solution.py:418
  115.7 24.0 %all-to-all-start.3 = ((bf16[16,16,128]{2,1,0:T(8,128)(2,1)}), bf16[16,16,128]{2,1,0:T(8,128)(2,1)S(1)}, u32[]{:S(2)}, u32[]{:S(2)}) async-start(bf16[16,16,128]{2,1,0:T(8,128)(2,1)} %get-tuple-element.46), calls=%async_computation.3 | async-start | bytes 131072 | tf_op jit(solution)/shard_map/all_to_all | solution.py:478
  123.6 12.8 %collective-permute-start.5 = (bf16[16,16,128]{2,1,0:T(8,128)(2,1)S(1)}, bf16[16,16,128]{2,1,0:T(8,128)(2,1)S(1)}, u32[]{:S(2)}, u32[]{:S(2)}) collective-permute-start(bf16[16,16,128]{2,1,0:T(8,128)(2,1)S(1)} %get-tuple-element.55), channel_id=1, source_target_pairs={{0,8},{8,0},{16,24},{24,16},{1,9},{9,1},{17,25},{25,17},{2,10},{10... | collective-permute-start | bytes 196616 | tf_op jit(solution)/shard_map/ppermute | solution.py:418
  125.5 10.9 %collective-permute-start.6 = (bf16[16,16,128]{2,1,0:T(8,128)(2,1)S(1)}, bf16[16,16,128]{2,1,0:T(8,128)(2,1)S(1)}, u32[]{:S(2)}, u32[]{:S(2)}) collective-permute-start(bf16[16,16,128]{2,1,0:T(8,128)(2,1)S(1)} %get-tuple-element.54), channel_id=1, source_target_pairs={{0,16},{8,24},{16,0},{24,8},{1,17},{9,25},{17,1},{25,9},{2,18},{10... | collective-permute-start | bytes 196616 | tf_op jit(solution)/shard_map/ppermute | solution.py:418
  129.7 7.4 %collective-permute-start.7 = (bf16[16,16,128]{2,1,0:T(8,128)(2,1)S(1)}, bf16[16,16,128]{2,1,0:T(8,128)(2,1)S(1)}, u32[]{:S(2)}, u32[]{:S(2)}) collective-permute-start(bf16[16,16,128]{2,1,0:T(8,128)(2,1)S(1)} %get-tuple-element.53), channel_id=1, source_target_pairs={{0,24},{8,16},{16,8},{24,0},{1,25},{9,17},{17,9},{25,1},{2,26},{10... | collective-permute-start | bytes 196616 | tf_op jit(solution)/shard_map/ppermute | solution.py:418

commit v4 on v3

--- a/solution.py
+++ b/solution.py
@@ -86,8 +86,8 @@
 
 def forward_kernel(
     branch, gate, shift, conv, decay_param, recur_map, input_map,
-    next_h, c0_h, c1_h, c2_h, c3_h, branch_h, turned_h, g0_h, state_h, back_o, rows,
-    next_o, c0_o, c1_o, c2_o, c3_o, branch_o, turned_o, g0_o,
+    next_h, c0_h, c1_h, c2_h, c3_h, branch_h, turned_h, g0_h, g1_h, back_o, rows,
+    next_o, c0_o, c1_o, c2_o, c3_o, branch_o, turned_o, g0_o, g1_o,
     b_s, decay_s, fed_s, slope_s, rate_s, recur_s, local_s, power_s, state_s, sems,
 ):
     copies = [
@@ -95,7 +95,7 @@
         for n, (source, target) in enumerate(
             (
                 (g0_o, g0_h), (next_o, next_h), (c0_o, c0_h), (c1_o, c1_h), (branch_o, branch_h),
-                (turned_o, turned_h), (c2_o, c2_h), (c3_o, c3_h), (state_s, state_h),
+                (turned_o, turned_h), (c2_o, c2_h), (c3_o, c3_h), (g1_o, g1_h),
             )
         )
     ]
@@ -200,21 +200,17 @@
         return 0
 
     lax.fori_loop(0, 8, slopes, 0)
-    for copy in copies[6:]:
+    for copy in copies[6:8]:
         copy.start()
+    for p in range(8):
+        state = jnp.transpose(strided(state_s, p))
+        for half in range(2):
+            at = slice((8 * half + p) * SPAN, (8 * half + p + 1) * SPAN)
+            turn = gelu_parts(gate[:, at].astype(f32))[1]
+            g1_o[:, at] = (state[GROUP * half : GROUP * half + GROUP] * turn).astype(bf16)
+    copies[8].start()
     for copy in copies:
         copy.wait()
-
-
-def gate_kernel(cot, gate, state_r, gate_o):
-    for p in range(8):
-        state = jnp.transpose(strided(state_r, p))
-        for half in range(2):
-            j = 8 * half + p
-            at = slice(j * SPAN, (j + 1) * SPAN)
-            turn = gelu_parts(gate[:, at].astype(f32))[1]
-            here = state[GROUP * half : GROUP * half + GROUP]
-            gate_o[:, at] = (cot[j].astype(f32) * here * turn).astype(bf16)
 
 
 def backward_kernel(
@@ -304,13 +300,13 @@
 
 
 def forward_part(branch, gate, shift, conv, decay_param, recur_map, input_map):
-    flat = [(FLAT, f32)] + [(FLAT, bf16)] * 5 + [((SPAN, 1024), bf16), (branch.shape, bf16)]
+    flat = [(FLAT, f32)] + [(FLAT, bf16)] * 5 + [((SPAN, 1024), bf16)] + [(branch.shape, bf16)] * 2
     ends = [((2, 2 * SPAN, SPAN), bf16), ((8, SPAN), f32)]
     return pl.pallas_call(
         forward_kernel,
         in_specs=[VMEM] * 7,
         out_specs=[ANY] * 9 + [VMEM] * 2,
-        out_shape=[jax.ShapeDtypeStruct(*each) for each in (*flat, (FLAT, f32), *ends)],
+        out_shape=[jax.ShapeDtypeStruct(*each) for each in (*flat, *ends)],
         scratch_shapes=[pltpu.VMEM(*each) for each in flat]
         + [pltpu.VMEM((1048, SPAN), f32)]
         + [pltpu.VMEM(FLAT, f32)] * 5
@@ -330,12 +326,6 @@
         scratch_shapes=[pltpu.VMEM(FLAT, f32)] * 3 + [pltpu.VMEM((1048, SPAN), f32), pltpu.VMEM((1024, 2 * SPAN), bf16)],
         name="backward_part",
     )(cot, *saved)
-
-
-def gate_part(cot, gate, state):
-    return pl.pallas_call(gate_kernel, out_shape=jax.ShapeDtypeStruct(gate.shape, bf16), name="gate_part")(
-        cot, gate, state
-    )
 
 
 def product_kernel(place, small, partner, own, near, far, grads, out):
@@ -394,7 +384,10 @@
     out[16:32, :] = pltpu.roll(total, GROUP, 1)[:, 0:GROUP]
 
 
-def token_grad_kernel(place, proj, proj_other, own, one, two, three, out, tokens_s):
+def token_grad_kernel(place, proj, proj_other, own, one, two, three, cot, g1, out, gate_o, tokens_s):
+    for j in range(cot.shape[0]):
+        at = slice(j * SPAN, (j + 1) * SPAN)
+        gate_o[:, at] = (cot[j].astype(f32) * g1[:, at].astype(f32)).astype(bf16)
     for n, piece in enumerate((own, one, two, three)):
         tokens_s[:, place[0] ^ n] = piece[...]
     tokens = tokens_s[...].reshape(1024, SPAN)
@@ -429,7 +422,7 @@
 ):
     spans = lax.axis_size("sp")
     cot = lax.all_to_all(cotangent[0].reshape(spans, GROUP, SPAN), "sp", 0, 0, tiled=True)
-    *saved, state, back_maps, taps = forward_part(
+    *saved, g1, back_maps, taps = forward_part(
         here_in_vmem(branch_in[0]), here_in_vmem(gate_pre[0]), decay_shift.reshape(spans, SPAN),
         conv_weight, decay_param[None], recur_weight[0], input_weight[0],
     )
@@ -456,7 +449,7 @@
         out_specs=VMEM,
         out_shape=jax.ShapeDtypeStruct((32, 56, 256), bf16),
         name="product",
-    )(place, small, here_in_vmem(partner), own, near, far, here_in_vmem(grads))
+    )(place, small, here_in_vmem(partner), own, here_in_vmem(near), here_in_vmem(far), here_in_vmem(grads))
     arrived = lax.all_to_all(pieces, DP, 0, 0, tiled=True)
 
     def part_for(n):
@@ -479,15 +472,14 @@
     grad_proj = pl.pallas_call(
         last_sum_kernel, out_shape=jax.ShapeDtypeStruct((32, GROUP), f32), name="last_sum"
     )(here_in_vmem(last))
-    grad_normed = pl.pallas_call(
+    grad_normed, grad_gate = pl.pallas_call(
         token_grad_kernel,
-        in_specs=[smem] + [VMEM] * 6,
-        out_specs=VMEM,
-        out_shape=jax.ShapeDtypeStruct((1024, SPAN), bf16),
+        in_specs=[smem] + [VMEM] * 8,
+        out_specs=[VMEM] * 2,
+        out_shape=[jax.ShapeDtypeStruct((1024, SPAN), bf16), jax.ShapeDtypeStruct(g1.shape, bf16)],
         scratch_shapes=[pltpu.VMEM((16, 4, 16, SPAN), bf16)],
         name="token_grad",
-    )(place, proj, here_in_vmem(proj_other), *map(here_in_vmem, (own_part, *others)))
-    grad_gate = gate_part(cot, gate_pre[0], state)
+    )(place, proj, here_in_vmem(proj_other), *map(here_in_vmem, (own_part, *others)), cot, g1)
     return (
         grad_normed[None],
         grad_gate[None],

time: 141 us -> 141 us (level)
  Pallas kernels: 18 us -> 15.7 us
  waiting for transfers between devices: 41 us -> 42.5 us
    ppermute x9, waiting for transfers between devices: 22.9 us -> 25.3 us  [exchanged(): return lax.ppermute(array, axis, [(n, n ^ bit) for n in range(size)])]
    pallas_call x2 -> x1, Pallas kernels: 5.02 us -> 2.91 us  [steps(): pl.pallas_call(token_grad_kernel, in_specs=[smem] + [VMEM] * 8, out_specs...]
    unnamed x30 -> x24, local copies, waits for them, and re-layouts: 5.65 us -> 5.03 us
  transfers between devices with their start and end apart: 13 -> 13, of which waited for: 5 -> 5; matrix products, arithmetic and copies ran while one was open for 1% -> 2% of each run, Pallas kernels for 10% -> 9%
where the time goes in v4:
time: 141 us; the launch traced here: 140 us
  starting transfers between devices  73.1 us (52%)
  waiting for transfers between devices  42.5 us (30%)
  Pallas kernels  15.7 us (11%)
  local copies, waits for them, and re-layouts  5.96 us (4%)
  other arithmetic  1.72 us (1%)
    ppermute x9, starting transfers between devices, exchanged(): return lax.ppermute(array, axis, [(n, n ^ bit) for n in range(size)])  29.6 us
    ppermute x9, waiting for transfers between devices, exchanged(): return lax.ppermute(array, axis, [(n, n ^ bit) for n in range(size)])  25.3 us
    all_to_all x1, starting transfers between devices, steps(): lax.all_to_all(cotangent[0].reshape(spans, GROUP, SPAN), 'sp', 0, 0, tile...  15.2 us
    all_to_all x1, starting transfers between devices, steps(): lax.all_to_all(gb.reshape(64, 16, SPAN), ('sp', 'y'), 0, 0, tiled=True)  14.2 us
    all_to_all x1, waiting for transfers between devices, steps(): arrived = lax.all_to_all(pieces, DP, 0, 0, tiled=True)  12.8 us
    all_to_all x1, starting transfers between devices, steps(): last = lax.all_to_all(sums, 'sp', 0, 0, tiled=True)  8.09 us
    all_to_all x1, starting transfers between devices, steps(): arrived = lax.all_to_all(pieces, DP, 0, 0, tiled=True)  6.03 us
    pallas_call x1, Pallas kernels, forward_part(): pl.pallas_call(forward_kernel, in_specs=[VMEM] * 7, out_specs=[ANY] * 9 +...  5.17 us
  transfers between devices with their start and end apart: 13, of which 5 were waited for; matrix products, arithmetic and copies ran while one was open for 2% of the time, Pallas kernels for 9%

profile of v4, /device:TPU:32, one launch (start us, length us, event | category | flops | bytes accessed | tf_op | source)
XLA Modules:
  0.0 139.9 jit_solution(4330993885298544118)
XLA Ops:
  0.6 1.1 fusion
  1.7 3.5 %collective-permute-start = (bf16[1280,128]{1,0:T(8,128)(2,1)S(1)}, bf16[1280,128]{1,0:T(8,128)(2,1)S(1)}, u32[]{:S(2)}, u32[]{:S(2)}) collective-permute-start(bf16[1280,128]{1,0:T(8,128)(2,1)S(1)} %get-tuple-element.56), channel_id=1, source_target_pairs={{0,8},{8,0},{16,24},{24,16},{1,9},{9,1},{17,25},{25,17},{2,10},{10... | collective-permute-start | bytes 983048 | tf_op jit(solution)/shard_map/ppermute | solution.py:411
  5.2 15.2 %all-to-all-start = ((bf16[16,64,128]{2,1,0:T(8,128)(2,1)}), bf16[16,64,128]{2,1,0:T(8,128)(2,1)S(1)}, u32[]{:S(2)}, u32[]{:S(2)}) async-start(bf16[16,64,128]{2,1,0:T(8,128)(2,1)} %bitcast.12), calls=%async_computation | async-start | bytes 524288 | tf_op jit(solution)/shard_map/all_to_all | solution.py:424
  20.5 4.1 %collective-permute-start.1 = (bf16[2,1280,128]{2,1,0:T(8,128)(2,1)S(1)}, bf16[2,1280,128]{2,1,0:T(8,128)(2,1)S(1)}, u32[]{:S(2)}, u32[]{:S(2)}) collective-permute-start(bf16[2,1280,128]{2,1,0:T(8,128)(2,1)S(1)} %pad_maximum_fusion), channel_id=1, source_target_pairs={{0,24},{8,16},{16,8},{24,0},{1,25},{9,17},{17,9},{25,1},{2,26},{10... | collective-permute-start | bytes 1966088 | tf_op jit(solution)/shard_map/ppermute | solution.py:411
  24.6 14.6 %collective-permute-done.1.far = bf16[2,1280,128]{2,1,0:T(8,128)(2,1)S(1)} collective-permute-done((bf16[2,1280,128]{2,1,0:T(8,128)(2,1)S(1)}, bf16[2,1280,128]{2,1,0:T(8,128)(2,1)S(1)}, u32[]{:S(2)}, u32[]{:S(2)}) %collective-permute-start.1) | collective-permute-done | bytes 655392 | tf_op jit(solution)/shard_map/ppermute | solution.py:411
  39.3 3.5 %collective-permute-start.2 = (bf16[4,256,128]{2,1,0:T(8,128)(2,1)S(1)}, bf16[4,256,128]{2,1,0:T(8,128)(2,1)S(1)}, u32[]{:S(2)}, u32[]{:S(2)}) collective-permute-start(bf16[4,256,128]{2,1,0:T(8,128)(2,1)S(1)} %pad_maximum_fusion.2), channel_id=1, source_target_pairs={{0,2},{2,0},{4,6},{6,4},{1,3},{3,1},{5,7},{7,5},{8,10},{10,8},{12,... | collective-permute-start | bytes 786440 | tf_op jit(solution)/shard_map/ppermute | solution.py:411
  42.9 5.2 %forward_part.1 = (f32[1024,128]{1,0:T(8,128)}, bf16[1024,128]{1,0:T(8,128)(2,1)}, bf16[1024,128]{1,0:T(8,128)(2,1)}, bf16[1024,128]{1,0:T(8,128)(2,1)}, bf16[10...) custom-call(bf16[64,2048]{1,0:T(8,128)(2,1)S(1)} %bitcast.41, ...), custom_call_target="tpu_custom_call" | custom-call | tf_op jit(solution)/shard_map/forward_part/pallas_call | solution.py:305
  48.1 1.1 copy-done.1
  49.2 0.9 copy-done.4
  50.2 0.9 copy-done.5
  51.1 0.9 copy-done.6
  52.1 3.4 %backward_part.1 = (bf16[16,64,128]{2,1,0:T(8,128)(2,1)}, bf16[72,128]{1,0:T(8,128)(2,1)}) custom-call(bf16[16,64,128]{2,1,0:T(8,128)(2,1)S(1)} %all-to-all-done.cot, f32[1024,128]{1,0:T(8,128)S(1)} %copy-done.1, bf16[1024,128]{1,0:T(8,128)(2,1)S(1)} %copy-done.4, bf16[1024,128]{1,0:T(8,128)(2,1)S(1)} %copy-done.5, bf16[1024,128]{1,0:T(8,128)(2,1)S(1)} %copy-done.6, ...), custom_call_target="tpu_custom_call" | custom-call | tf_op jit(solution)/shard_map/backward_part/pallas_call | solution.py:320
  55.5 14.2 %all-to-all-start.1 = ((bf16[64,16,128]{2,1,0:T(8,128)(2,1)}), bf16[64,16,128]{2,1,0:T(8,128)(2,1)S(1)}, u32[]{:S(2)}, u32[]{:S(2)}) async-start(bf16[64,16,128]{2,1,0:T(8,128)(2,1)} %bitcast.45), calls=%async_computation.1 | async-start | bytes 524288 | tf_op jit(solution)/shard_map/all_to_all | solution.py:441
  69.8 4.0 %collective-permute-start.3 = (bf16[8,256,128]{2,1,0:T(8,128)(2,1)S(1)}, bf16[8,256,128]{2,1,0:T(8,128)(2,1)S(1)}, u32[]{:S(2)}, u32[]{:S(2)}) collective-permute-start(bf16[8,256,128]{2,1,0:T(8,128)(2,1)S(1)} %constant_dynamic-update-slice_fusion), channel_id=1, source_target_pairs={{0,6},{2,4},{4,2},{6,0},{1,7},{3,5},{5,3},{7,1},{8,14},{10,12},{12... | collective-permute-start | bytes 1572872 | tf_op jit(solution)/shard_map/ppermute | solution.py:411
  73.8 0.6 pad_add_fusion.place
  74.4 1.9 %collective-permute-start.8 = (bf16[72,128]{1,0:T(8,128)(2,1)S(1)}, bf16[72,128]{1,0:T(8,128)(2,1)S(1)}, u32[]{:S(2)}, u32[]{:S(2)}) collective-permute-start(bf16[72,128]{1,0:T(8,128)(2,1)S(1)} %copy-done.10), channel_id=1, source_target_pairs={{0,1},{1,0},{2,3},{3,2},{4,5},{5,4},{6,7},{7,6},{8,9},{9,8},{10,11... | collective-permute-start | bytes 55304 | tf_op jit(solution)/shard_map/ppermute | solution.py:411
  76.3 7.7 %collective-permute-done.3 = bf16[8,256,128]{2,1,0:T(8,128)(2,1)S(1)} collective-permute-done((bf16[8,256,128]{2,1,0:T(8,128)(2,1)S(1)}, bf16[8,256,128]{2,1,0:T(8,128)(2,1)S(1)}, u32[]{:S(2)}, u32[]{:S(2)}) %collective-permute-start.3) | collective-permute-done | bytes 524320 | tf_op jit(solution)/shard_map/ppermute | solution.py:411
  84.0 0.9 constant_dynamic-update-slice_fusion.3
  85.0 4.3 %all-to-all-done.1 = bf16[64,16,128]{2,1,0:T(8,128)(2,1)S(1)} async-done(((bf16[64,16,128]{2,1,0:T(8,128)(2,1)}), bf16[64,16,128]{2,1,0:T(8,128)(2,1)S(1)}, u32[]{:S(2)}, u32[]{:S(2)}) %all-to-all-start.1) | async-done | bytes 262176 | tf_op jit(solution)/shard_map/all_to_all | solution.py:441
  89.4 2.6 %product.1 = bf16[32,56,256]{2,1,0:T(8,128)(2,1)} custom-call(s32[3]{0:T(128)} %pad_add_fusion.place, bf16[72,128]{1,0:T(8,128)(2,1)} %get-tuple-element.49.small, bf16[72,128]{1,0:T(8,128)(2,1)S(1)} %collective-permute-done.8.partner, bf16[1024,128]{1,0:T(8,128)(2,1)} %bitcast.44, bf16[1280,128]{1,0:T(8,128)(2,1)S(1)} %collective-permute-done.near, ...), custom_call_target="tpu_custom_call" | custom-call | tf_op jit(solution)/shard_map/product/pallas_call | solution.py:446
  92.0 6.0 %all-to-all-start.2 = ((bf16[32,56,256]{2,1,0:T(8,128)(2,1)}), bf16[32,56,256]{2,1,0:T(8,128)(2,1)S(1)}, u32[]{:S(2)}, u32[]{:S(2)}) async-start(bf16[32,56,256]{2,1,0:T(8,128)(2,1)} %product.1), calls=%async_computation.2 | async-start | bytes 1835008 | tf_op jit(solution)/shard_map/all_to_all | solution.py:453
  98.0 0.8 constant_dynamic-update-slice_fusion.2.proj
  98.9 2.2 %collective-permute-start.4 = (bf16[16,256,128]{2,1,0:T(8,128)(2,1)}, bf16[16,256,128]{2,1,0:T(8,128)(2,1)S(1)}, u32[]{:S(2)}, u32[]{:S(2)}) collective-permute-start(bf16[16,256,128]{2,1,0:T(8,128)(2,1)} %constant_dynamic-update-slice_fusion.2.proj), channel_id=1, source_target_pairs={{0,1},{1,0},{2,3},{3,2},{4,5},{5,4},{6,7},{7,6},{8,9},{9,8},{10,11... | collective-permute-start | bytes 3145736 | tf_op jit(solution)/shard_map/ppermute | solution.py:411
  101.0 12.8 %all-to-all-done.2.arrived = bf16[32,56,256]{2,1,0:T(8,128)(2,1)S(1)} async-done(((bf16[32,56,256]{2,1,0:T(8,128)(2,1)}), bf16[32,56,256]{2,1,0:T(8,128)(2,1)S(1)}, u32[]{:S(2)}, u32[]{:S(2)}) %all-to-all-start.2) | async-done | bytes 917536 | tf_op jit(solution)/shard_map/all_to_all | solution.py:453
  113.8 0.9 gather_sum.1
  114.7 8.1 %all-to-all-start.3 = ((bf16[16,16,128]{2,1,0:T(8,128)(2,1)}), bf16[16,16,128]{2,1,0:T(8,128)(2,1)S(1)}, u32[]{:S(2)}, u32[]{:S(2)}) async-start(bf16[16,16,128]{2,1,0:T(8,128)(2,1)} %get-tuple-element.50), calls=%async_computation.3 | async-start | bytes 131072 | tf_op jit(solution)/shard_map/all_to_all | solution.py:471
  122.8 1.9 %collective-permute-start.5 = (bf16[16,16,128]{2,1,0:T(8,128)(2,1)S(1)}, bf16[16,16,128]{2,1,0:T(8,128)(2,1)S(1)}, u32[]{:S(2)}, u32[]{:S(2)}) collective-permute-start(bf16[16,16,128]{2,1,0:T(8,128)(2,1)S(1)} %get-tuple-element.59), channel_id=1, source_target_pairs={{0,8},{8,0},{16,24},{24,16},{1,9},{9,1},{17,25},{25,17},{2,10},{10... | collective-permute-start | bytes 196616 | tf_op jit(solution)/shard_map/ppermute | solution.py:411
  124.8 4.1 %collective-permute-start.6 = (bf16[16,16,128]{2,1,0:T(8,128)(2,1)S(1)}, bf16[16,16,128]{2,1,0:T(8,128)(2,1)S(1)}, u32[]{:S(2)}, u32[]{:S(2)}) collective-permute-start(bf16[16,16,128]{2,1,0:T(8,128)(2,1)S(1)} %get-tuple-element.58), channel_id=1, source_target_pairs={{0,16},{8,24},{16,0},{24,8},{1,17},{9,25},{17,1},{25,9},{2,18},{10... | collective-permute-start | bytes 196616 | tf_op jit(solution)/shard_map/ppermute | solution.py:411
  128.9 4.4 %collective-permute-start.7 = (bf16[16,16,128]{2,1,0:T(8,128)(2,1)S(1)}, bf16[16,16,128]{2,1,0:T(8,128)(2,1)S(1)}, u32[]{:S(2)}, u32[]{:S(2)}) collective-permute-start(bf16[16,16,128]{2,1,0:T(8,128)(2,1)S(1)} %get-tuple-element.57), channel_id=1, source_target_pairs={{0,24},{8,16},{16,8},{24,0},{1,25},{9,17},{17,9},{25,1},{2,26},{10... | collective-permute-start | bytes 196616 | tf_op jit(solution)/shard_map/ppermute | solution.py:411
  133.3 3.0 %collective-permute-done.7.three = bf16[16,16,128]{2,1,0:T(8,128)(2,1)S(1)} collective-permute-done((bf16[16,16,128]{2,1,0:T(8,128)(2,1)S(1)}, bf16[16,16,128]{2,1,0:T(8,128)(2,1)S(1)}, u32[]{:S(2)}, u32[]{:S(2)}) %collective-permute-start.7) | collective-permute-done | bytes 65568 | tf_op jit(solution)/shard_map/ppermute | solution.py:411
  136.3 2.9 %token_grad.1 = (bf16[1024,128]{1,0:T(8,128)(2,1)}, bf16[64,2048]{1,0:T(8,128)(2,1)}) custom-call(s32[3]{0:T(128)} %pad_add_fusion.place, bf16[16,256,128]{2,1,0:T(8,128)(2,1)} %constant_dynamic-update-slice_fusion.2.proj, bf16[16,256,128]{2,1,0:T(8,128)(2,1)S(1)} %collective-permute-done.4.proj_other, bf16[16,16,128]{2,1,0:T(8,128)(2,1)S(1)} %get-tuple-element.60.own, ...), custom_call_target="tpu_custom_call" | custom-call | tf_op jit(solution)/shard_map/token_grad/pallas_call | solution.py:475
  139.2 0.7 last_sum.1
  (33 shorter events, 0.4 us)
Async XLA Ops:
  1.7 18.7 %collective-permute-start = (bf16[1280,128]{1,0:T(8,128)(2,1)S(1)}, bf16[1280,128]{1,0:T(8,128)(2,1)S(1)}, u32[]{:S(2)}, u32[]{:S(2)}) collective-permute-start(bf16[1280,128]{1,0:T(8,128)(2,1)S(1)} %get-tuple-element.56), channel_id=1, source_target_pairs={{0,8},{8,0},{16,24},{24,16},{1,9},{9,1},{17,25},{25,17},{2,10},{10... | collective-permute-start | bytes 983048 | tf_op jit(solution)/shard_map/ppermute | solution.py:411
  5.2 42.9 %all-to-all-start = ((bf16[16,64,128]{2,1,0:T(8,128)(2,1)}), bf16[16,64,128]{2,1,0:T(8,128)(2,1)S(1)}, u32[]{:S(2)}, u32[]{:S(2)}) async-start(bf16[16,64,128]{2,1,0:T(8,128)(2,1)} %bitcast.12), calls=%async_computation | async-start | bytes 524288 | tf_op jit(solution)/shard_map/all_to_all | solution.py:424
  20.5 18.7 %collective-permute-start.1 = (bf16[2,1280,128]{2,1,0:T(8,128)(2,1)S(1)}, bf16[2,1280,128]{2,1,0:T(8,128)(2,1)S(1)}, u32[]{:S(2)}, u32[]{:S(2)}) collective-permute-start(bf16[2,1280,128]{2,1,0:T(8,128)(2,1)S(1)} %pad_maximum_fusion), channel_id=1, source_target_pairs={{0,24},{8,16},{16,8},{24,0},{1,25},{9,17},{17,9},{25,1},{2,26},{10... | collective-permute-start | bytes 1966088 | tf_op jit(solution)/shard_map/ppermute | solution.py:411
  24.6 14.6 %copy-start.9 = (bf16[32,1024]{1,0:T(8,128)(2,1)S(1)}, bf16[32,1024]{1,0:T(8,128)(2,1)}, u32[]{:S(2)}) copy-start(bf16[32,1024]{1,0:T(8,128)(2,1)} %param.19) | copy-start | bytes 196612
  39.3 3.6 %copy-start.2 = (bf16[1,64,2048]{2,1,0:T(8,128)(2,1)S(1)}, bf16[1,64,2048]{2,1,0:T(8,128)(2,1)}, u32[]{:S(2)}) copy-start(bf16[1,64,2048]{2,1,0:T(8,128)(2,1)} %param.11) | copy-start | bytes 786436
  39.3 3.6 %copy-start.3 = (bf16[1,64,2048]{2,1,0:T(8,128)(2,1)S(1)}, bf16[1,64,2048]{2,1,0:T(8,128)(2,1)}, u32[]{:S(2)}) copy-start(bf16[1,64,2048]{2,1,0:T(8,128)(2,1)} %param.12) | copy-start | bytes 786436
  39.3 30.4 %collective-permute-start.2 = (bf16[4,256,128]{2,1,0:T(8,128)(2,1)S(1)}, bf16[4,256,128]{2,1,0:T(8,128)(2,1)S(1)}, u32[]{:S(2)}, u32[]{:S(2)}) collective-permute-start(bf16[4,256,128]{2,1,0:T(8,128)(2,1)S(1)} %pad_maximum_fusion.2), channel_id=1, source_target_pairs={{0,2},{2,0},{4,6},{6,4},{1,3},{3,1},{5,7},{7,5},{8,10},{10,8},{12,... | collective-permute-start | bytes 786440 | tf_op jit(solution)/shard_map/ppermute | solution.py:411
  48.1 7.4 %copy-start = (bf16[16,64,128]{2,1,0:T(8,128)(2,1)}, bf16[16,64,128]{2,1,0:T(8,128)(2,1)S(1)}, u32[]{:S(2)}) copy-start(bf16[16,64,128]{2,1,0:T(8,128)(2,1)S(1)} %all-to-all-done.cot) | copy-start | bytes 786436
  48.1 1.1 copy-start.1
  49.2 0.9 copy-start.4
  50.2 0.9 copy-start.5
  51.1 0.9 copy-start.6
  55.5 33.9 %all-to-all-start.1 = ((bf16[64,16,128]{2,1,0:T(8,128)(2,1)}), bf16[64,16,128]{2,1,0:T(8,128)(2,1)S(1)}, u32[]{:S(2)}, u32[]{:S(2)}) async-start(bf16[64,16,128]{2,1,0:T(8,128)(2,1)} %bitcast.45), calls=%async_computation.1 | async-start | bytes 524288 | tf_op jit(solution)/shard_map/all_to_all | solution.py:441
  69.8 4.6 %copy-start.10 = (bf16[72,128]{1,0:T(8,128)(2,1)S(1)}, bf16[72,128]{1,0:T(8,128)(2,1)}, u32[]{:S(2)}) copy-start(bf16[72,128]{1,0:T(8,128)(2,1)} %get-tuple-element.49.small) | copy-start | bytes 55300
  69.8 14.2 %collective-permute-start.3 = (bf16[8,256,128]{2,1,0:T(8,128)(2,1)S(1)}, bf16[8,256,128]{2,1,0:T(8,128)(2,1)S(1)}, u32[]{:S(2)}, u32[]{:S(2)}) collective-permute-start(bf16[8,256,128]{2,1,0:T(8,128)(2,1)S(1)} %constant_dynamic-update-slice_fusion), channel_id=1, source_target_pairs={{0,6},{2,4},{4,2},{6,0},{1,7},{3,5},{5,3},{7,1},{8,14},{10,12},{12... | collective-permute-start | bytes 1572872 | tf_op jit(solution)/shard_map/ppermute | solution.py:411
  74.4 10.7 %collective-permute-start.8 = (bf16[72,128]{1,0:T(8,128)(2,1)S(1)}, bf16[72,128]{1,0:T(8,128)(2,1)S(1)}, u32[]{:S(2)}, u32[]{:S(2)}) collective-permute-start(bf16[72,128]{1,0:T(8,128)(2,1)S(1)} %copy-done.10), channel_id=1, source_target_pairs={{0,1},{1,0},{2,3},{3,2},{4,5},{5,4},{6,7},{7,6},{8,9},{9,8},{10,11... | collective-permute-start | bytes 55304 | tf_op jit(solution)/shard_map/ppermute | solution.py:411
  84.0 1.0 copy-start.7
  92.0 6.0 %copy-start.8 = (bf16[8,256,128]{2,1,0:T(8,128)(2,1)S(1)}, bf16[8,256,128]{2,1,0:T(8,128)(2,1)}, u32[]{:S(2)}) copy-start(bf16[8,256,128]{2,1,0:T(8,128)(2,1)} %copy-done.7) | copy-start | bytes 1572868
  92.0 21.9 %all-to-all-start.2 = ((bf16[32,56,256]{2,1,0:T(8,128)(2,1)}), bf16[32,56,256]{2,1,0:T(8,128)(2,1)S(1)}, u32[]{:S(2)}, u32[]{:S(2)}) async-start(bf16[32,56,256]{2,1,0:T(8,128)(2,1)} %product.1), calls=%async_computation.2 | async-start | bytes 1835008 | tf_op jit(solution)/shard_map/all_to_all | solution.py:453
  98.9 37.4 %collective-permute-start.4 = (bf16[16,256,128]{2,1,0:T(8,128)(2,1)}, bf16[16,256,128]{2,1,0:T(8,128)(2,1)S(1)}, u32[]{:S(2)}, u32[]{:S(2)}) collective-permute-start(bf16[16,256,128]{2,1,0:T(8,128)(2,1)} %constant_dynamic-update-slice_fusion.2.proj), channel_id=1, source_target_pairs={{0,1},{1,0},{2,3},{3,2},{4,5},{5,4},{6,7},{7,6},{8,9},{9,8},{10,11... | collective-permute-start | bytes 3145736 | tf_op jit(solution)/shard_map/ppermute | solution.py:411
  114.7 24.5 %all-to-all-start.3 = ((bf16[16,16,128]{2,1,0:T(8,128)(2,1)}), bf16[16,16,128]{2,1,0:T(8,128)(2,1)S(1)}, u32[]{:S(2)}, u32[]{:S(2)}) async-start(bf16[16,16,128]{2,1,0:T(8,128)(2,1)} %get-tuple-element.50), calls=%async_computation.3 | async-start | bytes 131072 | tf_op jit(solution)/shard_map/all_to_all | solution.py:471
  122.8 10.4 %collective-permute-start.5 = (bf16[16,16,128]{2,1,0:T(8,128)(2,1)S(1)}, bf16[16,16,128]{2,1,0:T(8,128)(2,1)S(1)}, u32[]{:S(2)}, u32[]{:S(2)}) collective-permute-start(bf16[16,16,128]{2,1,0:T(8,128)(2,1)S(1)} %get-tuple-element.59), channel_id=1, source_target_pairs={{0,8},{8,0},{16,24},{24,16},{1,9},{9,1},{17,25},{25,17},{2,10},{10... | collective-permute-start | bytes 196616 | tf_op jit(solution)/shard_map/ppermute | solution.py:411
  124.8 8.5 %collective-permute-start.6 = (bf16[16,16,128]{2,1,0:T(8,128)(2,1)S(1)}, bf16[16,16,128]{2,1,0:T(8,128)(2,1)S(1)}, u32[]{:S(2)}, u32[]{:S(2)}) collective-permute-start(bf16[16,16,128]{2,1,0:T(8,128)(2,1)S(1)} %get-tuple-element.58), channel_id=1, source_target_pairs={{0,16},{8,24},{16,0},{24,8},{1,17},{9,25},{17,1},{25,9},{2,18},{10... | collective-permute-start | bytes 196616 | tf_op jit(solution)/shard_map/ppermute | solution.py:411
  128.9 7.4 %collective-permute-start.7 = (bf16[16,16,128]{2,1,0:T(8,128)(2,1)S(1)}, bf16[16,16,128]{2,1,0:T(8,128)(2,1)S(1)}, u32[]{:S(2)}, u32[]{:S(2)}) collective-permute-start(bf16[16,16,128]{2,1,0:T(8,128)(2,1)S(1)} %get-tuple-element.57), channel_id=1, source_target_pairs={{0,24},{8,16},{16,8},{24,0},{1,25},{9,17},{17,9},{25,1},{2,26},{10... | collective-permute-start | bytes 196616 | tf_op jit(solution)/shard_map/ppermute | solution.py:411

commit v5 on v4

--- a/solution.py
+++ b/solution.py
@@ -384,25 +384,25 @@
     out[16:32, :] = pltpu.roll(total, GROUP, 1)[:, 0:GROUP]
 
 
-def token_grad_kernel(place, proj, proj_other, own, one, two, three, cot, g1, out, gate_o, tokens_s):
+def token_grad_kernel(place, close, away, close_other, away_other, own, one, two, three, cot, g1, out, gate_o, tokens_s):
     for j in range(cot.shape[0]):
         at = slice(j * SPAN, (j + 1) * SPAN)
         gate_o[:, at] = (cot[j].astype(f32) * g1[:, at].astype(f32)).astype(bf16)
     for n, piece in enumerate((own, one, two, three)):
         tokens_s[:, place[0] ^ n] = piece[...]
     tokens = tokens_s[...].reshape(1024, SPAN)
-    for k, half in enumerate((proj, proj_other)):
-        tiles = half[...].reshape(16, 4, 8, 8, SPAN)
+    for part, half in enumerate((close, away, close_other, away_other)):
+        tiles = half[...].reshape(8, 4, 8, 8, SPAN)
         result = None
         for n in range(8):
             term = jnp.dot(
-                tiles[:, :, n].reshape(512, SPAN), tokens[n * SPAN : (n + 1) * SPAN], preferred_element_type=f32
+                tiles[:, :, n].reshape(256, SPAN), tokens[n * SPAN : (n + 1) * SPAN], preferred_element_type=f32
             )
             result = term if result is None else result + term
         result = result.astype(bf16)
-        for n in range(16):
-            y, x = place[0] ^ NEAREST[n % 4], place[1] ^ NEAREST[n // 4]
-            row = ((y * 4 + x) * 2 + (place[2] ^ k)) * 32
+        for n in range(8):
+            y, x = place[0] ^ NEAREST[n % 4], place[1] ^ NEAREST[n // 4 + 2 * (part % 2)]
+            row = ((y * 4 + x) * 2 + (place[2] ^ (part // 2))) * 32
             out[pl.ds(pl.multiple_of(row, 32), 32), :] = result[32 * n : 32 * n + 32]
 
 
@@ -434,8 +434,9 @@
     near = exchanged(packed, "y", 1)
     far = exchanged(jnp.stack([packed, near]), "y", 3)
     held = jnp.stack([rows, near[1024:], far[0, 1024:], far[1, 1024:]])
-    proj = joined(joined(held, "x", 1), "x", 3)
-    proj_other = exchanged(proj, "core", 1)
+    close = joined(held, "x", 1)
+    away = exchanged(close, "x", 3)
+    halves_here = (close, away, exchanged(close, "core", 1), exchanged(away, "core", 1))
     gb, small = backward_part(here_in_vmem(cot), saved)
     partner = exchanged(small, "core", 1)
     grads = lax.all_to_all(gb.reshape(64, 16, SPAN), ("sp", "y"), 0, 0, tiled=True)
@@ -474,12 +475,12 @@
     )(here_in_vmem(last))
     grad_normed, grad_gate = pl.pallas_call(
         token_grad_kernel,
-        in_specs=[smem] + [VMEM] * 8,
+        in_specs=[smem] + [VMEM] * 10,
         out_specs=[VMEM] * 2,
         out_shape=[jax.ShapeDtypeStruct((1024, SPAN), bf16), jax.ShapeDtypeStruct(g1.shape, bf16)],
         scratch_shapes=[pltpu.VMEM((16, 4, 16, SPAN), bf16)],
         name="token_grad",
-    )(place, proj, here_in_vmem(proj_other), *map(here_in_vmem, (own_part, *others)), cot, g1)
+    )(place, *halves_here[:2], *map(here_in_vmem, halves_here[2:]), *map(here_in_vmem, (own_part, *others)), cot, g1)
     return (
         grad_normed[None],
         grad_gate[None],

time: 141 us -> 139 us (0.986)
  waiting for transfers between devices: 42.5 us -> 44.4 us
  local copies, waits for them, and re-layouts: 5.96 us -> 4.12 us
    all_to_all x1, waiting for transfers between devices: 12.8 us -> 0.01 us  [steps(): arrived = lax.all_to_all(pieces, DP, 0, 0, tiled=True)]
    ppermute x9 -> x10, waiting for transfers between devices: 25.3 us -> 32.8 us  [exchanged(): return lax.ppermute(array, axis, [(n, n ^ bit) for n in range(size)])]
    all_to_all x1, waiting for transfers between devices: 4.32 us -> 11.5 us  [steps(): lax.all_to_all(gb.reshape(64, 16, SPAN), ('sp', 'y'), 0, 0, tiled=True)]
    all_to_all x1, starting transfers between devices: 8.09 us -> 4.66 us  [steps(): last = lax.all_to_all(sums, 'sp', 0, 0, tiled=True)]
    ppermute x9 -> x10, starting transfers between devices: 29.6 us -> 33 us  [exchanged(): return lax.ppermute(array, axis, [(n, n ^ bit) for n in range(size)])]
    all_to_all x1, starting transfers between devices: 14.2 us -> 12.6 us  [steps(): lax.all_to_all(gb.reshape(64, 16, SPAN), ('sp', 'y'), 0, 0, tiled=True)]
    unnamed x24 -> x25, local copies, waits for them, and re-layouts: 5.03 us -> 4.03 us
  transfers between devices with their start and end apart: 13 -> 14, of which waited for: 5 -> 6; matrix products, arithmetic and copies ran while one was open for 2% -> 1% of each run, Pallas kernels for 9% -> 9%
where the time goes in v5:
time: 139 us; the launch traced here: 138 us
  starting transfers between devices  71.9 us (52%)
  waiting for transfers between devices  44.4 us (32%)
  Pallas kernels  15.6 us (11%)
  local copies, waits for them, and re-layouts  4.12 us (3%)
    ppermute x10, starting transfers between devices, exchanged(): return lax.ppermute(array, axis, [(n, n ^ bit) for n in range(size)])  33 us
    ppermute x10, waiting for transfers between devices, exchanged(): return lax.ppermute(array, axis, [(n, n ^ bit) for n in range(size)])  32.8 us
    all_to_all x1, starting transfers between devices, steps(): lax.all_to_all(cotangent[0].reshape(spans, GROUP, SPAN), 'sp', 0, 0, tile...  15.4 us
    all_to_all x1, starting transfers between devices, steps(): lax.all_to_all(gb.reshape(64, 16, SPAN), ('sp', 'y'), 0, 0, tiled=True)  12.6 us
    all_to_all x1, waiting for transfers between devices, steps(): lax.all_to_all(gb.reshape(64, 16, SPAN), ('sp', 'y'), 0, 0, tiled=True)  11.5 us
    all_to_all x1, starting transfers between devices, steps(): arrived = lax.all_to_all(pieces, DP, 0, 0, tiled=True)  6.21 us
    pallas_call x1, Pallas kernels, forward_part(): pl.pallas_call(forward_kernel, in_specs=[VMEM] * 7, out_specs=[ANY] * 9 +...  5.13 us
    all_to_all x1, starting transfers between devices, steps(): last = lax.all_to_all(sums, 'sp', 0, 0, tiled=True)  4.66 us
  transfers between devices with their start and end apart: 14, of which 6 were waited for; matrix products, arithmetic and copies ran while one was open for 1% of the time, Pallas kernels for 9%

profile of v5, /device:TPU:32, one launch (start us, length us, event | category | flops | bytes accessed | tf_op | source)
XLA Modules:
  0.0 137.7 jit_solution(13858246296141549225)
XLA Ops:
  0.7 15.4 %all-to-all-start = ((bf16[16,64,128]{2,1,0:T(8,128)(2,1)}), bf16[16,64,128]{2,1,0:T(8,128)(2,1)S(1)}, u32[]{:S(2)}, u32[]{:S(2)}) async-start(bf16[16,64,128]{2,1,0:T(8,128)(2,1)} %bitcast.45), calls=%async_computation | async-start | bytes 524288 | tf_op jit(solution)/shard_map/all_to_all | solution.py:424
  16.1 3.5 %collective-permute-start = (bf16[1280,128]{1,0:T(8,128)(2,1)S(1)}, bf16[1280,128]{1,0:T(8,128)(2,1)S(1)}, u32[]{:S(2)}, u32[]{:S(2)}) collective-permute-start(bf16[1280,128]{1,0:T(8,128)(2,1)S(1)} %get-tuple-element.52), channel_id=1, source_target_pairs={{0,8},{8,0},{16,24},{24,16},{1,9},{9,1},{17,25},{25,17},{2,10},{10... | collective-permute-start | bytes 983048 | tf_op jit(solution)/shard_map/ppermute | solution.py:411
  19.6 7.3 %collective-permute-done.near = bf16[1280,128]{1,0:T(8,128)(2,1)S(1)} collective-permute-done((bf16[1280,128]{1,0:T(8,128)(2,1)S(1)}, bf16[1280,128]{1,0:T(8,128)(2,1)S(1)}, u32[]{:S(2)}, u32[]{:S(2)}) %collective-permute-start) | collective-permute-done | bytes 327712 | tf_op jit(solution)/shard_map/ppermute | solution.py:411
  26.9 0.1 pad_maximum_fusion
  26.9 5.1 %collective-permute-start.1 = (bf16[2,1280,128]{2,1,0:T(8,128)(2,1)S(1)}, bf16[2,1280,128]{2,1,0:T(8,128)(2,1)S(1)}, u32[]{:S(2)}, u32[]{:S(2)}) collective-permute-start(bf16[2,1280,128]{2,1,0:T(8,128)(2,1)S(1)} %pad_maximum_fusion), channel_id=1, source_target_pairs={{0,24},{8,16},{16,8},{24,0},{1,25},{9,17},{17,9},{25,1},{2,26},{10... | collective-permute-start | bytes 1966088 | tf_op jit(solution)/shard_map/ppermute | solution.py:411
  32.0 5.1 %forward_part.1 = (f32[1024,128]{1,0:T(8,128)}, bf16[1024,128]{1,0:T(8,128)(2,1)}, bf16[1024,128]{1,0:T(8,128)(2,1)}, bf16[1024,128]{1,0:T(8,128)(2,1)}, bf16[10...) custom-call(bf16[64,2048]{1,0:T(8,128)(2,1)S(1)} %bitcast.41, ...), custom_call_target="tpu_custom_call" | custom-call | tf_op jit(solution)/shard_map/forward_part/pallas_call | solution.py:305
  37.2 1.1 copy-done.1
  38.3 0.9 copy-done.4
  39.3 0.9 copy-done.5
  40.2 0.9 copy-done.6
  41.2 3.4 %backward_part.1 = (bf16[16,64,128]{2,1,0:T(8,128)(2,1)}, bf16[72,128]{1,0:T(8,128)(2,1)}) custom-call(bf16[16,64,128]{2,1,0:T(8,128)(2,1)S(1)} %all-to-all-done.cot, f32[1024,128]{1,0:T(8,128)S(1)} %copy-done.1, bf16[1024,128]{1,0:T(8,128)(2,1)S(1)} %copy-done.4, bf16[1024,128]{1,0:T(8,128)(2,1)S(1)} %copy-done.5, bf16[1024,128]{1,0:T(8,128)(2,1)S(1)} %copy-done.6, ...), custom_call_target="tpu_custom_call" | custom-call | tf_op jit(solution)/shard_map/backward_part/pallas_call | solution.py:320
  44.6 12.6 %all-to-all-start.1 = ((bf16[64,16,128]{2,1,0:T(8,128)(2,1)}), bf16[64,16,128]{2,1,0:T(8,128)(2,1)S(1)}, u32[]{:S(2)}, u32[]{:S(2)}) async-start(bf16[64,16,128]{2,1,0:T(8,128)(2,1)} %bitcast.46), calls=%async_computation.1 | async-start | bytes 524288 | tf_op jit(solution)/shard_map/all_to_all | solution.py:442
  57.3 3.4 %collective-permute-start.2 = (bf16[4,256,128]{2,1,0:T(8,128)(2,1)S(1)}, bf16[4,256,128]{2,1,0:T(8,128)(2,1)S(1)}, u32[]{:S(2)}, u32[]{:S(2)}) collective-permute-start(bf16[4,256,128]{2,1,0:T(8,128)(2,1)S(1)} %pad_maximum_fusion.2), channel_id=1, source_target_pairs={{0,2},{2,0},{4,6},{6,4},{1,3},{3,1},{5,7},{7,5},{8,10},{10,8},{12,... | collective-permute-start | bytes 786440 | tf_op jit(solution)/shard_map/ppermute | solution.py:411
  60.8 0.6 pad_add_fusion.place
  61.4 1.9 %collective-permute-start.9 = (bf16[72,128]{1,0:T(8,128)(2,1)S(1)}, bf16[72,128]{1,0:T(8,128)(2,1)S(1)}, u32[]{:S(2)}, u32[]{:S(2)}) collective-permute-start(bf16[72,128]{1,0:T(8,128)(2,1)S(1)} %copy-done.11), channel_id=1, source_target_pairs={{0,1},{1,0},{2,3},{3,2},{4,5},{5,4},{6,7},{7,6},{8,9},{9,8},{10,11... | collective-permute-start | bytes 55304 | tf_op jit(solution)/shard_map/ppermute | solution.py:411
  63.3 2.3 %collective-permute-done.2 = bf16[4,256,128]{2,1,0:T(8,128)(2,1)S(1)} collective-permute-done((bf16[4,256,128]{2,1,0:T(8,128)(2,1)S(1)}, bf16[4,256,128]{2,1,0:T(8,128)(2,1)S(1)}, u32[]{:S(2)}, u32[]{:S(2)}) %collective-permute-start.2) | collective-permute-done | bytes 262176 | tf_op jit(solution)/shard_map/ppermute | solution.py:411
  65.6 11.5 %all-to-all-done.1 = bf16[64,16,128]{2,1,0:T(8,128)(2,1)S(1)} async-done(((bf16[64,16,128]{2,1,0:T(8,128)(2,1)}), bf16[64,16,128]{2,1,0:T(8,128)(2,1)S(1)}, u32[]{:S(2)}, u32[]{:S(2)}) %all-to-all-start.1) | async-done | bytes 262176 | tf_op jit(solution)/shard_map/all_to_all | solution.py:442
  77.2 2.6 %product.1 = bf16[32,56,256]{2,1,0:T(8,128)(2,1)} custom-call(s32[3]{0:T(128)} %pad_add_fusion.place, bf16[72,128]{1,0:T(8,128)(2,1)} %get-tuple-element.45.small, bf16[72,128]{1,0:T(8,128)(2,1)S(1)} %collective-permute-done.9.partner, bf16[1024,128]{1,0:T(8,128)(2,1)} %bitcast.43, bf16[1280,128]{1,0:T(8,128)(2,1)S(1)} %collective-permute-done.near, ...), custom_call_target="tpu_custom_call" | custom-call | tf_op jit(solution)/shard_map/product/pallas_call | solution.py:447
  79.8 6.2 %all-to-all-start.2 = ((bf16[32,56,256]{2,1,0:T(8,128)(2,1)}), bf16[32,56,256]{2,1,0:T(8,128)(2,1)S(1)}, u32[]{:S(2)}, u32[]{:S(2)}) async-start(bf16[32,56,256]{2,1,0:T(8,128)(2,1)} %product.1), calls=%async_computation.2 | async-start | bytes 1835008 | tf_op jit(solution)/shard_map/all_to_all | solution.py:454
  86.1 4.9 %collective-permute-start.3 = (bf16[8,256,128]{2,1,0:T(8,128)(2,1)S(1)}, bf16[8,256,128]{2,1,0:T(8,128)(2,1)S(1)}, u32[]{:S(2)}, u32[]{:S(2)}) collective-permute-start(bf16[8,256,128]{2,1,0:T(8,128)(2,1)S(1)} %constant_dynamic-update-slice_fusion.close), channel_id=1, source_target_pairs={{0,6},{2,4},{4,2},{6,0},{1,7},{3,5},{5,3},{7,1},{8,14},{10,12},{12... | collective-permute-start | bytes 1572872 | tf_op jit(solution)/shard_map/ppermute | solution.py:411
  91.0 1.9 %collective-permute-start.4 = (bf16[8,256,128]{2,1,0:T(8,128)(2,1)S(1)}, bf16[8,256,128]{2,1,0:T(8,128)(2,1)S(1)}, u32[]{:S(2)}, u32[]{:S(2)}) collective-permute-start(bf16[8,256,128]{2,1,0:T(8,128)(2,1)S(1)} %constant_dynamic-update-slice_fusion.close), channel_id=1, source_target_pairs={{0,1},{1,0},{2,3},{3,2},{4,5},{5,4},{6,7},{7,6},{8,9},{9,8},{10,11... | collective-permute-start | bytes 1572872 | tf_op jit(solution)/shard_map/ppermute | solution.py:411
  92.9 18.2 %collective-permute-done.3.away = bf16[8,256,128]{2,1,0:T(8,128)(2,1)S(1)} collective-permute-done((bf16[8,256,128]{2,1,0:T(8,128)(2,1)S(1)}, bf16[8,256,128]{2,1,0:T(8,128)(2,1)S(1)}, u32[]{:S(2)}, u32[]{:S(2)}) %collective-permute-start.3) | collective-permute-done | bytes 524320 | tf_op jit(solution)/shard_map/ppermute | solution.py:411
  111.2 1.9 %collective-permute-start.5 = (bf16[8,256,128]{2,1,0:T(8,128)(2,1)S(1)}, bf16[8,256,128]{2,1,0:T(8,128)(2,1)S(1)}, u32[]{:S(2)}, u32[]{:S(2)}) collective-permute-start(bf16[8,256,128]{2,1,0:T(8,128)(2,1)S(1)} %collective-permute-done.3.away), channel_id=1, source_target_pairs={{0,1},{1,0},{2,3},{3,2},{4,5},{5,4},{6,7},{7,6},{8,9},{9,8},{10,11... | collective-permute-start | bytes 1572872 | tf_op jit(solution)/shard_map/ppermute | solution.py:411
  113.1 0.9 gather_sum.1
  114.0 4.7 %all-to-all-start.3 = ((bf16[16,16,128]{2,1,0:T(8,128)(2,1)}), bf16[16,16,128]{2,1,0:T(8,128)(2,1)S(1)}, u32[]{:S(2)}, u32[]{:S(2)}) async-start(bf16[16,16,128]{2,1,0:T(8,128)(2,1)} %get-tuple-element.46), calls=%async_computation.3 | async-start | bytes 131072 | tf_op jit(solution)/shard_map/all_to_all | solution.py:472
  118.7 3.4 %collective-permute-start.6 = (bf16[16,16,128]{2,1,0:T(8,128)(2,1)S(1)}, bf16[16,16,128]{2,1,0:T(8,128)(2,1)S(1)}, u32[]{:S(2)}, u32[]{:S(2)}) collective-permute-start(bf16[16,16,128]{2,1,0:T(8,128)(2,1)S(1)} %get-tuple-element.55), channel_id=1, source_target_pairs={{0,8},{8,0},{16,24},{24,16},{1,9},{9,1},{17,25},{25,17},{2,10},{10... | collective-permute-start | bytes 196616 | tf_op jit(solution)/shard_map/ppermute | solution.py:411
  122.1 4.7 %collective-permute-start.7 = (bf16[16,16,128]{2,1,0:T(8,128)(2,1)S(1)}, bf16[16,16,128]{2,1,0:T(8,128)(2,1)S(1)}, u32[]{:S(2)}, u32[]{:S(2)}) collective-permute-start(bf16[16,16,128]{2,1,0:T(8,128)(2,1)S(1)} %get-tuple-element.54), channel_id=1, source_target_pairs={{0,16},{8,24},{16,0},{24,8},{1,17},{9,25},{17,1},{25,9},{2,18},{10... | collective-permute-start | bytes 196616 | tf_op jit(solution)/shard_map/ppermute | solution.py:411
  126.7 2.4 %collective-permute-start.8 = (bf16[16,16,128]{2,1,0:T(8,128)(2,1)S(1)}, bf16[16,16,128]{2,1,0:T(8,128)(2,1)S(1)}, u32[]{:S(2)}, u32[]{:S(2)}) collective-permute-start(bf16[16,16,128]{2,1,0:T(8,128)(2,1)S(1)} %get-tuple-element.53), channel_id=1, source_target_pairs={{0,24},{8,16},{16,8},{24,0},{1,25},{9,17},{17,9},{25,1},{2,26},{10... | collective-permute-start | bytes 196616 | tf_op jit(solution)/shard_map/ppermute | solution.py:411
  129.1 0.6 collective-permute-done.7.two
  129.7 4.4 %collective-permute-done.8.three = bf16[16,16,128]{2,1,0:T(8,128)(2,1)S(1)} collective-permute-done((bf16[16,16,128]{2,1,0:T(8,128)(2,1)S(1)}, bf16[16,16,128]{2,1,0:T(8,128)(2,1)S(1)}, u32[]{:S(2)}, u32[]{:S(2)}) %collective-permute-start.8) | collective-permute-done | bytes 65568 | tf_op jit(solution)/shard_map/ppermute | solution.py:411
  134.1 2.9 %token_grad.1 = (bf16[1024,128]{1,0:T(8,128)(2,1)}, bf16[64,2048]{1,0:T(8,128)(2,1)}) custom-call(s32[3]{0:T(128)} %pad_add_fusion.place, bf16[8,256,128]{2,1,0:T(8,128)(2,1)} %copy-done.7, bf16[8,256,128]{2,1,0:T(8,128)(2,1)} %copy-done.9, bf16[8,256,128]{2,1,0:T(8,128)(2,1)S(1)} %collective-permute-done.4.close_other, ...), custom_call_target="tpu_custom_call" | custom-call | tf_op jit(solution)/shard_map/token_grad/pallas_call | solution.py:476
  137.0 0.7 last_sum.1
  (35 shorter events, 0.2 us)
Async XLA Ops:
  0.6 15.4 %copy-start.8 = (bf16[1,1024,128]{2,1,0:T(8,128)(2,1)S(1)}, bf16[1,1024,128]{2,1,0:T(8,128)(2,1)}, u32[]{:S(2)}) copy-start(bf16[1,1024,128]{2,1,0:T(8,128)(2,1)} %param.10) | copy-start | bytes 786436
  0.6 15.4 %copy-start.10 = (bf16[32,1024]{1,0:T(8,128)(2,1)S(1)}, bf16[32,1024]{1,0:T(8,128)(2,1)}, u32[]{:S(2)}) copy-start(bf16[32,1024]{1,0:T(8,128)(2,1)} %param.19) | copy-start | bytes 196612
  0.7 36.5 %all-to-all-start = ((bf16[16,64,128]{2,1,0:T(8,128)(2,1)}), bf16[16,64,128]{2,1,0:T(8,128)(2,1)S(1)}, u32[]{:S(2)}, u32[]{:S(2)}) async-start(bf16[16,64,128]{2,1,0:T(8,128)(2,1)} %bitcast.45), calls=%async_computation | async-start | bytes 524288 | tf_op jit(solution)/shard_map/all_to_all | solution.py:424
  16.1 10.8 %collective-permute-start = (bf16[1280,128]{1,0:T(8,128)(2,1)S(1)}, bf16[1280,128]{1,0:T(8,128)(2,1)S(1)}, u32[]{:S(2)}, u32[]{:S(2)}) collective-permute-start(bf16[1280,128]{1,0:T(8,128)(2,1)S(1)} %get-tuple-element.52), channel_id=1, source_target_pairs={{0,8},{8,0},{16,24},{24,16},{1,9},{9,1},{17,25},{25,17},{2,10},{10... | collective-permute-start | bytes 983048 | tf_op jit(solution)/shard_map/ppermute | solution.py:411
  26.9 5.1 %copy-start.2 = (bf16[1,64,2048]{2,1,0:T(8,128)(2,1)S(1)}, bf16[1,64,2048]{2,1,0:T(8,128)(2,1)}, u32[]{:S(2)}) copy-start(bf16[1,64,2048]{2,1,0:T(8,128)(2,1)} %param.11) | copy-start | bytes 786436
  26.9 5.1 %copy-start.3 = (bf16[1,64,2048]{2,1,0:T(8,128)(2,1)S(1)}, bf16[1,64,2048]{2,1,0:T(8,128)(2,1)}, u32[]{:S(2)}) copy-start(bf16[1,64,2048]{2,1,0:T(8,128)(2,1)} %param.12) | copy-start | bytes 786436
  26.9 30.3 %collective-permute-start.1 = (bf16[2,1280,128]{2,1,0:T(8,128)(2,1)S(1)}, bf16[2,1280,128]{2,1,0:T(8,128)(2,1)S(1)}, u32[]{:S(2)}, u32[]{:S(2)}) collective-permute-start(bf16[2,1280,128]{2,1,0:T(8,128)(2,1)S(1)} %pad_maximum_fusion), channel_id=1, source_target_pairs={{0,24},{8,16},{16,8},{24,0},{1,25},{9,17},{17,9},{25,1},{2,26},{10... | collective-permute-start | bytes 1966088 | tf_op jit(solution)/shard_map/ppermute | solution.py:411
  37.2 7.4 %copy-start = (bf16[16,64,128]{2,1,0:T(8,128)(2,1)}, bf16[16,64,128]{2,1,0:T(8,128)(2,1)S(1)}, u32[]{:S(2)}) copy-start(bf16[16,64,128]{2,1,0:T(8,128)(2,1)S(1)} %all-to-all-done.cot) | copy-start | bytes 786436
  37.2 1.1 copy-start.1
  38.3 0.9 copy-start.4
  39.3 0.9 copy-start.5
  40.2 0.9 copy-start.6
  44.6 32.6 %all-to-all-start.1 = ((bf16[64,16,128]{2,1,0:T(8,128)(2,1)}), bf16[64,16,128]{2,1,0:T(8,128)(2,1)S(1)}, u32[]{:S(2)}, u32[]{:S(2)}) async-start(bf16[64,16,128]{2,1,0:T(8,128)(2,1)} %bitcast.46), calls=%async_computation.1 | async-start | bytes 524288 | tf_op jit(solution)/shard_map/all_to_all | solution.py:442
  57.3 4.0 %copy-start.11 = (bf16[72,128]{1,0:T(8,128)(2,1)S(1)}, bf16[72,128]{1,0:T(8,128)(2,1)}, u32[]{:S(2)}) copy-start(bf16[72,128]{1,0:T(8,128)(2,1)} %get-tuple-element.45.small) | copy-start | bytes 55300
  57.3 8.3 %collective-permute-start.2 = (bf16[4,256,128]{2,1,0:T(8,128)(2,1)S(1)}, bf16[4,256,128]{2,1,0:T(8,128)(2,1)S(1)}, u32[]{:S(2)}, u32[]{:S(2)}) collective-permute-start(bf16[4,256,128]{2,1,0:T(8,128)(2,1)S(1)} %pad_maximum_fusion.2), channel_id=1, source_target_pairs={{0,2},{2,0},{4,6},{6,4},{1,3},{3,1},{5,7},{7,5},{8,10},{10,8},{12,... | collective-permute-start | bytes 786440 | tf_op jit(solution)/shard_map/ppermute | solution.py:411
  61.4 4.3 %collective-permute-start.9 = (bf16[72,128]{1,0:T(8,128)(2,1)S(1)}, bf16[72,128]{1,0:T(8,128)(2,1)S(1)}, u32[]{:S(2)}, u32[]{:S(2)}) collective-permute-start(bf16[72,128]{1,0:T(8,128)(2,1)S(1)} %copy-done.11), channel_id=1, source_target_pairs={{0,1},{1,0},{2,3},{3,2},{4,5},{5,4},{6,7},{7,6},{8,9},{9,8},{10,11... | collective-permute-start | bytes 55304 | tf_op jit(solution)/shard_map/ppermute | solution.py:411
  79.8 33.3 %all-to-all-start.2 = ((bf16[32,56,256]{2,1,0:T(8,128)(2,1)}), bf16[32,56,256]{2,1,0:T(8,128)(2,1)S(1)}, u32[]{:S(2)}, u32[]{:S(2)}) async-start(bf16[32,56,256]{2,1,0:T(8,128)(2,1)} %product.1), calls=%async_computation.2 | async-start | bytes 1835008 | tf_op jit(solution)/shard_map/all_to_all | solution.py:454
  86.1 27.9 %copy-start.7 = (bf16[8,256,128]{2,1,0:T(8,128)(2,1)}, bf16[8,256,128]{2,1,0:T(8,128)(2,1)S(1)}, u32[]{:S(2)}) copy-start(bf16[8,256,128]{2,1,0:T(8,128)(2,1)S(1)} %constant_dynamic-update-slice_fusion.close) | copy-start | bytes 1572868
  86.1 25.1 %collective-permute-start.3 = (bf16[8,256,128]{2,1,0:T(8,128)(2,1)S(1)}, bf16[8,256,128]{2,1,0:T(8,128)(2,1)S(1)}, u32[]{:S(2)}, u32[]{:S(2)}) collective-permute-start(bf16[8,256,128]{2,1,0:T(8,128)(2,1)S(1)} %constant_dynamic-update-slice_fusion.close), channel_id=1, source_target_pairs={{0,6},{2,4},{4,2},{6,0},{1,7},{3,5},{5,3},{7,1},{8,14},{10,12},{12... | collective-permute-start | bytes 1572872 | tf_op jit(solution)/shard_map/ppermute | solution.py:411
  91.0 38.1 %collective-permute-start.4 = (bf16[8,256,128]{2,1,0:T(8,128)(2,1)S(1)}, bf16[8,256,128]{2,1,0:T(8,128)(2,1)S(1)}, u32[]{:S(2)}, u32[]{:S(2)}) collective-permute-start(bf16[8,256,128]{2,1,0:T(8,128)(2,1)S(1)} %constant_dynamic-update-slice_fusion.close), channel_id=1, source_target_pairs={{0,1},{1,0},{2,3},{3,2},{4,5},{5,4},{6,7},{7,6},{8,9},{9,8},{10,11... | collective-permute-start | bytes 1572872 | tf_op jit(solution)/shard_map/ppermute | solution.py:411
  111.2 2.8 %copy-start.9 = (bf16[8,256,128]{2,1,0:T(8,128)(2,1)}, bf16[8,256,128]{2,1,0:T(8,128)(2,1)S(1)}, u32[]{:S(2)}) copy-start(bf16[8,256,128]{2,1,0:T(8,128)(2,1)S(1)} %collective-permute-done.3.away) | copy-start | bytes 1572868
  111.2 22.9 %collective-permute-start.5 = (bf16[8,256,128]{2,1,0:T(8,128)(2,1)S(1)}, bf16[8,256,128]{2,1,0:T(8,128)(2,1)S(1)}, u32[]{:S(2)}, u32[]{:S(2)}) collective-permute-start(bf16[8,256,128]{2,1,0:T(8,128)(2,1)S(1)} %collective-permute-done.3.away), channel_id=1, source_target_pairs={{0,1},{1,0},{2,3},{3,2},{4,5},{5,4},{6,7},{7,6},{8,9},{9,8},{10,11... | collective-permute-start | bytes 1572872 | tf_op jit(solution)/shard_map/ppermute | solution.py:411
  114.0 23.0 %all-to-all-start.3 = ((bf16[16,16,128]{2,1,0:T(8,128)(2,1)}), bf16[16,16,128]{2,1,0:T(8,128)(2,1)S(1)}, u32[]{:S(2)}, u32[]{:S(2)}) async-start(bf16[16,16,128]{2,1,0:T(8,128)(2,1)} %get-tuple-element.46), calls=%async_computation.3 | async-start | bytes 131072 | tf_op jit(solution)/shard_map/all_to_all | solution.py:472
  118.7 10.5 %collective-permute-start.6 = (bf16[16,16,128]{2,1,0:T(8,128)(2,1)S(1)}, bf16[16,16,128]{2,1,0:T(8,128)(2,1)S(1)}, u32[]{:S(2)}, u32[]{:S(2)}) collective-permute-start(bf16[16,16,128]{2,1,0:T(8,128)(2,1)S(1)} %get-tuple-element.55), channel_id=1, source_target_pairs={{0,8},{8,0},{16,24},{24,16},{1,9},{9,1},{17,25},{25,17},{2,10},{10... | collective-permute-start | bytes 196616 | tf_op jit(solution)/shard_map/ppermute | solution.py:411
  122.1 7.7 %collective-permute-start.7 = (bf16[16,16,128]{2,1,0:T(8,128)(2,1)S(1)}, bf16[16,16,128]{2,1,0:T(8,128)(2,1)S(1)}, u32[]{:S(2)}, u32[]{:S(2)}) collective-permute-start(bf16[16,16,128]{2,1,0:T(8,128)(2,1)S(1)} %get-tuple-element.54), channel_id=1, source_target_pairs={{0,16},{8,24},{16,0},{24,8},{1,17},{9,25},{17,1},{25,9},{2,18},{10... | collective-permute-start | bytes 196616 | tf_op jit(solution)/shard_map/ppermute | solution.py:411
  126.7 7.4 %collective-permute-start.8 = (bf16[16,16,128]{2,1,0:T(8,128)(2,1)S(1)}, bf16[16,16,128]{2,1,0:T(8,128)(2,1)S(1)}, u32[]{:S(2)}, u32[]{:S(2)}) collective-permute-start(bf16[16,16,128]{2,1,0:T(8,128)(2,1)S(1)} %get-tuple-element.53), channel_id=1, source_target_pairs={{0,24},{8,16},{16,8},{24,0},{1,25},{9,17},{17,9},{25,1},{2,26},{10... | collective-permute-start | bytes 196616 | tf_op jit(solution)/shard_map/ppermute | solution.py:411
